TPU v7x, 512 devices: a whole 4x8x8 slice. The times are simulated.
512 devices in a mesh: fs: 64 (over z, y), tp: 8 (over x, core).
Axes of the slice: x: 4, y: 8, z: 8, core: 2. Of those that a mesh axis runs over, the one named last changes fastest.
Arguments:
- sequence_entries: bfloat16 [16384, 2048], P('fs', 'tp'), may hold values from -6 to 6
- former_norm_factor: float32 [2048], replicated, may hold values from 0.1 to 1.9
- conveyor_matrix: float32 [2048, 1536], P('fs', 'tp'), may hold values from -0.125 to 0.125
- conveyor_rescalers: float32 [1536], P('tp'), may hold values from 0.3 to 3
- blend_value_matrix: float32 [2048, 1536], P('fs', 'tp'), may hold values from -0.125 to 0.125
- blend_rescalers: float32 [1536], P('tp'), may hold values from 0.18 to 4.8, as said below
- blend_norm_factor: float32 [1536], P('tp'), may hold values from 0.1 to 1.9
- location_matrices: bfloat16 [24, 128, 128], P('tp'), may hold values from -0.5 to 0.5
- location_offsets: float32 [24, 128], P('tp'), may hold values from 0.1 to 1.9
- branch_emission_matrix: float32 [1536, 2048], P('tp', 'fs'), may hold values from -0.15625 to 0.15625
- emission_rescalers: float32 [2048], P('fs'), may hold values from 0.3 to 3
- latter_norm_factor: float32 [2048], replicated, may hold values from 0.1 to 1.9
- valve_matrix: float32 [2048, 5632], P('fs', 'tp'), may hold values from -0.125 to 0.125
- valve_rescalers: float32 [5632], P('tp'), may hold values from 0.3 to 3
- raising_matrix: float32 [2048, 5632], P('fs', 'tp'), may hold values from -0.125 to 0.125
- raising_rescalers: float32 [5632], P('tp'), may hold values from 0.3 to 3
- lowering_matrix: float32 [5632, 2048], P('tp', 'fs'), may hold values from -0.078125 to 0.078125
- lowering_rescalers: float32 [2048], P('fs'), may hold values from 0.3 to 3
Outputs:
- layer_out: bfloat16 [16384, 2048], P('fs', 'tp')
Inputs may be any that keep to these rules, and one draw needn't show every extreme that they name: `blend_rescalers`: positive column scales.
All inputs are finite; a program needn't handle non-finite values.
Results may differ from a plain program's by a relative error of at most 0.02.
Values may be sent and summed in bfloat16 or wider, within the bound.
No kernel may reach another device: no remote copies, remote signals or barrier semaphores. Data moves between devices by JAX's collectives and lax.ppermute only.
A program may use at most 64 MiB of HBM per device.

v0:
```python
import jax
import jax.numpy as jnp
from jax import lax
from jax.sharding import Mesh
from jax.sharding import PartitionSpec as P

FS = ("fs_0", "fs_1")


EPS = 1e-06


def gather_turned(arrays, axis, dims):
    turned = [jnp.moveaxis(a, dim, 0) for a, dim in zip(arrays, dims)]
    widths = [t[0].size for t in turned]
    both = jnp.concatenate([t.reshape(-1, w) for t, w in zip(turned, widths)], axis=1)
    filled = lax.all_gather(both, axis, axis=0, tiled=True)
    pieces = jnp.split(filled, [sum(widths[:k]) for k in range(1, len(widths))], axis=1)
    return tuple(
        (
            jnp.moveaxis(b.reshape(-1, *t.shape[1:]), 0, dim)
            for b, t, dim in zip(pieces, turned, dims)
        )
    )


def in_order(pieces, dim):
    shape = list(pieces.shape[1:])
    shape[dim] *= pieces.shape[0]
    return jnp.moveaxis(pieces, 0, dim).reshape(shape)


def from_everyone(x, axis):
    copies = jnp.broadcast_to(x, (lax.axis_size(axis), *x.shape))
    return lax.all_to_all(copies, axis, split_axis=0, concat_axis=0, tiled=True)


def collect(x, axis, dim):
    return in_order(from_everyone(x, axis), dim)


def side_by_side(arrays, axis, dim, along):
    widths = [a.shape[along] for a in arrays]
    both = jnp.concatenate(arrays, axis=along)
    filled = lax.all_gather(both, axis, axis=dim, tiled=True)
    return tuple(jnp.split(filled, [sum(widths[:k]) for k in range(1, len(widths))], axis=along))


def of_everyone(x, axis):
    return from_everyone(x, axis).sum(axis=0)


def split_up(x, dim, size):
    before, after = (x.shape[:dim], x.shape[dim + 1 :])
    return jnp.moveaxis(x.reshape(*before, size, -1, *after), dim, 0)


def summed_on_arrival(x, axis, dim):
    size = lax.axis_size(axis)
    pieces = lax.all_to_all(split_up(x, dim, size), axis, 0, 0, tiled=True)
    return jnp.sum(pieces.astype(jnp.float32), axis=0)


def gather_in_order(x, axes, order):
    pieces = x[None]
    for k in order:
        pieces = lax.all_gather(pieces, axes[k], axis=0, tiled=True)
    block = [lax.axis_size(axes[k]) for k in reversed(order)]
    pieces = pieces.reshape(*block, *x.shape)
    turned = sorted(range(len(order)), key=lambda place: order[len(order) - 1 - place])
    return pieces.transpose(*turned, *range(len(order), pieces.ndim)).reshape(-1, *x.shape)


def whole_of(x, axes, order, dim):
    return in_order(gather_in_order(x, axes, order), dim)


def normalize(rows, gain):
    values = rows.astype(jnp.float32)
    factor = lax.rsqrt(jnp.mean(values * values, axis=-1, keepdims=True) + EPS)
    return (values * factor * gain).astype(jnp.bfloat16)


def elementwise_plus(left_rows, pieces):
    return (
        jnp.dot(left_rows, pieces[0], preferred_element_type=jnp.float32),
        jnp.dot(left_rows, pieces[1], preferred_element_type=jnp.float32),
    )


def project_cols(left_rows, scales, piece):
    return jnp.dot(left_rows, piece, preferred_element_type=jnp.float32) * scales


def on_device(
    sequence_entries,
    former_norm_factor,
    conveyor_matrix,
    conveyor_rescalers,
    blend_value_matrix,
    blend_rescalers,
    blend_norm_factor,
    location_matrices,
    location_offsets,
    branch_emission_matrix,
    emission_rescalers,
    latter_norm_factor,
    valve_matrix,
    valve_rescalers,
    raising_matrix,
    raising_rescalers,
    lowering_matrix,
    lowering_rescalers,
):
    out_scales, down_scales = gather_turned((emission_rescalers, lowering_rescalers), FS, (0, 0))
    full_rows = collect(sequence_entries, "tp", 1)
    standardized_source = normalize(full_rows, former_norm_factor)
    conveyor_prior, stream_prior = elementwise_plus(
        standardized_source,
        side_by_side(
            (conveyor_matrix.astype(jnp.bfloat16), blend_value_matrix.astype(jnp.bfloat16)),
            FS,
            0,
            1,
        ),
    )
    conveyor_current = jax.nn.gelu(conveyor_prior * conveyor_rescalers)
    signal = jax.nn.gelu(stream_prior * blend_rescalers)
    total_sq = of_everyone(jnp.sum(signal * signal, axis=1), "tp")
    channels = signal.shape[1] * lax.axis_size("tp")
    signal_norm = (
        signal * lax.rsqrt(total_sq / channels + EPS)[:, None] * blend_norm_factor
    ).astype(jnp.bfloat16)
    local_groups = location_matrices.shape[0]
    block_len = location_matrices.shape[1]
    group_width = signal.shape[1] // local_groups
    lower_mask = jnp.tril(jnp.ones((block_len, block_len), bool))
    masked = jnp.where(lower_mask[None], location_matrices, jnp.zeros((), jnp.bfloat16))
    signal_blocks = signal_norm.reshape(-1, block_len, local_groups, group_width)
    location_blended = jnp.einsum(
        "gts,bsgd->btgd", masked, signal_blocks, preferred_element_type=jnp.float32
    )
    location_blended = location_blended + location_offsets.T[None, :, :, None]
    filtered_result = (conveyor_current * location_blended.reshape(conveyor_current.shape)).astype(
        jnp.bfloat16
    )
    mixer_terms = project_cols(
        filtered_result, out_scales, collect(branch_emission_matrix.astype(jnp.bfloat16), FS, 1)
    )
    mixer_share = summed_on_arrival(mixer_terms.astype(jnp.bfloat16), "tp", 1)
    mid_own = (sequence_entries.astype(jnp.float32) + mixer_share).astype(jnp.bfloat16)
    mid_rows = collect(mid_own, "tp", 1)
    ffn_in = normalize(mid_rows, latter_norm_factor)
    gate_half = valve_matrix.astype(jnp.bfloat16)
    up_half = raising_matrix.astype(jnp.bfloat16)
    whole_gate, whole_up = side_by_side((gate_half, up_half), FS, 0, 1)
    pre_gate = jnp.dot(ffn_in, whole_gate, preferred_element_type=jnp.float32)
    pre_up = jnp.dot(ffn_in, whole_up, preferred_element_type=jnp.float32)
    hidden = (jax.nn.silu(pre_gate * valve_rescalers) * (pre_up * raising_rescalers)).astype(
        jnp.bfloat16
    )
    ffn_terms = project_cols(
        hidden, down_scales, whole_of(lowering_matrix.astype(jnp.bfloat16), FS, (0, 1), 1)
    )
    ffn_share = summed_on_arrival(ffn_terms.astype(jnp.bfloat16), "tp", 1)
    return (mid_own.astype(jnp.float32) + ffn_share).astype(jnp.bfloat16)


def solution(mesh):
    finer = Mesh(mesh.devices.reshape(8, 8, mesh.shape["tp"]), ("fs_0", "fs_1", "tp"))
    return jax.shard_map(
        on_device,
        mesh=finer,
        in_specs=(
            P(FS, "tp"),
            P(),
            P(FS, "tp"),
            P("tp"),
            P(FS, "tp"),
            P("tp"),
            P("tp"),
            P("tp", None, None),
            P("tp", None),
            P("tp", FS),
            P(FS),
            P(),
            P(FS, "tp"),
            P("tp"),
            P(FS, "tp"),
            P("tp"),
            P("tp", FS),
            P(FS),
        ),
        out_specs=P(FS, "tp"),
        check_vma=False,
    )
```

profile of v0, /device:TPU:1, one launch (start us, length us, event | category | flops | bytes accessed | tf_op | source)
XLA Modules:
  0.0 300.0 jit_solution(10084314948373725602)
XLA Ops:
  6.5 0.8 convert_element_type.90
  7.3 0.8 convert_element_type.89
  8.1 0.7 pad_maximum_fusion.1
  8.8 0.9 convert_bitcast_fusion
  9.7 27.8 %all-gather.2 = bf16[8,704,32]{1,2,0:T(8,128)(2,1)} all-gather(bf16[1,704,32]{1,2,0:T(8,128)(2,1)S(1)} %convert_bitcast_fusion), channel_id=2, replica_groups=mesh['fs_0'=8,'fs_1'=8,'tp'=8] {'fs_0'}, dimensions={0}, use_global_device_ids=true | all-gather | bytes 405504 | tf_op jit(solution)/shard_map/all_gather | solution.py:67
  37.6 0.9 convert_element_type.104
  38.5 0.9 convert_element_type.103
  39.4 0.7 pad_maximum_fusion
  40.2 1.0 copy.49
  41.3 26.3 %all_to_all.31 = bf16[8,256,256]{1,2,0:T(8,128)(2,1)S(1)} all-to-all(bf16[8,256,256]{1,2,0:T(8,128)(2,1)S(1)} %broadcast_in_dim.24), channel_id=1, replica_groups=mesh['fs_0'=8,'fs_1'=8,'tp'=8] {'tp'}, dimensions={0} | all-to-all | bytes 2097152 | tf_op jit(solution)/shard_map/all_to_all | solution.py:35
  67.6 0.3 multiply_reduce_fusion.1
  67.9 0.3 fusion.9
  68.3 25.9 %all-gather.7.cloned.1.call-done = bf16[2048,384]{1,0:T(8,128)(2,1)} async-done(((bf16[32,384]{1,0:T(8,128)(2,1)}), bf16[2048,384]{1,0:T(8,128)(2,1)}) %all-gather.7.cloned.1.call-update) | async-done | bytes 1572880 | tf_op jit(solution)/shard_map/all_gather | solution.py:45
  94.2 2.3 multiply_reduce_fusion.2
  96.6 0.6 broadcast_in_dim.25
  97.2 9.2 %all-to-all-start.1 = ((f32[8,1,256]{2,1,0:T(1,128)}), f32[8,1,256]{2,1,0:T(1,128)S(1)}, u32[]{:S(2)}, u32[]{:S(2)}) async-start(f32[8,1,256]{2,1,0:T(1,128)} %broadcast_in_dim.25), calls=%async_computation.1 | async-start | bytes 16384 | tf_op jit(solution)/shard_map/all_to_all | solution.py:35
  106.4 4.6 %all-to-all-done.1 = f32[8,1,256]{2,1,0:T(1,128)S(1)} async-done(((f32[8,1,256]{2,1,0:T(1,128)}), f32[8,1,256]{2,1,0:T(1,128)S(1)}, u32[]{:S(2)}, u32[]{:S(2)}) %all-to-all-start.1) | async-done | bytes 8224 | tf_op jit(solution)/shard_map/all_to_all | solution.py:35
  111.0 1.1 broadcast_in_dim.46
  112.1 9.0 %all-to-all-start.2 = ((bf16[64,192,32]{1,2,0:T(8,128)(2,1)}), bf16[64,192,32]{1,2,0:T(8,128)(2,1)S(1)}, u32[]{:S(2)}, u32[]{:S(2)}) async-start(bf16[64,192,32]{1,2,0:T(8,128)(2,1)} %broadcast_in_dim.46), calls=%async_computation.2 | async-start | bytes 2097152 | tf_op jit(solution)/shard_map/all_to_all | solution.py:35
  121.2 69.0 %all-gather.1 = f32[64,32,2]{1,2,0:T(2,128)S(1)} all-gather(f32[1,32,2]{1,2,0:T(2,128)S(1)} %maximum_bitcast_fusion), channel_id=1, replica_groups=mesh['fs_0'=8,'fs_1'=8,'tp'=8] {'fs_0','fs_1'}, dimensions={0}, use_global_device_ids=true | all-gather | bytes 16640 | tf_op jit(solution)/shard_map/all_gather | solution.py:17
  190.9 2.5 fusion.5
  193.5 28.3 %all_to_all.32 = bf16[8,256,256]{2,1,0:T(8,128)(2,1)S(1)} all-to-all(bf16[8,256,256]{2,1,0:T(8,128)(2,1)S(1)} %bitcast.78), channel_id=1, replica_groups=mesh['fs_0'=8,'fs_1'=8,'tp'=8] {'tp'}, dimensions={0} | all-to-all | bytes 2097152 | tf_op jit(solution)/shard_map/all_to_all | solution.py:60
  222.2 18.5 %all_to_all.33 = bf16[8,256,256]{1,2,0:T(8,128)(2,1)S(1)} all-to-all(bf16[8,256,256]{1,2,0:T(8,128)(2,1)S(1)} %broadcast_in_dim.47), channel_id=1, replica_groups=mesh['fs_0'=8,'fs_1'=8,'tp'=8] {'tp'}, dimensions={0} | all-to-all | bytes 2097152 | tf_op jit(solution)/shard_map/all_to_all | solution.py:35
  240.7 0.3 multiply_reduce_fusion
  241.0 1.3 fusion.7
  242.3 2.2 copy.56
  244.5 11.6 %all-gather.9.cloned.1.call-done = bf16[2048,1408]{1,0:T(8,128)(2,1)} async-done(((bf16[32,1408]{1,0:T(8,128)(2,1)}), bf16[2048,1408]{1,0:T(8,128)(2,1)}) %all-gather.9.cloned.1.call-update) | async-done | bytes 5767184 | tf_op jit(solution)/shard_map/all_gather | solution.py:45
  256.1 4.4 %fusion.10 = f32[256,704]{0,1:T(8,128)} fusion(bf16[256,2048]{0,1:T(8,128)(2,1)} %fusion.7, bf16[2048,1408]{1,0:T(8,128)(2,1)} %all-gather.9.cloned.1.call-done, f32[704]{0:T(1024)S(1)} %copy-done.9), kind=kOutput, calls=%fused_computation.18 | convolution fusion | flops 738377728 | bytes 4918016 | tf_op jit(solution)/shard_map/dot_general | solution.py:157
  260.5 7.8 %fusion.4 = bf16[256,2048]{1,0:T(8,128)(2,1)} fusion(bf16[704,2048]{0,1:T(8,128)(2,1)S(1)} %bitcast.81, f32[2048]{0:T(1024)S(1)} %bitcast.86, bf16[256,2048]{0,1:T(8,128)(2,1)} %fusion.7, bf16[2048,1408]{1,0:T(8,128)(2,1)} %all-gather.9.cloned.1.call-done, f32[256,704]{0,1:T(8,128)} %fusion.10, f32[704]{0:T(1024)S(1)} %copy-done.10), kind=kOutput, calls=%fused_computation.6 | convolution fusion | flops 1478705152 | bytes 8858368 | tf_op jit(solution)/shard_map/dot_general | solution.py:92
  268.4 1.3 copy.71
  269.7 23.0 %all_to_all.34 = bf16[8,256,256]{2,1,0:T(8,128)(2,1)S(1)} all-to-all(bf16[8,256,256]{2,1,0:T(8,128)(2,1)S(1)} %bitcast.79), channel_id=1, replica_groups=mesh['fs_0'=8,'fs_1'=8,'tp'=8] {'tp'}, dimensions={0} | all-to-all | bytes 2097152 | tf_op jit(solution)/shard_map/all_to_all | solution.py:60
  292.8 0.7 add_convert_fusion
  (55 shorter events, 1.5 us)
Async XLA Ops:
  6.5 87.7 %all-gather.7.cloned.1.call-start = ((), (), s32[]{:S(2)}) async-start(), calls=%async_computation.6 | async-start | bytes 1597440 | tf_op jit(solution)/shard_map/all_gather | solution.py:45
  8.8 233.6 %all-gather.11.cloned.1.call-start = ((), (), s32[]{:S(2)}) async-start(), calls=%async_computation.8 | async-start | bytes 3538944 | tf_op jit(solution)/shard_map/all_gather | solution.py:67
  37.6 218.5 %all-gather.9.cloned.1.call-start = ((), (), s32[]{:S(2)}) async-start(), calls=%async_computation.7 | async-start | bytes 5857280 | tf_op jit(solution)/shard_map/all_gather | solution.py:45
  41.2 26.7 %copy-start.3 = (f32[2048]{0:T(1024)S(1)}, f32[2048]{0:T(1024)}, u32[]{:S(2)}) copy-start(f32[2048]{0:T(1024)} %param.19) | copy-start | bytes 24580
  67.6 26.6 %copy-start.11 = (f32[192]{0:T(256)S(1)}, f32[192]{0:T(256)}, u32[]{:S(2)}) copy-start(f32[192]{0:T(256)} %param.23) | copy-start | bytes 2308
  68.3 38.2 %copy-start.2 = (f32[192,32]{0,1:T(8,128)S(1)}, f32[192,32]{0,1:T(8,128)}, u32[]{:S(2)}) copy-start(f32[192,32]{0,1:T(8,128)} %param.27) | copy-start | bytes 73732
  96.5 24.6 %copy-start.7 = (f32[32]{0:T(128)S(1)}, f32[32]{0:T(128)}, u32[]{:S(2)}) copy-start(f32[32]{0:T(128)} %param.35) | copy-start | bytes 388
  96.5 24.6 %copy-start.8 = (f32[32]{0:T(128)S(1)}, f32[32]{0:T(128)}, u32[]{:S(2)}) copy-start(f32[32]{0:T(128)} %param.28) | copy-start | bytes 388
  96.6 93.8 %copy-start.6 = (f32[192]{0:T(256)S(1)}, f32[192]{0:T(256)}, u32[]{:S(2)}) copy-start(f32[192]{0:T(256)} %param.24) | copy-start | bytes 2308
  96.6 93.9 %copy-start.1 = (bf16[3,128,128]{2,1,0:T(8,128)(2,1)S(1)}, bf16[3,128,128]{2,1,0:T(8,128)(2,1)}, u32[]{:S(2)}) copy-start(bf16[3,128,128]{2,1,0:T(8,128)(2,1)} %param.25) | copy-start | bytes 294916
  96.6 93.9 %copy-start.5 = (f32[3,128]{1,0:T(4,128)S(1)}, f32[3,128]{1,0:T(4,128)}, u32[]{:S(2)}) copy-start(f32[3,128]{1,0:T(4,128)} %param.26) | copy-start | bytes 4612
  97.2 13.8 %all-to-all-start.1 = ((f32[8,1,256]{2,1,0:T(1,128)}), f32[8,1,256]{2,1,0:T(1,128)S(1)}, u32[]{:S(2)}, u32[]{:S(2)}) async-start(f32[8,1,256]{2,1,0:T(1,128)} %broadcast_in_dim.25), calls=%async_computation.1 | async-start | bytes 16384 | tf_op jit(solution)/shard_map/all_to_all | solution.py:35
  112.1 78.8 %copy-start.12 = (f32[192]{0:T(256)S(1)}, f32[192]{0:T(256)}, u32[]{:S(2)}) copy-start(f32[192]{0:T(256)} %param.21) | copy-start | bytes 2308
  112.1 78.8 %all-to-all-start.2 = ((bf16[64,192,32]{1,2,0:T(8,128)(2,1)}), bf16[64,192,32]{1,2,0:T(8,128)(2,1)S(1)}, u32[]{:S(2)}, u32[]{:S(2)}) async-start(bf16[64,192,32]{1,2,0:T(8,128)(2,1)} %broadcast_in_dim.46), calls=%async_computation.2 | async-start | bytes 2097152 | tf_op jit(solution)/shard_map/all_to_all | solution.py:35
  193.5 28.5 %copy-start = (bf16[256,256]{1,0:T(8,128)(2,1)S(1)}, bf16[256,256]{1,0:T(8,128)(2,1)}, u32[]{:S(2)}) copy-start(bf16[256,256]{1,0:T(8,128)(2,1)} %param.18) | copy-start | bytes 393220
  222.2 18.9 %copy-start.4 = (f32[2048]{0:T(1024)S(1)}, f32[2048]{0:T(1024)}, u32[]{:S(2)}) copy-start(f32[2048]{0:T(1024)} %param.29) | copy-start | bytes 24580
  242.3 13.8 %copy-start.9 = (f32[704]{0:T(1024)S(1)}, f32[704]{0:T(1024)}, u32[]{:S(2)}) copy-start(f32[704]{0:T(1024)} %param.31) | copy-start | bytes 8452
  244.5 16.0 %copy-start.10 = (f32[704]{0:T(1024)S(1)}, f32[704]{0:T(1024)}, u32[]{:S(2)}) copy-start(f32[704]{0:T(1024)} %param.33) | copy-start | bytes 8452
Sparse Core Ops, SparseCore 0:
  10.3 83.8 all-gather.6
  96.3 70.5 all-gather.10
  169.8 86.2 all-gather.8
where the time goes:
time: 301 us; the launch traced here: 300 us
  blocking collectives  193 us (64%)
  waiting for transfers between devices  42.1 us (14%)
  starting transfers between devices  18.3 us (6%)
  matrix products  17.3 us (6%)
  between operations  13.4 us (4%)
  other arithmetic  9.09 us (3%)
  local copies, waits for them, and re-layouts  6.88 us (2%)
    all_gather x1, blocking collectives, gather_turned(): filled = lax.all_gather(both, axis, axis=0, tiled=True)  69 us
    all_to_all x2, blocking collectives, summed_on_arrival(): pieces = lax.all_to_all(split_up(x, dim, size), axis, 0, 0, tiled=True)  51.3 us
    all_to_all x2, blocking collectives, from_everyone(): return lax.all_to_all(copies, axis, split_axis=0, concat_axis=0, tiled=True)  44.8 us
    all_gather x2, waiting for transfers between devices, side_by_side(): filled = lax.all_gather(both, axis, axis=dim, tiled=True)  37.5 us
    all_gather x1, blocking collectives, gather_in_order(): pieces = lax.all_gather(pieces, axes[k], axis=0, tiled=True)  27.8 us
    all_to_all x2, starting transfers between devices, from_everyone(): return lax.all_to_all(copies, axis, split_axis=0, concat_axis=0, tiled=True)  18.2 us
    dot_general x2, matrix products, project_cols(): jnp.dot(left_rows, piece, preferred_element_type=jnp.float32) * scales  10.4 us
  transfers between devices with their start and end apart: 5, of which 3 were waited for; matrix products, arithmetic and copies ran while one was open for 6% of the time, Pallas kernels for 0%

commit v1 on v0

v1 whole, which is shorter than its diff:
```python
import jax
import jax.numpy as jnp
from jax import lax
from jax.experimental import pallas as pl
from jax.experimental.pallas import tpu as pltpu
from jax.sharding import Mesh
from jax.sharding import PartitionSpec as P

FS = ("z", "y")
TP = ("x", "c")
EPS = 1e-06
BF = jnp.bfloat16
F32 = jnp.float32
NT = (((1,), (1,)), ((), ()))
VM = pl.BlockSpec(memory_space=pltpu.VMEM)
SM = pl.BlockSpec(memory_space=pltpu.SMEM)
ANY = pl.BlockSpec(memory_space=pl.ANY)


def from_everyone(x, axis):
    copies = jnp.broadcast_to(x, (lax.axis_size(axis), *x.shape))
    return lax.all_to_all(copies, axis, split_axis=0, concat_axis=0, tiled=True)


def gelu(v):
    return 0.5 * v * (1.0 + jnp.tanh(0.7978845608028654 * (v + 0.044715 * v * v * v)))


def project_kernel(order, x_ref, gain, scales, *refs):
    pieces, act_ref, sq_ref = refs[:8], refs[8], refs[9]
    total = jnp.zeros((256, 1), F32)
    for k in range(8):
        v = x_ref[k].astype(F32)
        total = total + jnp.sum(v * v, axis=1, keepdims=True)
    factor = lax.rsqrt(total / 2048.0 + EPS)
    prior = jnp.zeros((256, 384), F32)
    for d in range(8):
        k = order[d]
        rows = (x_ref[k].astype(F32) * factor * gain[k]).astype(BF)
        prior = prior + jnp.dot(rows, pieces[d][:, 0:384], preferred_element_type=F32)
    act = gelu(prior * scales[...])
    act_ref[...] = act
    signal = act[:, 192:384]
    ones = jnp.ones((8, 192), F32)
    sums = lax.dot_general(
        ones, signal * signal, NT, precision=lax.Precision.HIGHEST, preferred_element_type=F32
    )
    sq_ref[...] = sums[0:1]


def gate_kernel(order, act_ref, sq_ref, mats, offs, gain, *refs):
    pieces, out_ref, gated = refs[:8], refs[8], refs[9]
    total = jnp.sum(sq_ref[...], axis=0, keepdims=True)
    factor = lax.rsqrt(total / 1536.0 + EPS)
    rows = lax.broadcasted_iota(jnp.int32, (128, 128), 0)
    cols = lax.broadcasted_iota(jnp.int32, (128, 128), 1)
    lower = cols <= rows
    for g in range(3):
        mat = jnp.where(lower, mats[g].astype(F32), 0.0)
        for b in range(2):
            at = pl.ds(128 * b, 128)
            mix = (mat * factor[:, 128 * b : 128 * b + 128]).astype(BF)
            sig = (act_ref[at, 192 + 64 * g : 256 + 64 * g] * gain[:, 64 * g : 64 * g + 64]).astype(BF)
            mixed = jnp.dot(mix, sig, preferred_element_type=F32) + offs[:, g : g + 1]
            gated[at, 64 * g : 64 * g + 64] = (act_ref[at, 64 * g : 64 * g + 64] * mixed).astype(BF)
    left = gated[...]
    for d in range(8):
        part = lax.dot_general(left, pieces[d][:, 384:576], NT, preferred_element_type=F32)
        out_ref[0, order[d]] = part[0:128].astype(BF)
        out_ref[1, order[d]] = part[128:256].astype(BF)


def ffn_kernel(mid_ref, gain, w_ref, out_ref, w, acc, hid, sems):
    def fetch(k):
        return pltpu.make_async_copy(w_ref.at[k], w.at[k], sems.at[k])

    for k in range(8):
        fetch(k).start()
    total = jnp.zeros((128, 1), F32)
    for k in range(8):
        v = mid_ref[k].astype(F32)
        total = total + jnp.sum(v * v, axis=1, keepdims=True)
    factor = lax.rsqrt(total / 2048.0 + EPS)
    for k in range(8):
        rows = (mid_ref[k].astype(F32) * factor * gain[k]).astype(BF)
        fetch(k).wait()
        for c in range(2):
            piece = w[k, :, c, :, 0:1408].reshape(256, 1408)
            part = jnp.dot(rows, piece, preferred_element_type=F32)
            if k == 0:
                acc[c] = part
            else:
                acc[c] = acc[c] + part
    for c in range(2):
        g = acc[c, :, 0:640]
        u = acc[c, :, 640:1280]
        hid[c, :, 0:640] = (g * jax.nn.sigmoid(g) * u).astype(BF)
        g = acc[c, :, 1280:1344]
        u = acc[c, :, 1344:1408]
        hid[c, :, 640:704] = (g * jax.nn.sigmoid(g) * u).astype(BF)
    for k in range(8):
        part = jnp.zeros((128, 256), F32)
        for c in range(2):
            piece = w[k, :, c, :, 1408:2112].reshape(256, 704)
            part = part + lax.dot_general(hid[c], piece, NT, preferred_element_type=F32)
        out_ref[k] = part.astype(BF)


def on_device(
    sequence_entries,
    former_norm_factor,
    conveyor_matrix,
    conveyor_rescalers,
    blend_value_matrix,
    blend_rescalers,
    blend_norm_factor,
    location_matrices,
    location_offsets,
    branch_emission_matrix,
    emission_rescalers,
    latter_norm_factor,
    valve_matrix,
    valve_rescalers,
    raising_matrix,
    raising_rescalers,
    lowering_matrix,
    lowering_rescalers,
):
    z, x, c = lax.axis_index("z"), lax.axis_index("x"), lax.axis_index("c")
    swap = [(0, 1), (1, 0)]
    emission = (branch_emission_matrix * emission_rescalers).T.astype(BF)
    own = jnp.concatenate(
        [
            conveyor_matrix.astype(BF),
            blend_value_matrix.astype(BF),
            emission,
            jnp.zeros((32, 64), BF),
        ],
        axis=1,
    )
    gate = (valve_matrix * valve_rescalers).astype(BF)
    up = (raising_matrix * raising_rescalers).astype(BF)
    down = (lowering_matrix * lowering_rescalers).T.astype(BF)
    ffn_own = jnp.concatenate([gate[:, :640], up[:, :640], gate[:, 640:], up[:, 640:], down], axis=1)
    ffn_all = lax.all_gather(ffn_own, ("z", "y", "c"), axis=0, tiled=True)

    first = from_everyone(own, "y").reshape(256, 640)
    rows = from_everyone(sequence_entries, TP)
    pieces, order = [first], [z]
    ahead = behind = first
    for step in range(1, 5):
        ahead = lax.ppermute(ahead, "z", [(i, (i + 1) % 8) for i in range(8)])
        pieces.append(ahead)
        order.append((z - step) % 8)
        if step < 4:
            behind = lax.ppermute(behind, "z", [(i, (i - 1) % 8) for i in range(8)])
            pieces.append(behind)
            order.append((z + step) % 8)
    order = jnp.stack(order).astype(jnp.int32)

    act, own_sq = pl.pallas_call(
        project_kernel,
        in_specs=[SM] + [VM] * 11,
        out_specs=[VM, VM],
        out_shape=[jax.ShapeDtypeStruct((256, 384), F32), jax.ShapeDtypeStruct((1, 256), F32)],
        name="project",
    )(
        order,
        rows,
        former_norm_factor.reshape(8, 1, 256),
        jnp.concatenate([conveyor_rescalers, blend_rescalers]).reshape(1, 384),
        *pieces,
    )
    all_sq = lax.all_gather(own_sq, TP, axis=0, tiled=True)
    parts = pl.pallas_call(
        gate_kernel,
        in_specs=[SM] + [VM] * 13,
        out_specs=VM,
        out_shape=jax.ShapeDtypeStruct((2, 8, 128, 256), BF),
        scratch_shapes=[pltpu.VMEM((256, 192), BF)],
        name="gating",
    )(
        order,
        act,
        all_sq,
        location_matrices,
        location_offsets.T,
        blend_norm_factor.reshape(1, 192),
        *pieces,
    )
    kept = lax.dynamic_index_in_dim(parts, c, 0, keepdims=False)
    sent = lax.dynamic_index_in_dim(parts, 1 - c, 0, keepdims=False)
    got = lax.ppermute(sent, "c", swap)
    both = (kept.astype(F32) + got.astype(F32)).astype(BF).reshape(4, 2, 128, 256)
    shares = lax.all_to_all(both, "x", 0, 0, tiled=True)
    base = lax.dynamic_slice(rows, (2 * x, 128 * c, 0), (2, 128, 256))
    mid_own = (base.astype(F32) + jnp.sum(shares.astype(F32), axis=0)).astype(BF)
    mid = lax.all_gather(mid_own, "x", axis=0, tiled=True)
    outs = pl.pallas_call(
        ffn_kernel,
        in_specs=[VM, VM, ANY],
        out_specs=VM,
        out_shape=jax.ShapeDtypeStruct((8, 128, 256), BF),
        scratch_shapes=[
            pltpu.VMEM((8, 8, 2, 32, 2112), BF),
            pltpu.VMEM((2, 128, 1408), F32),
            pltpu.VMEM((2, 128, 704), BF),
            pltpu.SemaphoreType.DMA((8,)),
        ],
        name="ffn",
    )(mid, latter_norm_factor.reshape(8, 1, 256), ffn_all.reshape(8, 8, 2, 32, 2112))
    ffn_shares = lax.all_to_all(outs, TP, 0, 0, tiled=True).reshape(4, 2, 128, 256)
    mid_kept = lax.dynamic_index_in_dim(mid_own, c, 0, keepdims=False)
    mid_sent = lax.dynamic_index_in_dim(mid_own, 1 - c, 0, keepdims=False)
    mid_got = lax.ppermute(mid_sent, "c", swap)
    lower = jnp.where(c == 0, mid_kept, mid_got)
    upper = jnp.where(c == 0, mid_got, mid_kept)
    mid_here = jnp.stack([lower, upper])
    out = mid_here.astype(F32) + jnp.sum(ffn_shares.astype(F32), axis=0)
    return out.astype(BF).reshape(256, 256)


def solution(mesh):
    finer = Mesh(mesh.devices.reshape(8, 8, 4, 2), ("z", "y", "x", "c"))
    return jax.shard_map(
        on_device,
        mesh=finer,
        in_specs=(
            P(FS, TP),
            P(),
            P(FS, TP),
            P(TP),
            P(FS, TP),
            P(TP),
            P(TP),
            P(TP, None, None),
            P(TP, None),
            P(TP, FS),
            P(FS),
            P(),
            P(FS, TP),
            P(TP),
            P(FS, TP),
            P(TP),
            P(TP, FS),
            P(FS),
        ),
        out_specs=P(FS, TP),
        check_vma=False,
    )
```

time: 301 us -> 191 us (0.63)
  blocking collectives: 193 us -> 42.9 us
  starting transfers between devices: 18.3 us -> 53.6 us
  Pallas kernels: 0 us -> 18.8 us
  matrix products: 17.3 us -> 0 us
    all_gather x2, blocking collectives: 96.8 us -> 24.7 us  [the longest x1 14 us: on_device(): all_sq = lax.all_gather(own_sq, TP, axis=0, tiled=True)]
    all_to_all x2 -> x0, blocking collectives: 51.3 us -> none  [summed_on_arrival(): pieces = lax.all_to_all(split_up(x, dim, size), axis, 0, 0, tiled=True)]
    all_gather x3 -> x1, waiting for transfers between devices: 37.5 us -> 0.01 us  [on_device(): ffn_all = lax.all_gather(ffn_own, ('z', 'y', 'c'), axis=0, tiled=True)]
    ppermute x0 -> x9, starting transfers between devices: none -> 33.8 us  [the longest x3 18.9 us: on_device(): behind = lax.ppermute(behind, 'z', [(i, (i - 1) % 8) for i in range(8)])]
    ppermute x0 -> x9, waiting for transfers between devices: none -> 28.7 us  [the longest x4 12.9 us: on_device(): ahead = lax.ppermute(ahead, 'z', [(i, (i + 1) % 8) for i in range(8)])]
    all_to_all x2 -> x1, blocking collectives: 44.8 us -> 18.2 us  [from_everyone(): return lax.all_to_all(copies, axis, split_axis=0, concat_axis=0, tiled=True)]
    pallas_call x0 -> x3, Pallas kernels: none -> 18.8 us  [the longest x1 10.5 us: on_device(): pl.pallas_call(ffn_kernel, in_specs=[VM, VM, ANY], out_specs=VM, out_shap...]
    dot_general x5 -> x0, matrix products: 17.3 us -> none  [the longest x2 10.4 us: project_cols(): jnp.dot(left_rows, piece, preferred_element_type=jnp.float32) * scales]
  transfers between devices with their start and end apart: 5 -> 13, of which waited for: 3 -> 9; matrix products, arithmetic and copies ran while one was open for 6% -> 7% of each run, Pallas kernels for 0% -> 4%
where the time goes in v1:
time: 191 us; the launch traced here: 190 us
  starting transfers between devices  53.6 us (28%)
  waiting for transfers between devices  44.1 us (23%)
  blocking collectives  42.9 us (22%)
  Pallas kernels  18.8 us (10%)
  between operations  13.7 us (7%)
  other arithmetic  9.76 us (5%)
  local copies, waits for them, and re-layouts  7.14 us (4%)
    ppermute x3, starting transfers between devices, on_device(): behind = lax.ppermute(behind, 'z', [(i, (i - 1) % 8) for i in range(8)])  18.9 us
    all_to_all x1, blocking collectives, from_everyone(): return lax.all_to_all(copies, axis, split_axis=0, concat_axis=0, tiled=True)  18.2 us
    all_gather x1, blocking collectives, on_device(): all_sq = lax.all_gather(own_sq, TP, axis=0, tiled=True)  14 us
    ppermute x4, waiting for transfers between devices, on_device(): ahead = lax.ppermute(ahead, 'z', [(i, (i + 1) % 8) for i in range(8)])  12.9 us
    ppermute x3, waiting for transfers between devices, on_device(): behind = lax.ppermute(behind, 'z', [(i, (i - 1) % 8) for i in range(8)])  12.9 us
    ppermute x4, starting transfers between devices, on_device(): ahead = lax.ppermute(ahead, 'z', [(i, (i + 1) % 8) for i in range(8)])  10.8 us
    all_gather x1, blocking collectives, on_device(): mid = lax.all_gather(mid_own, 'x', axis=0, tiled=True)  10.7 us
    pallas_call x1, Pallas kernels, on_device(): pl.pallas_call(ffn_kernel, in_specs=[VM, VM, ANY], out_specs=VM, out_shap...  10.5 us
  transfers between devices with their start and end apart: 13, of which 9 were waited for; matrix products, arithmetic and copies ran while one was open for 7% of the time, Pallas kernels for 4%

profile of v1, /device:TPU:1, one launch (start us, length us, event | category | flops | bytes accessed | tf_op | source)
XLA Modules:
  0.0 190.0 jit_solution(8179723277811461609)
XLA Ops:
  8.4 1.0 fusion.3
  12.7 18.2 %all_to_all.20 = bf16[8,32,640]{2,1,0:T(8,128)(2,1)S(1)} all-to-all(bf16[8,32,640]{2,1,0:T(8,128)(2,1)S(1)} %broadcast_in_dim.15), channel_id=1, replica_groups=mesh['z'=8,'y'=8,'x'=4,'c'=2] {'y'}, dimensions={0} | all-to-all | bytes 655360 | tf_op jit(solution)/shard_map/all_to_all | solution.py:22
  30.9 5.0 %collective-permute-start = (bf16[256,640]{1,0:T(8,128)(2,1)S(1)}, bf16[256,640]{1,0:T(8,128)(2,1)S(1)}, u32[]{:S(2)}, u32[]{:S(2)}) collective-permute-start(bf16[256,640]{1,0:T(8,128)(2,1)S(1)} %bitcast.45), channel_id=1, source_target_pairs={{0,64},{64,128},{128,192},{192,256},{256,320},{320,384},{384,448},... | collective-permute-start | bytes 983048 | tf_op jit(solution)/shard_map/ppermute | solution.py:152
  35.9 8.6 %collective-permute-start.1 = (bf16[256,640]{1,0:T(8,128)(2,1)S(1)}, bf16[256,640]{1,0:T(8,128)(2,1)S(1)}, u32[]{:S(2)}, u32[]{:S(2)}) collective-permute-start(bf16[256,640]{1,0:T(8,128)(2,1)S(1)} %bitcast.46), channel_id=1, source_target_pairs={{0,448},{64,0},{128,64},{192,128},{256,192},{320,256},{384,320},{4... | collective-permute-start | bytes 983048 | tf_op jit(solution)/shard_map/ppermute | solution.py:156
  44.5 5.0 %collective-permute-done.refs_1_ = bf16[256,640]{1,0:T(8,128)(2,1)S(1)} collective-permute-done((bf16[256,640]{1,0:T(8,128)(2,1)S(1)}, bf16[256,640]{1,0:T(8,128)(2,1)S(1)}, u32[]{:S(2)}, u32[]{:S(2)}) %collective-permute-start) | collective-permute-done | bytes 327712 | tf_op jit(solution)/shard_map/ppermute | solution.py:152
  49.5 1.9 %collective-permute-start.2 = (bf16[256,640]{1,0:T(8,128)(2,1)S(1)}, bf16[256,640]{1,0:T(8,128)(2,1)S(1)}, u32[]{:S(2)}, u32[]{:S(2)}) collective-permute-start(bf16[256,640]{1,0:T(8,128)(2,1)S(1)} %collective-permute-done.refs_1_), channel_id=1, source_target_pairs={{0,64},{64,128},{128,192},{192,256},{256,320},{320,384},{384,448},... | collective-permute-start | bytes 983048 | tf_op jit(solution)/shard_map/ppermute | solution.py:152
  51.4 1.9 %broadcast_in_dim.6 = bf16[8,256,256]{2,1,0:T(8,128)(2,1)} broadcast(bf16[256,256]{1,0:T(8,128)(2,1)} %param.18), dimensions={1,2} | broadcast | bytes 1179648 | tf_op jit(solution)/shard_map/broadcast_in_dim | solution.py:21
  53.3 8.2 %all-to-all-start = ((bf16[8,256,256]{2,1,0:T(8,128)(2,1)}), bf16[8,256,256]{2,1,0:T(8,128)(2,1)S(1)}, u32[]{:S(2)}, u32[]{:S(2)}) async-start(bf16[8,256,256]{2,1,0:T(8,128)(2,1)} %broadcast_in_dim.6), calls=%async_computation | async-start | bytes 2097152 | tf_op jit(solution)/shard_map/all_to_all | solution.py:22
  61.5 4.9 %collective-permute-start.3 = (bf16[256,640]{1,0:T(8,128)(2,1)S(1)}, bf16[256,640]{1,0:T(8,128)(2,1)S(1)}, u32[]{:S(2)}, u32[]{:S(2)}) collective-permute-start(bf16[256,640]{1,0:T(8,128)(2,1)S(1)} %collective-permute-done.1.refs_2_), channel_id=1, source_target_pairs={{0,448},{64,0},{128,64},{192,128},{256,192},{320,256},{384,320},{4... | collective-permute-start | bytes 983048 | tf_op jit(solution)/shard_map/ppermute | solution.py:156
  66.4 1.9 %collective-permute-start.4 = (bf16[256,640]{1,0:T(8,128)(2,1)S(1)}, bf16[256,640]{1,0:T(8,128)(2,1)S(1)}, u32[]{:S(2)}, u32[]{:S(2)}) collective-permute-start(bf16[256,640]{1,0:T(8,128)(2,1)S(1)} %collective-permute-done.2.refs_3_), channel_id=1, source_target_pairs={{0,64},{64,128},{128,192},{192,256},{256,320},{320,384},{384,448},... | collective-permute-start | bytes 983048 | tf_op jit(solution)/shard_map/ppermute | solution.py:152
  68.3 6.5 %collective-permute-done.3.refs_4_ = bf16[256,640]{1,0:T(8,128)(2,1)S(1)} collective-permute-done((bf16[256,640]{1,0:T(8,128)(2,1)S(1)}, bf16[256,640]{1,0:T(8,128)(2,1)S(1)}, u32[]{:S(2)}, u32[]{:S(2)}) %collective-permute-start.3) | collective-permute-done | bytes 327712 | tf_op jit(solution)/shard_map/ppermute | solution.py:156
  74.9 5.4 %collective-permute-start.5 = (bf16[256,640]{1,0:T(8,128)(2,1)S(1)}, bf16[256,640]{1,0:T(8,128)(2,1)S(1)}, u32[]{:S(2)}, u32[]{:S(2)}) collective-permute-start(bf16[256,640]{1,0:T(8,128)(2,1)S(1)} %collective-permute-done.3.refs_4_), channel_id=1, source_target_pairs={{0,448},{64,0},{128,64},{192,128},{256,192},{320,256},{384,320},{4... | collective-permute-start | bytes 983048 | tf_op jit(solution)/shard_map/ppermute | solution.py:156
  81.0 2.0 %collective-permute-start.6 = (bf16[256,640]{1,0:T(8,128)(2,1)S(1)}, bf16[256,640]{1,0:T(8,128)(2,1)}, u32[]{:S(2)}, u32[]{:S(2)}) collective-permute-start(bf16[256,640]{1,0:T(8,128)(2,1)S(1)} %collective-permute-done.4.refs_5_), channel_id=1, source_target_pairs={{0,64},{64,128},{128,192},{192,256},{256,320},{320,384},{384,448},... | collective-permute-start | bytes 983048 | tf_op jit(solution)/shard_map/ppermute | solution.py:152
  84.4 1.4 copy.20
  86.5 6.3 %collective-permute-done.5.refs_6_ = bf16[256,640]{1,0:T(8,128)(2,1)S(1)} collective-permute-done((bf16[256,640]{1,0:T(8,128)(2,1)S(1)}, bf16[256,640]{1,0:T(8,128)(2,1)S(1)}, u32[]{:S(2)}, u32[]{:S(2)}) %collective-permute-start.5) | collective-permute-done | bytes 327712 | tf_op jit(solution)/shard_map/ppermute | solution.py:156
  92.8 7.3 %collective-permute-done.6.refs_7_ = bf16[256,640]{1,0:T(8,128)(2,1)} collective-permute-done((bf16[256,640]{1,0:T(8,128)(2,1)S(1)}, bf16[256,640]{1,0:T(8,128)(2,1)}, u32[]{:S(2)}, u32[]{:S(2)}) %collective-permute-start.6) | collective-permute-done | bytes 327712 | tf_op jit(solution)/shard_map/ppermute | solution.py:152
  100.2 4.4 %project.1 = (f32[256,384]{1,0:T(8,128)}, f32[1,256]{1,0:T(1,128)}) custom-call(s32[8]{0:T(128)} %stack.44.order, bf16[8,256,256]{2,1,0:T(8,128)(2,1)} %copy-done, f32[8,1,256]{2,1,0:T(1,128)} %bitcast.52, f32[1,384]{1,0:T(1,128)} %reshape.37.scales, bf16[256,640]{1,0:T(8,128)(2,1)} %bitcast.47, bf16[256,640]{1,0:T(8,128)(2,1)} %copy-done.2, ...), custom_call_target="tpu_custom_call" | custom-call | tf_op jit(solution)/shard_map/project/pallas_call | solution.py:161
  104.6 14.0 %all-gather = f32[8,1,256]{2,1,0:T(1,128)S(1)} all-gather(f32[1,1,256]{2,1,0:T(1,128)} %bitcast.55), channel_id=1, replica_groups=mesh['z'=8,'y'=8,'x'=4,'c'=2] {'x','c'}, dimensions={0}, use_global_device_ids=true | all-gather | bytes 9216 | tf_op jit(solution)/shard_map/all_gather | solution.py:174
  119.2 3.9 %gating.1 = bf16[2,8,128,256]{3,2,1,0:T(8,128)(2,1)} custom-call(s32[8]{0:T(128)} %stack.44.order, f32[256,384]{1,0:T(8,128)} %get-tuple-element.7.act_ref, f32[8,256]{1,0:T(8,128)} %bitcast.51, bf16[3,128,128]{2,1,0:T(8,128)(2,1)} %mats.1, f32[128,3]{1,0:T(8,128)} %bitcast.50, f32[1,192]{1,0:T(1,128)} %bitcast.54, bf16[256,640]{1,0:T(8,128)(2,1)} %bitcast.48, ...), custom_call_target="tpu_custom_call" | custom-call | tf_op jit(solution)/shard_map/gating/pallas_call | solution.py:175
  123.1 1.1 dynamic-slice_bitcast_fusion
  124.2 2.1 %collective-permute-start.7 = (bf16[8,128,256]{2,1,0:T(8,128)(2,1)S(1)}, bf16[8,128,256]{2,1,0:T(8,128)(2,1)S(1)}, u32[]{:S(2)}, u32[]{:S(2)}) collective-permute-start(bf16[8,128,256]{2,1,0:T(8,128)(2,1)S(1)} %dynamic-slice_bitcast_fusion), channel_id=1, source_target_pairs={{0,1},{1,0},{2,3},{3,2},{4,5},{5,4},{6,7},{7,6},{8,9},{9,8},{10,11... | collective-permute-start | bytes 1572872 | tf_op jit(solution)/shard_map/ppermute | solution.py:193
  126.3 1.7 collective-permute-done.7
  128.0 2.0 %fusion = bf16[8,128,256]{2,1,0:T(8,128)(2,1)} fusion(bf16[8,128,256]{2,1,0:T(8,128)(2,1)S(1)} %collective-permute-done.7, bf16[2,8,128,256]{3,2,1,0:T(8,128)(2,1)} %gating.1, s32[]{:T(128)S(6)} %select_n.69), kind=kLoop, calls=%fused_computation.2 | loop fusion | flops 1048576 | bytes 1572868 | tf_op jit(solution)/shard_map/convert_element_type | solution.py:194
  130.0 3.5 %all-to-all-start.2 = ((bf16[4,2,128,256]{3,2,1,0:T(8,128)(2,1)}), bf16[4,2,128,256]{3,2,1,0:T(8,128)(2,1)S(1)}, u32[]{:S(2)}, u32[]{:S(2)}) async-start(bf16[4,2,128,256]{3,2,1,0:T(8,128)(2,1)} %bitcast.16), calls=%async_computation.2 | async-start | bytes 1048576 | tf_op jit(solution)/shard_map/all_to_all | solution.py:195
  133.5 9.2 %all-to-all-done.2 = bf16[4,2,128,256]{3,2,1,0:T(8,128)(2,1)S(1)} async-done(((bf16[4,2,128,256]{3,2,1,0:T(8,128)(2,1)}), bf16[4,2,128,256]{3,2,1,0:T(8,128)(2,1)S(1)}, u32[]{:S(2)}, u32[]{:S(2)}) %all-to-all-start.2) | async-done | bytes 524320 | tf_op jit(solution)/shard_map/all_to_all | solution.py:195
  142.7 1.0 add_convert_fusion.1
  143.7 10.7 %all_gather.10.mid_ref = bf16[8,128,256]{2,1,0:T(8,128)(2,1)} all-gather(bf16[2,128,256]{2,1,0:T(8,128)(2,1)S(1)} %add_convert_fusion.1), channel_id=1, replica_groups=mesh['z'=8,'y'=8,'x'=4,'c'=2] {'x'}, dimensions={0}, use_global_device_ids=true | all-gather | bytes 655360 | tf_op jit(solution)/shard_map/all_gather | solution.py:198
  154.3 10.5 %ffn.1 = bf16[8,128,256]{2,1,0:T(8,128)(2,1)} custom-call(bf16[8,128,256]{2,1,0:T(8,128)(2,1)} %all_gather.10.mid_ref, f32[8,1,256]{2,1,0:T(1,128)} %bitcast.53, bf16[8,8,2,32,2112]{4,3,2,1,0:T(8,128)(2,1)} %bitcast.44), custom_call_target="tpu_custom_call" | custom-call | tf_op jit(solution)/shard_map/ffn/pallas_call | solution.py:199
  164.8 8.2 %all-to-all-start.3 = ((bf16[8,128,256]{2,1,0:T(8,128)(2,1)}), bf16[8,128,256]{2,1,0:T(8,128)(2,1)S(1)}, u32[]{:S(2)}, u32[]{:S(2)}) async-start(bf16[8,128,256]{2,1,0:T(8,128)(2,1)} %ffn.1), calls=%async_computation.3 | async-start | bytes 1048576 | tf_op jit(solution)/shard_map/all_to_all | solution.py:212
  173.0 2.0 %collective-permute-start.8 = (bf16[128,256]{1,0:T(8,128)(2,1)S(1)}, bf16[128,256]{1,0:T(8,128)(2,1)S(1)}, u32[]{:S(2)}, u32[]{:S(2)}) collective-permute-start(bf16[128,256]{1,0:T(8,128)(2,1)S(1)} %dynamic-slice_bitcast_fusion.1), channel_id=1, source_target_pairs={{0,1},{1,0},{2,3},{3,2},{4,5},{5,4},{6,7},{7,6},{8,9},{9,8},{10,11... | collective-permute-start | bytes 196616 | tf_op jit(solution)/shard_map/ppermute | solution.py:215
  175.0 1.1 collective-permute-done.8
  176.2 6.2 %all-to-all-done.3 = bf16[8,128,256]{2,1,0:T(8,128)(2,1)S(1)} async-done(((bf16[8,128,256]{2,1,0:T(8,128)(2,1)}), bf16[8,128,256]{2,1,0:T(8,128)(2,1)S(1)}, u32[]{:S(2)}, u32[]{:S(2)}) %all-to-all-start.3) | async-done | bytes 524320 | tf_op jit(solution)/shard_map/all_to_all | solution.py:212
  (46 shorter events, 9.3 us)
Async XLA Ops:
  6.5 147.8 %all-gather.3.cloned.1.call-start = ((), (), s32[]{:S(2)}) async-start(), calls=%async_computation.4 | async-start | bytes 17965056 | tf_op jit(solution)/shard_map/all_gather | solution.py:145
  30.9 69.2 %copy-start.1 = (bf16[8,32,640]{2,1,0:T(8,128)(2,1)}, bf16[8,32,640]{2,1,0:T(8,128)(2,1)S(1)}, u32[]{:S(2)}) copy-start(bf16[8,32,640]{2,1,0:T(8,128)(2,1)S(1)} %all_to_all.20) | copy-start | bytes 983044
  30.9 18.6 %collective-permute-start = (bf16[256,640]{1,0:T(8,128)(2,1)S(1)}, bf16[256,640]{1,0:T(8,128)(2,1)S(1)}, u32[]{:S(2)}, u32[]{:S(2)}) collective-permute-start(bf16[256,640]{1,0:T(8,128)(2,1)S(1)} %bitcast.45), channel_id=1, source_target_pairs={{0,64},{64,128},{128,192},{192,256},{256,320},{320,384},{384,448},... | collective-permute-start | bytes 983048 | tf_op jit(solution)/shard_map/ppermute | solution.py:152
  35.9 25.6 %collective-permute-start.1 = (bf16[256,640]{1,0:T(8,128)(2,1)S(1)}, bf16[256,640]{1,0:T(8,128)(2,1)S(1)}, u32[]{:S(2)}, u32[]{:S(2)}) collective-permute-start(bf16[256,640]{1,0:T(8,128)(2,1)S(1)} %bitcast.46), channel_id=1, source_target_pairs={{0,448},{64,0},{128,64},{192,128},{256,192},{320,256},{384,320},{4... | collective-permute-start | bytes 983048 | tf_op jit(solution)/shard_map/ppermute | solution.py:156
  49.5 50.6 %copy-start.2 = (bf16[256,640]{1,0:T(8,128)(2,1)}, bf16[256,640]{1,0:T(8,128)(2,1)S(1)}, u32[]{:S(2)}) copy-start(bf16[256,640]{1,0:T(8,128)(2,1)S(1)} %collective-permute-done.refs_1_) | copy-start | bytes 983044
  49.5 16.9 %collective-permute-start.2 = (bf16[256,640]{1,0:T(8,128)(2,1)S(1)}, bf16[256,640]{1,0:T(8,128)(2,1)S(1)}, u32[]{:S(2)}, u32[]{:S(2)}) collective-permute-start(bf16[256,640]{1,0:T(8,128)(2,1)S(1)} %collective-permute-done.refs_1_), channel_id=1, source_target_pairs={{0,64},{64,128},{128,192},{192,256},{256,320},{320,384},{384,448},... | collective-permute-start | bytes 983048 | tf_op jit(solution)/shard_map/ppermute | solution.py:152
  53.3 33.2 %all-to-all-start = ((bf16[8,256,256]{2,1,0:T(8,128)(2,1)}), bf16[8,256,256]{2,1,0:T(8,128)(2,1)S(1)}, u32[]{:S(2)}, u32[]{:S(2)}) async-start(bf16[8,256,256]{2,1,0:T(8,128)(2,1)} %broadcast_in_dim.6), calls=%async_computation | async-start | bytes 2097152 | tf_op jit(solution)/shard_map/all_to_all | solution.py:22
  61.5 38.6 %copy-start.3 = (bf16[256,640]{1,0:T(8,128)(2,1)}, bf16[256,640]{1,0:T(8,128)(2,1)S(1)}, u32[]{:S(2)}) copy-start(bf16[256,640]{1,0:T(8,128)(2,1)S(1)} %collective-permute-done.1.refs_2_) | copy-start | bytes 983044
  61.5 13.3 %collective-permute-start.3 = (bf16[256,640]{1,0:T(8,128)(2,1)S(1)}, bf16[256,640]{1,0:T(8,128)(2,1)S(1)}, u32[]{:S(2)}, u32[]{:S(2)}) collective-permute-start(bf16[256,640]{1,0:T(8,128)(2,1)S(1)} %collective-permute-done.1.refs_2_), channel_id=1, source_target_pairs={{0,448},{64,0},{128,64},{192,128},{256,192},{320,256},{384,320},{4... | collective-permute-start | bytes 983048 | tf_op jit(solution)/shard_map/ppermute | solution.py:156
  66.4 33.7 %copy-start.4 = (bf16[256,640]{1,0:T(8,128)(2,1)}, bf16[256,640]{1,0:T(8,128)(2,1)S(1)}, u32[]{:S(2)}) copy-start(bf16[256,640]{1,0:T(8,128)(2,1)S(1)} %collective-permute-done.2.refs_3_) | copy-start | bytes 983044
  66.4 14.6 %collective-permute-start.4 = (bf16[256,640]{1,0:T(8,128)(2,1)S(1)}, bf16[256,640]{1,0:T(8,128)(2,1)S(1)}, u32[]{:S(2)}, u32[]{:S(2)}) collective-permute-start(bf16[256,640]{1,0:T(8,128)(2,1)S(1)} %collective-permute-done.2.refs_3_), channel_id=1, source_target_pairs={{0,64},{64,128},{128,192},{192,256},{256,320},{320,384},{384,448},... | collective-permute-start | bytes 983048 | tf_op jit(solution)/shard_map/ppermute | solution.py:152
  74.9 25.3 %copy-start.5 = (bf16[256,640]{1,0:T(8,128)(2,1)}, bf16[256,640]{1,0:T(8,128)(2,1)S(1)}, u32[]{:S(2)}) copy-start(bf16[256,640]{1,0:T(8,128)(2,1)S(1)} %collective-permute-done.3.refs_4_) | copy-start | bytes 983044
  74.9 18.0 %collective-permute-start.5 = (bf16[256,640]{1,0:T(8,128)(2,1)S(1)}, bf16[256,640]{1,0:T(8,128)(2,1)S(1)}, u32[]{:S(2)}, u32[]{:S(2)}) collective-permute-start(bf16[256,640]{1,0:T(8,128)(2,1)S(1)} %collective-permute-done.3.refs_4_), channel_id=1, source_target_pairs={{0,448},{64,0},{128,64},{192,128},{256,192},{320,256},{384,320},{4... | collective-permute-start | bytes 983048 | tf_op jit(solution)/shard_map/ppermute | solution.py:156
  81.0 19.2 %copy-start.6 = (bf16[256,640]{1,0:T(8,128)(2,1)}, bf16[256,640]{1,0:T(8,128)(2,1)S(1)}, u32[]{:S(2)}) copy-start(bf16[256,640]{1,0:T(8,128)(2,1)S(1)} %collective-permute-done.4.refs_5_) | copy-start | bytes 983044
  81.0 19.1 %collective-permute-start.6 = (bf16[256,640]{1,0:T(8,128)(2,1)S(1)}, bf16[256,640]{1,0:T(8,128)(2,1)}, u32[]{:S(2)}, u32[]{:S(2)}) collective-permute-start(bf16[256,640]{1,0:T(8,128)(2,1)S(1)} %collective-permute-done.4.refs_5_), channel_id=1, source_target_pairs={{0,64},{64,128},{128,192},{192,256},{256,320},{320,384},{384,448},... | collective-permute-start | bytes 983048 | tf_op jit(solution)/shard_map/ppermute | solution.py:152
  86.5 13.7 %copy-start = (bf16[8,256,256]{2,1,0:T(8,128)(2,1)}, bf16[8,256,256]{2,1,0:T(8,128)(2,1)S(1)}, u32[]{:S(2)}) copy-start(bf16[8,256,256]{2,1,0:T(8,128)(2,1)S(1)} %all-to-all-done.x_ref) | copy-start | bytes 3145732
  92.8 7.3 %copy-start.7 = (bf16[256,640]{1,0:T(8,128)(2,1)}, bf16[256,640]{1,0:T(8,128)(2,1)S(1)}, u32[]{:S(2)}) copy-start(bf16[256,640]{1,0:T(8,128)(2,1)S(1)} %collective-permute-done.5.refs_6_) | copy-start | bytes 983044
  124.2 3.8 %collective-permute-start.7 = (bf16[8,128,256]{2,1,0:T(8,128)(2,1)S(1)}, bf16[8,128,256]{2,1,0:T(8,128)(2,1)S(1)}, u32[]{:S(2)}, u32[]{:S(2)}) collective-permute-start(bf16[8,128,256]{2,1,0:T(8,128)(2,1)S(1)} %dynamic-slice_bitcast_fusion), channel_id=1, source_target_pairs={{0,1},{1,0},{2,3},{3,2},{4,5},{5,4},{6,7},{7,6},{8,9},{9,8},{10,11... | collective-permute-start | bytes 1572872 | tf_op jit(solution)/shard_map/ppermute | solution.py:193
  130.0 12.6 %all-to-all-start.2 = ((bf16[4,2,128,256]{3,2,1,0:T(8,128)(2,1)}), bf16[4,2,128,256]{3,2,1,0:T(8,128)(2,1)S(1)}, u32[]{:S(2)}, u32[]{:S(2)}) async-start(bf16[4,2,128,256]{3,2,1,0:T(8,128)(2,1)} %bitcast.16), calls=%async_computation.2 | async-start | bytes 1048576 | tf_op jit(solution)/shard_map/all_to_all | solution.py:195
  164.8 17.6 %all-to-all-start.3 = ((bf16[8,128,256]{2,1,0:T(8,128)(2,1)}), bf16[8,128,256]{2,1,0:T(8,128)(2,1)S(1)}, u32[]{:S(2)}, u32[]{:S(2)}) async-start(bf16[8,128,256]{2,1,0:T(8,128)(2,1)} %ffn.1), calls=%async_computation.3 | async-start | bytes 1048576 | tf_op jit(solution)/shard_map/all_to_all | solution.py:212
  173.0 3.1 %collective-permute-start.8 = (bf16[128,256]{1,0:T(8,128)(2,1)S(1)}, bf16[128,256]{1,0:T(8,128)(2,1)S(1)}, u32[]{:S(2)}, u32[]{:S(2)}) collective-permute-start(bf16[128,256]{1,0:T(8,128)(2,1)S(1)} %dynamic-slice_bitcast_fusion.1), channel_id=1, source_target_pairs={{0,1},{1,0},{2,3},{3,2},{4,5},{5,4},{6,7},{7,6},{8,9},{9,8},{10,11... | collective-permute-start | bytes 196616 | tf_op jit(solution)/shard_map/ppermute | solution.py:215
Sparse Core Ops, SparseCore 0:
  10.5 119.6 all-gather.2

commit v2 on v1

--- a/solution.py
+++ b/solution.py
@@ -26,48 +26,104 @@
     return 0.5 * v * (1.0 + jnp.tanh(0.7978845608028654 * (v + 0.044715 * v * v * v)))
 
 
-def project_kernel(order, x_ref, gain, scales, *refs):
-    pieces, act_ref, sq_ref = refs[:8], refs[8], refs[9]
+def upright(row, n):
+    same = lax.broadcasted_iota(jnp.int32, (n, n), 0) == lax.broadcasted_iota(jnp.int32, (n, n), 1)
+    return jnp.sum(jnp.where(same, row.reshape(1, n), 0.0), axis=1, keepdims=True)
+
+
+def pack_kernel(conv, blend, emis, emis_s, valve, valve_s, raising, raising_s, low, low_s, own, ffn):
+    emission = emis[...] * upright(emis_s[...], 32)
+    packed = jnp.concatenate([conv[...], blend[...], emission, jnp.zeros((32, 64), F32)], axis=1)
+    packed = packed.astype(BF)
+    for k in range(8):
+        own[k] = packed
+    gate = valve[...] * valve_s[...].reshape(1, 704)
+    up = raising[...] * raising_s[...].reshape(1, 704)
+    ffn[:, 0:640] = gate[:, 0:640].astype(BF)
+    ffn[:, 640:1280] = up[:, 0:640].astype(BF)
+    ffn[:, 1280:1408] = jnp.concatenate([gate[:, 640:704], up[:, 640:704]], axis=1).astype(BF)
+    ffn[:, 1408:2112] = (low[...] * upright(low_s[...], 32)).astype(BF)
+
+
+def spread(order, left, right):
+    found = []
+    for half, refs in enumerate((left, right)):
+        place = 0
+        for ref in refs:
+            for k in range(ref.shape[0]):
+                found.append((order[half, place], half, ref, k))
+                place += 1
+    return found
+
+
+def project_kernel(order, x_ref, gain, conv_s, blend_s, *refs):
+    pieces, act_ref, sq_ref = refs[:10], refs[10], refs[11]
     total = jnp.zeros((256, 1), F32)
     for k in range(8):
         v = x_ref[k].astype(F32)
         total = total + jnp.sum(v * v, axis=1, keepdims=True)
     factor = lax.rsqrt(total / 2048.0 + EPS)
     prior = jnp.zeros((256, 384), F32)
-    for d in range(8):
-        k = order[d]
-        rows = (x_ref[k].astype(F32) * factor * gain[k]).astype(BF)
-        prior = prior + jnp.dot(rows, pieces[d][:, 0:384], preferred_element_type=F32)
-    act = gelu(prior * scales[...])
+    for block, half, ref, k in spread(order, pieces[:5], pieces[5:]):
+        cols = pl.ds(128 * half, 128)
+        rows = (x_ref[block, :, cols].astype(F32) * factor * gain[block, :, cols]).astype(BF)
+        prior = prior + jnp.dot(rows, ref[k, :, 0:384], preferred_element_type=F32)
+    scales = jnp.concatenate([conv_s[...].reshape(1, 192), blend_s[...].reshape(1, 192)], axis=1)
+    act = gelu(prior * scales)
     act_ref[...] = act
     signal = act[:, 192:384]
     ones = jnp.ones((8, 192), F32)
     sums = lax.dot_general(
         ones, signal * signal, NT, precision=lax.Precision.HIGHEST, preferred_element_type=F32
     )
-    sq_ref[...] = sums[0:1]
-
-
-def gate_kernel(order, act_ref, sq_ref, mats, offs, gain, *refs):
-    pieces, out_ref, gated = refs[:8], refs[8], refs[9]
-    total = jnp.sum(sq_ref[...], axis=0, keepdims=True)
+    sq_ref[0] = sums[0:1]
+
+
+def gate_kernel(order, core, act_ref, sq_ref, mats, offs, gain, *refs):
+    pieces, kept, sent, gated = refs[:10], refs[10], refs[11], refs[12]
+    total = jnp.sum(sq_ref[...], axis=0)
     factor = lax.rsqrt(total / 1536.0 + EPS)
     rows = lax.broadcasted_iota(jnp.int32, (128, 128), 0)
     cols = lax.broadcasted_iota(jnp.int32, (128, 128), 1)
     lower = cols <= rows
+    gains = gain[...].reshape(1, 192)
     for g in range(3):
         mat = jnp.where(lower, mats[g].astype(F32), 0.0)
         for b in range(2):
             at = pl.ds(128 * b, 128)
             mix = (mat * factor[:, 128 * b : 128 * b + 128]).astype(BF)
-            sig = (act_ref[at, 192 + 64 * g : 256 + 64 * g] * gain[:, 64 * g : 64 * g + 64]).astype(BF)
-            mixed = jnp.dot(mix, sig, preferred_element_type=F32) + offs[:, g : g + 1]
-            gated[at, 64 * g : 64 * g + 64] = (act_ref[at, 64 * g : 64 * g + 64] * mixed).astype(BF)
-    left = gated[...]
-    for d in range(8):
-        part = lax.dot_general(left, pieces[d][:, 384:576], NT, preferred_element_type=F32)
-        out_ref[0, order[d]] = part[0:128].astype(BF)
-        out_ref[1, order[d]] = part[128:256].astype(BF)
+            sig = (act_ref[at, 192 + 64 * g : 256 + 64 * g] * gains[:, 64 * g : 64 * g + 64]).astype(BF)
+            mixed = jnp.dot(mix, sig, preferred_element_type=F32) + upright(offs[g], 128)
+            gated[b, :, 64 * g : 64 * g + 64] = (
+                act_ref[at, 64 * g : 64 * g + 64] * mixed
+            ).astype(BF)
+    here = core[0]
+    mine, other = gated[here], gated[1 - here]
+    for block, half, ref, k in spread(order, pieces[:5], pieces[5:]):
+        piece = ref[k, :, 384:576]
+        cols = pl.ds(128 * half, 128)
+        part = lax.dot_general(mine, piece, NT, preferred_element_type=F32)
+        kept[block, :, cols] = part.astype(BF)
+        part = lax.dot_general(other, piece, NT, preferred_element_type=F32)
+        sent[block, :, cols] = part.astype(BF)
+
+
+def exchange(own, flip):
+    to_pair = [(i, (((i + flip) ^ 1) - flip) % 8) for i in range(8)]
+    to_next = [(i, (((i + 1 - flip) ^ 1) - 1 + flip) % 8) for i in range(8)]
+    got = lax.ppermute(own, "z", to_pair)
+    batch = jnp.concatenate([own, got])
+    pieces = [own, got]
+    for turn in (to_next, to_pair, to_next):
+        batch = lax.ppermute(batch, "z", turn)
+        pieces.append(batch)
+    return pieces
+
+
+def blocks(z):
+    out = 2 * ((z + jnp.arange(2)) & 1) - 1
+    steps = jnp.array([0, -1, 1, 2, -2, -3, 3, 4])
+    return ((z + out[:, None] * steps) & 7).astype(jnp.int32)
 
 
 def ffn_kernel(mid_ref, gain, w_ref, out_ref, w, acc, hid, sems):
@@ -128,68 +184,65 @@
 ):
     z, x, c = lax.axis_index("z"), lax.axis_index("x"), lax.axis_index("c")
     swap = [(0, 1), (1, 0)]
-    emission = (branch_emission_matrix * emission_rescalers).T.astype(BF)
-    own = jnp.concatenate(
-        [
-            conveyor_matrix.astype(BF),
-            blend_value_matrix.astype(BF),
-            emission,
-            jnp.zeros((32, 64), BF),
-        ],
-        axis=1,
-    )
-    gate = (valve_matrix * valve_rescalers).astype(BF)
-    up = (raising_matrix * raising_rescalers).astype(BF)
-    down = (lowering_matrix * lowering_rescalers).T.astype(BF)
-    ffn_own = jnp.concatenate([gate[:, :640], up[:, :640], gate[:, 640:], up[:, 640:], down], axis=1)
+    own, ffn_own = pl.pallas_call(
+        pack_kernel,
+        in_specs=[VM] * 10,
+        out_specs=[VM, VM],
+        out_shape=[jax.ShapeDtypeStruct((8, 32, 640), BF), jax.ShapeDtypeStruct((32, 2112), BF)],
+        name="pack",
+    )(
+        conveyor_matrix,
+        blend_value_matrix,
+        branch_emission_matrix.T,
+        emission_rescalers,
+        valve_matrix,
+        valve_rescalers,
+        raising_matrix,
+        raising_rescalers,
+        lowering_matrix.T,
+        lowering_rescalers,
+    )
     ffn_all = lax.all_gather(ffn_own, ("z", "y", "c"), axis=0, tiled=True)
 
-    first = from_everyone(own, "y").reshape(256, 640)
+    first = lax.all_to_all(own, "y", 0, 0, tiled=True)
     rows = from_everyone(sequence_entries, TP)
-    pieces, order = [first], [z]
-    ahead = behind = first
-    for step in range(1, 5):
-        ahead = lax.ppermute(ahead, "z", [(i, (i + 1) % 8) for i in range(8)])
-        pieces.append(ahead)
-        order.append((z - step) % 8)
-        if step < 4:
-            behind = lax.ppermute(behind, "z", [(i, (i - 1) % 8) for i in range(8)])
-            pieces.append(behind)
-            order.append((z + step) % 8)
-    order = jnp.stack(order).astype(jnp.int32)
+    left = exchange(first[:4].reshape(1, 128, 640), 0)
+    right = exchange(first[4:].reshape(1, 128, 640), 1)
+    pieces = left + right
+    order = blocks(z)
 
     act, own_sq = pl.pallas_call(
         project_kernel,
-        in_specs=[SM] + [VM] * 11,
+        in_specs=[SM] + [VM] * 14,
         out_specs=[VM, VM],
-        out_shape=[jax.ShapeDtypeStruct((256, 384), F32), jax.ShapeDtypeStruct((1, 256), F32)],
+        out_shape=[jax.ShapeDtypeStruct((256, 384), F32), jax.ShapeDtypeStruct((1, 1, 256), F32)],
         name="project",
     )(
         order,
         rows,
         former_norm_factor.reshape(8, 1, 256),
-        jnp.concatenate([conveyor_rescalers, blend_rescalers]).reshape(1, 384),
+        conveyor_rescalers,
+        blend_rescalers,
         *pieces,
     )
     all_sq = lax.all_gather(own_sq, TP, axis=0, tiled=True)
-    parts = pl.pallas_call(
+    kept, sent = pl.pallas_call(
         gate_kernel,
-        in_specs=[SM] + [VM] * 13,
-        out_specs=VM,
-        out_shape=jax.ShapeDtypeStruct((2, 8, 128, 256), BF),
-        scratch_shapes=[pltpu.VMEM((256, 192), BF)],
+        in_specs=[SM, SM] + [VM] * 15,
+        out_specs=[VM, VM],
+        out_shape=[jax.ShapeDtypeStruct((8, 128, 256), BF)] * 2,
+        scratch_shapes=[pltpu.VMEM((2, 128, 192), BF)],
         name="gating",
     )(
         order,
+        c.astype(jnp.int32).reshape(1),
         act,
         all_sq,
         location_matrices,
-        location_offsets.T,
-        blend_norm_factor.reshape(1, 192),
+        location_offsets,
+        blend_norm_factor,
         *pieces,
     )
-    kept = lax.dynamic_index_in_dim(parts, c, 0, keepdims=False)
-    sent = lax.dynamic_index_in_dim(parts, 1 - c, 0, keepdims=False)
     got = lax.ppermute(sent, "c", swap)
     both = (kept.astype(F32) + got.astype(F32)).astype(BF).reshape(4, 2, 128, 256)
     shares = lax.all_to_all(both, "x", 0, 0, tiled=True)

time: 191 us -> 182 us (0.953)
  waiting for transfers between devices: 44.1 us -> 38.6 us
  local copies, waits for them, and re-layouts: 7.14 us -> 2.01 us
  starting transfers between devices: 53.6 us -> 58.6 us
  other arithmetic: 9.76 us -> 5.16 us
  Pallas kernels: 18.8 us -> 21.5 us
    ppermute x7 -> x8, waiting for transfers between devices: 25.8 us -> 19.5 us  [the longest x6 19.5 us: exchange(): batch = lax.ppermute(batch, 'z', turn)]
    ppermute x7 -> x8, starting transfers between devices: 29.7 us -> 35.3 us  [the longest x6 20.7 us: exchange(): batch = lax.ppermute(batch, 'z', turn)]
    convert_element_type x6 -> x0, other arithmetic: 5.14 us -> none  [the longest x1 0.97 us: on_device(): down = (lowering_matrix * lowering_rescalers).T.astype(BF)]
    pallas_call x2 -> x3, Pallas kernels: 8.33 us -> 11 us  [the longest x1 4.87 us: on_device(): pl.pallas_call(project_kernel, in_specs=[SM] + [VM] * 14, out_specs=[VM,...]
    unnamed x18 -> x20, local copies, waits for them, and re-layouts: 2.05 us -> 0.04 us
  transfers between devices with their start and end apart: 13 -> 14, of which waited for: 9 -> 7; matrix products, arithmetic and copies ran while one was open for 7% -> 4% of each run, Pallas kernels for 4% -> 5%
where the time goes in v2:
time: 182 us; the launch traced here: 181 us
  starting transfers between devices  58.6 us (32%)
  blocking collectives  41.5 us (23%)
  waiting for transfers between devices  38.6 us (21%)
  Pallas kernels  21.5 us (12%)
  between operations  13.7 us (8%)
  other arithmetic  5.16 us (3%)
  local copies, waits for them, and re-layouts  2.01 us (1%)
    ppermute x6, starting transfers between devices, exchange(): batch = lax.ppermute(batch, 'z', turn)  20.7 us
    ppermute x6, waiting for transfers between devices, exchange(): batch = lax.ppermute(batch, 'z', turn)  19.5 us
    all_to_all x1, blocking collectives, on_device(): first = lax.all_to_all(own, 'y', 0, 0, tiled=True)  17.6 us
    ppermute x2, starting transfers between devices, exchange(): got = lax.ppermute(own, 'z', to_pair)  14.6 us
    all_gather x1, blocking collectives, on_device(): all_sq = lax.all_gather(own_sq, TP, axis=0, tiled=True)  13.2 us
    all_gather x1, blocking collectives, on_device(): mid = lax.all_gather(mid_own, 'x', axis=0, tiled=True)  10.6 us
    pallas_call x1, Pallas kernels, on_device(): pl.pallas_call(ffn_kernel, in_specs=[VM, VM, ANY], out_specs=VM, out_shap...  10.5 us
    all_to_all x1, waiting for transfers between devices, on_device(): shares = lax.all_to_all(both, 'x', 0, 0, tiled=True)  9.38 us
  transfers between devices with their start and end apart: 14, of which 7 were waited for; matrix products, arithmetic and copies ran while one was open for 4% of the time, Pallas kernels for 5%

profile of v2, /device:TPU:1, one launch (start us, length us, event | category | flops | bytes accessed | tf_op | source)
XLA Modules:
  0.0 181.1 jit_solution(16805712044667052030)
XLA Ops:
  6.5 2.0 %pack.1 = (bf16[8,32,640]{2,1,0:T(8,128)(2,1)}, bf16[32,2112]{1,0:T(8,128)(2,1)}) custom-call(f32[32,192]{1,0:T(8,128)} %conv.1, f32[32,192]{1,0:T(8,128)} %blend.1, f32[32,192]{1,0:T(8,128)} %bitcast.36, f32[32]{0:T(128)} %emis_s.1, f32[32,704]{1,0:T(8,128)} %valve.1, f32[704]{0:T(1024)} %valve_s.1, f32[32,704]{1,0:T(8,128)} %raising.1, f32[704]{0:T(1024)} %raising_s.1, ...), custom_call_target="tpu_custom_call" | custom-call | tf_op jit(solution)/shard_map/pack/pallas_call | solution.py:187
  8.6 17.6 %all_to_all.20 = bf16[8,32,640]{2,1,0:T(8,128)(2,1)S(1)} all-to-all(bf16[8,32,640]{2,1,0:T(8,128)(2,1)} %get-tuple-element.11), channel_id=1, replica_groups=mesh['z'=8,'y'=8,'x'=4,'c'=2] {'y'}, dimensions={0} | all-to-all | bytes 655360 | tf_op jit(solution)/shard_map/all_to_all | solution.py:207
  26.3 5.8 %collective-permute-start = (bf16[1,128,640]{2,1,0:T(8,128)(2,1)S(1)}, bf16[1,128,640]{2,1,0:T(8,128)(2,1)S(1)}, u32[]{:S(2)}, u32[]{:S(2)}) collective-permute-start(bf16[1,128,640]{2,1,0:T(8,128)(2,1)S(1)} %bitcast.30), channel_id=1, source_target_pairs={{0,64},{64,0},{128,192},{192,128},{256,320},{320,256},{384,448},{4... | collective-permute-start | bytes 491528 | tf_op jit(solution)/shard_map/ppermute | solution.py:114
  32.0 8.8 %collective-permute-start.4 = (bf16[1,128,640]{2,1,0:T(8,128)(2,1)S(1)}, bf16[1,128,640]{2,1,0:T(8,128)(2,1)S(1)}, u32[]{:S(2)}, u32[]{:S(2)}) collective-permute-start(bf16[1,128,640]{2,1,0:T(8,128)(2,1)S(1)} %bitcast.26), channel_id=1, source_target_pairs={{0,448},{64,128},{128,64},{192,256},{256,192},{320,384},{384,320},... | collective-permute-start | bytes 491528 | tf_op jit(solution)/shard_map/ppermute | solution.py:114
  40.9 4.8 %collective-permute-start.1 = (bf16[2,128,640]{2,1,0:T(8,128)(2,1)S(1)}, bf16[2,128,640]{2,1,0:T(8,128)(2,1)S(1)}, u32[]{:S(2)}, u32[]{:S(2)}) collective-permute-start(bf16[2,128,640]{2,1,0:T(8,128)(2,1)S(1)} %pad_maximum_fusion), channel_id=1, source_target_pairs={{0,448},{64,128},{128,64},{192,256},{256,192},{320,384},{384,320},... | collective-permute-start | bytes 983048 | tf_op jit(solution)/shard_map/ppermute | solution.py:118
  45.8 1.9 %collective-permute-start.5 = (bf16[2,128,640]{2,1,0:T(8,128)(2,1)S(1)}, bf16[2,128,640]{2,1,0:T(8,128)(2,1)S(1)}, u32[]{:S(2)}, u32[]{:S(2)}) collective-permute-start(bf16[2,128,640]{2,1,0:T(8,128)(2,1)S(1)} %pad_maximum_fusion.1), channel_id=1, source_target_pairs={{0,64},{64,0},{128,192},{192,128},{256,320},{320,256},{384,448},{4... | collective-permute-start | bytes 983048 | tf_op jit(solution)/shard_map/ppermute | solution.py:118
  47.7 1.9 %broadcast_in_dim.2 = bf16[8,256,256]{2,1,0:T(8,128)(2,1)} broadcast(bf16[256,256]{1,0:T(8,128)(2,1)} %param.19), dimensions={1,2} | broadcast | bytes 1179648 | tf_op jit(solution)/shard_map/broadcast_in_dim | solution.py:21
  49.6 7.8 %all-to-all-start = ((bf16[8,256,256]{2,1,0:T(8,128)(2,1)}), bf16[8,256,256]{2,1,0:T(8,128)(2,1)S(1)}, u32[]{:S(2)}, u32[]{:S(2)}) async-start(bf16[8,256,256]{2,1,0:T(8,128)(2,1)} %broadcast_in_dim.2), calls=%async_computation | async-start | bytes 2097152 | tf_op jit(solution)/shard_map/all_to_all | solution.py:22
  57.5 3.6 %collective-permute-start.2 = (bf16[2,128,640]{2,1,0:T(8,128)(2,1)S(1)}, bf16[2,128,640]{2,1,0:T(8,128)(2,1)S(1)}, u32[]{:S(2)}, u32[]{:S(2)}) collective-permute-start(bf16[2,128,640]{2,1,0:T(8,128)(2,1)S(1)} %collective-permute-done.1.refs_2_), channel_id=1, source_target_pairs={{0,64},{64,0},{128,192},{192,128},{256,320},{320,256},{384,448},{4... | collective-permute-start | bytes 983048 | tf_op jit(solution)/shard_map/ppermute | solution.py:118
  61.2 3.6 %collective-permute-start.6 = (bf16[2,128,640]{2,1,0:T(8,128)(2,1)S(1)}, bf16[2,128,640]{2,1,0:T(8,128)(2,1)S(1)}, u32[]{:S(2)}, u32[]{:S(2)}) collective-permute-start(bf16[2,128,640]{2,1,0:T(8,128)(2,1)S(1)} %collective-permute-done.5.refs_7_), channel_id=1, source_target_pairs={{0,448},{64,128},{128,64},{192,256},{256,192},{320,384},{384,320},... | collective-permute-start | bytes 983048 | tf_op jit(solution)/shard_map/ppermute | solution.py:118
  64.8 4.4 %collective-permute-done.2.refs_3_ = bf16[2,128,640]{2,1,0:T(8,128)(2,1)S(1)} collective-permute-done((bf16[2,128,640]{2,1,0:T(8,128)(2,1)S(1)}, bf16[2,128,640]{2,1,0:T(8,128)(2,1)S(1)}, u32[]{:S(2)}, u32[]{:S(2)}) %collective-permute-start.2) | collective-permute-done | bytes 327712 | tf_op jit(solution)/shard_map/ppermute | solution.py:118
  69.2 4.8 %collective-permute-start.3 = (bf16[2,128,640]{2,1,0:T(8,128)(2,1)S(1)}, bf16[2,128,640]{2,1,0:T(8,128)(2,1)S(1)}, u32[]{:S(2)}, u32[]{:S(2)}) collective-permute-start(bf16[2,128,640]{2,1,0:T(8,128)(2,1)S(1)} %collective-permute-done.2.refs_3_), channel_id=1, source_target_pairs={{0,448},{64,128},{128,64},{192,256},{256,192},{320,384},{384,320},... | collective-permute-start | bytes 983048 | tf_op jit(solution)/shard_map/ppermute | solution.py:118
  74.0 1.9 %collective-permute-start.7 = (bf16[2,128,640]{2,1,0:T(8,128)(2,1)S(1)}, bf16[2,128,640]{2,1,0:T(8,128)(2,1)}, u32[]{:S(2)}, u32[]{:S(2)}) collective-permute-start(bf16[2,128,640]{2,1,0:T(8,128)(2,1)S(1)} %collective-permute-done.6.refs_8_), channel_id=1, source_target_pairs={{0,64},{64,0},{128,192},{192,128},{256,320},{320,256},{384,448},{4... | collective-permute-start | bytes 983048 | tf_op jit(solution)/shard_map/ppermute | solution.py:118
  76.0 1.3 add_and_fusion.order
  77.3 11.0 %collective-permute-done.3.refs_4_ = bf16[2,128,640]{2,1,0:T(8,128)(2,1)S(1)} collective-permute-done((bf16[2,128,640]{2,1,0:T(8,128)(2,1)S(1)}, bf16[2,128,640]{2,1,0:T(8,128)(2,1)S(1)}, u32[]{:S(2)}, u32[]{:S(2)}) %collective-permute-start.3) | collective-permute-done | bytes 327712 | tf_op jit(solution)/shard_map/ppermute | solution.py:118
  88.2 4.1 %collective-permute-done.7.refs_9_ = bf16[2,128,640]{2,1,0:T(8,128)(2,1)} collective-permute-done((bf16[2,128,640]{2,1,0:T(8,128)(2,1)S(1)}, bf16[2,128,640]{2,1,0:T(8,128)(2,1)}, u32[]{:S(2)}, u32[]{:S(2)}) %collective-permute-start.7) | collective-permute-done | bytes 327712 | tf_op jit(solution)/shard_map/ppermute | solution.py:118
  92.5 4.9 %project.1 = (f32[256,384]{1,0:T(8,128)}, f32[1,1,256]{2,1,0:T(1,128)}) custom-call(s32[2,8]{1,0:T(2,128)} %add_and_fusion.order, bf16[8,256,256]{2,1,0:T(8,128)(2,1)} %copy-done, f32[8,1,256]{2,1,0:T(1,128)} %bitcast.37, f32[192]{0:T(256)} %conv_s.1, f32[192]{0:T(256)} %blend_s.1, bf16[1,128,640]{2,1,0:T(8,128)(2,1)} %bitcast.32, ...), custom_call_target="tpu_custom_call" | custom-call | tf_op jit(solution)/shard_map/project/pallas_call | solution.py:214
  97.3 13.2 %all_gather.9.sq_ref = f32[8,1,256]{2,1,0:T(1,128)} all-gather(f32[1,1,256]{2,1,0:T(1,128)} %get-tuple-element.13), channel_id=1, replica_groups=mesh['z'=8,'y'=8,'x'=4,'c'=2] {'x','c'}, dimensions={0}, use_global_device_ids=true | all-gather | bytes 9216 | tf_op jit(solution)/shard_map/all_gather | solution.py:228
  110.6 4.2 %gating.1 = (bf16[8,128,256]{2,1,0:T(8,128)(2,1)}, bf16[8,128,256]{2,1,0:T(8,128)(2,1)}) custom-call(s32[2,8]{1,0:T(2,128)} %add_and_fusion.order, s32[1]{0:T(128)} %bitcast.core, f32[256,384]{1,0:T(8,128)} %get-tuple-element.12.act_ref, f32[8,1,256]{2,1,0:T(1,128)} %all_gather.9.sq_ref, bf16[3,128,128]{2,1,0:T(8,128)(2,1)} %mats.1, f32[3,128]{1,0:T(4,128)} %offs.1, ...), custom_call_target="tpu_custom_call" | custom-call | tf_op jit(solution)/shard_map/gating/pallas_call | solution.py:229
  114.7 2.0 %collective-permute-start.8 = (bf16[8,128,256]{2,1,0:T(8,128)(2,1)}, bf16[8,128,256]{2,1,0:T(8,128)(2,1)S(1)}, u32[]{:S(2)}, u32[]{:S(2)}) collective-permute-start(bf16[8,128,256]{2,1,0:T(8,128)(2,1)} %get-tuple-element.15), channel_id=1, source_target_pairs={{0,1},{1,0},{2,3},{3,2},{4,5},{5,4},{6,7},{7,6},{8,9},{9,8},{10,11... | collective-permute-start | bytes 1572872 | tf_op jit(solution)/shard_map/ppermute | solution.py:246
  116.8 2.4 %collective-permute-done.8 = bf16[8,128,256]{2,1,0:T(8,128)(2,1)S(1)} collective-permute-done((bf16[8,128,256]{2,1,0:T(8,128)(2,1)}, bf16[8,128,256]{2,1,0:T(8,128)(2,1)S(1)}, u32[]{:S(2)}, u32[]{:S(2)}) %collective-permute-start.8) | collective-permute-done | bytes 524320 | tf_op jit(solution)/shard_map/ppermute | solution.py:246
  119.1 2.0 %add_convert_fusion = bf16[8,128,256]{2,1,0:T(8,128)(2,1)} fusion(bf16[8,128,256]{2,1,0:T(8,128)(2,1)S(1)} %collective-permute-done.8, bf16[8,128,256]{2,1,0:T(8,128)(2,1)} %get-tuple-element.14), kind=kLoop, calls=%fused_computation.2 | loop fusion | flops 1048576 | bytes 1572864 | tf_op jit(solution)/shard_map/convert_element_type | solution.py:247
  121.1 3.5 %all-to-all-start.2 = ((bf16[4,2,128,256]{3,2,1,0:T(8,128)(2,1)}), bf16[4,2,128,256]{3,2,1,0:T(8,128)(2,1)S(1)}, u32[]{:S(2)}, u32[]{:S(2)}) async-start(bf16[4,2,128,256]{3,2,1,0:T(8,128)(2,1)} %bitcast.6), calls=%async_computation.2 | async-start | bytes 1048576 | tf_op jit(solution)/shard_map/all_to_all | solution.py:248
  124.6 9.4 %all-to-all-done.2 = bf16[4,2,128,256]{3,2,1,0:T(8,128)(2,1)S(1)} async-done(((bf16[4,2,128,256]{3,2,1,0:T(8,128)(2,1)}), bf16[4,2,128,256]{3,2,1,0:T(8,128)(2,1)S(1)}, u32[]{:S(2)}, u32[]{:S(2)}) %all-to-all-start.2) | async-done | bytes 524320 | tf_op jit(solution)/shard_map/all_to_all | solution.py:248
  134.0 1.0 add_convert_fusion.2
  135.0 10.6 %all_gather.10.mid_ref = bf16[8,128,256]{2,1,0:T(8,128)(2,1)} all-gather(bf16[2,128,256]{2,1,0:T(8,128)(2,1)S(1)} %add_convert_fusion.2), channel_id=1, replica_groups=mesh['z'=8,'y'=8,'x'=4,'c'=2] {'x'}, dimensions={0}, use_global_device_ids=true | all-gather | bytes 655360 | tf_op jit(solution)/shard_map/all_gather | solution.py:251
  145.6 10.5 %ffn.1 = bf16[8,128,256]{2,1,0:T(8,128)(2,1)} custom-call(bf16[8,128,256]{2,1,0:T(8,128)(2,1)} %all_gather.10.mid_ref, f32[8,1,256]{2,1,0:T(1,128)} %bitcast.38, bf16[8,8,2,32,2112]{4,3,2,1,0:T(8,128)(2,1)} %bitcast.25), custom_call_target="tpu_custom_call" | custom-call | tf_op jit(solution)/shard_map/ffn/pallas_call | solution.py:252
  156.1 8.0 %all-to-all-start.3 = ((bf16[8,128,256]{2,1,0:T(8,128)(2,1)}), bf16[8,128,256]{2,1,0:T(8,128)(2,1)S(1)}, u32[]{:S(2)}, u32[]{:S(2)}) async-start(bf16[8,128,256]{2,1,0:T(8,128)(2,1)} %ffn.1), calls=%async_computation.3 | async-start | bytes 1048576 | tf_op jit(solution)/shard_map/all_to_all | solution.py:265
  164.1 2.0 %collective-permute-start.9 = (bf16[128,256]{1,0:T(8,128)(2,1)S(1)}, bf16[128,256]{1,0:T(8,128)(2,1)S(1)}, u32[]{:S(2)}, u32[]{:S(2)}) collective-permute-start(bf16[128,256]{1,0:T(8,128)(2,1)S(1)} %dynamic-slice_bitcast_fusion), channel_id=1, source_target_pairs={{0,1},{1,0},{2,3},{3,2},{4,5},{5,4},{6,7},{7,6},{8,9},{9,8},{10,11... | collective-permute-start | bytes 196616 | tf_op jit(solution)/shard_map/ppermute | solution.py:268
  166.1 1.1 collective-permute-done.9
  167.3 6.2 %all-to-all-done.3 = bf16[8,128,256]{2,1,0:T(8,128)(2,1)S(1)} async-done(((bf16[8,128,256]{2,1,0:T(8,128)(2,1)}), bf16[8,128,256]{2,1,0:T(8,128)(2,1)S(1)}, u32[]{:S(2)}, u32[]{:S(2)}) %all-to-all-start.3) | async-done | bytes 524320 | tf_op jit(solution)/shard_map/all_to_all | solution.py:265
  173.6 0.7 add_convert_fusion.1
  (37 shorter events, 0.4 us)
Async XLA Ops:
  6.5 139.1 %all-gather.2.cloned.1.call-start = ((), (), s32[]{:S(2)}) async-start(), calls=%async_computation.4 | async-start | bytes 17965056 | tf_op jit(solution)/shard_map/all_gather | solution.py:205
  26.2 66.2 %copy-start.1 = (bf16[4,32,640]{2,1,0:T(8,128)(2,1)}, bf16[4,32,640]{2,1,0:T(8,128)(2,1)S(1)}, u32[]{:S(2)}) copy-start(bf16[4,32,640]{2,1,0:T(8,128)(2,1)S(1)} %get-tuple-element.17) | copy-start | bytes 491524
  26.2 66.2 %copy-start.2 = (bf16[4,32,640]{2,1,0:T(8,128)(2,1)}, bf16[4,32,640]{2,1,0:T(8,128)(2,1)S(1)}, u32[]{:S(2)}) copy-start(bf16[4,32,640]{2,1,0:T(8,128)(2,1)S(1)} %get-tuple-element.18) | copy-start | bytes 491524
  26.3 14.6 %collective-permute-start = (bf16[1,128,640]{2,1,0:T(8,128)(2,1)S(1)}, bf16[1,128,640]{2,1,0:T(8,128)(2,1)S(1)}, u32[]{:S(2)}, u32[]{:S(2)}) collective-permute-start(bf16[1,128,640]{2,1,0:T(8,128)(2,1)S(1)} %bitcast.30), channel_id=1, source_target_pairs={{0,64},{64,0},{128,192},{192,128},{256,320},{320,256},{384,448},{4... | collective-permute-start | bytes 491528 | tf_op jit(solution)/shard_map/ppermute | solution.py:114
  32.0 13.7 %collective-permute-start.4 = (bf16[1,128,640]{2,1,0:T(8,128)(2,1)S(1)}, bf16[1,128,640]{2,1,0:T(8,128)(2,1)S(1)}, u32[]{:S(2)}, u32[]{:S(2)}) collective-permute-start(bf16[1,128,640]{2,1,0:T(8,128)(2,1)S(1)} %bitcast.26), channel_id=1, source_target_pairs={{0,448},{64,128},{128,64},{192,256},{256,192},{320,384},{384,320},... | collective-permute-start | bytes 491528 | tf_op jit(solution)/shard_map/ppermute | solution.py:114
  40.9 51.5 %copy-start.3 = (bf16[1,128,640]{2,1,0:T(8,128)(2,1)}, bf16[1,128,640]{2,1,0:T(8,128)(2,1)S(1)}, u32[]{:S(2)}) copy-start(bf16[1,128,640]{2,1,0:T(8,128)(2,1)S(1)} %collective-permute-done.refs_1_) | copy-start | bytes 491524
  40.9 16.5 %collective-permute-start.1 = (bf16[2,128,640]{2,1,0:T(8,128)(2,1)S(1)}, bf16[2,128,640]{2,1,0:T(8,128)(2,1)S(1)}, u32[]{:S(2)}, u32[]{:S(2)}) collective-permute-start(bf16[2,128,640]{2,1,0:T(8,128)(2,1)S(1)} %pad_maximum_fusion), channel_id=1, source_target_pairs={{0,448},{64,128},{128,64},{192,256},{256,192},{320,384},{384,320},... | collective-permute-start | bytes 983048 | tf_op jit(solution)/shard_map/ppermute | solution.py:118
  45.7 46.7 %copy-start.4 = (bf16[1,128,640]{2,1,0:T(8,128)(2,1)}, bf16[1,128,640]{2,1,0:T(8,128)(2,1)S(1)}, u32[]{:S(2)}) copy-start(bf16[1,128,640]{2,1,0:T(8,128)(2,1)S(1)} %collective-permute-done.4.refs_6_) | copy-start | bytes 491524
  45.8 15.4 %collective-permute-start.5 = (bf16[2,128,640]{2,1,0:T(8,128)(2,1)S(1)}, bf16[2,128,640]{2,1,0:T(8,128)(2,1)S(1)}, u32[]{:S(2)}, u32[]{:S(2)}) collective-permute-start(bf16[2,128,640]{2,1,0:T(8,128)(2,1)S(1)} %pad_maximum_fusion.1), channel_id=1, source_target_pairs={{0,64},{64,0},{128,192},{192,128},{256,320},{320,256},{384,448},{4... | collective-permute-start | bytes 983048 | tf_op jit(solution)/shard_map/ppermute | solution.py:118
  49.6 27.6 %all-to-all-start = ((bf16[8,256,256]{2,1,0:T(8,128)(2,1)}), bf16[8,256,256]{2,1,0:T(8,128)(2,1)S(1)}, u32[]{:S(2)}, u32[]{:S(2)}) async-start(bf16[8,256,256]{2,1,0:T(8,128)(2,1)} %broadcast_in_dim.2), calls=%async_computation | async-start | bytes 2097152 | tf_op jit(solution)/shard_map/all_to_all | solution.py:22
  57.5 34.9 %copy-start.5 = (bf16[2,128,640]{2,1,0:T(8,128)(2,1)}, bf16[2,128,640]{2,1,0:T(8,128)(2,1)S(1)}, u32[]{:S(2)}) copy-start(bf16[2,128,640]{2,1,0:T(8,128)(2,1)S(1)} %collective-permute-done.1.refs_2_) | copy-start | bytes 983044
  57.5 11.7 %collective-permute-start.2 = (bf16[2,128,640]{2,1,0:T(8,128)(2,1)S(1)}, bf16[2,128,640]{2,1,0:T(8,128)(2,1)S(1)}, u32[]{:S(2)}, u32[]{:S(2)}) collective-permute-start(bf16[2,128,640]{2,1,0:T(8,128)(2,1)S(1)} %collective-permute-done.1.refs_2_), channel_id=1, source_target_pairs={{0,64},{64,0},{128,192},{192,128},{256,320},{320,256},{384,448},{4... | collective-permute-start | bytes 983048 | tf_op jit(solution)/shard_map/ppermute | solution.py:118
  61.1 31.3 %copy-start.6 = (bf16[2,128,640]{2,1,0:T(8,128)(2,1)}, bf16[2,128,640]{2,1,0:T(8,128)(2,1)S(1)}, u32[]{:S(2)}) copy-start(bf16[2,128,640]{2,1,0:T(8,128)(2,1)S(1)} %collective-permute-done.5.refs_7_) | copy-start | bytes 983044
  61.2 12.8 %collective-permute-start.6 = (bf16[2,128,640]{2,1,0:T(8,128)(2,1)S(1)}, bf16[2,128,640]{2,1,0:T(8,128)(2,1)S(1)}, u32[]{:S(2)}, u32[]{:S(2)}) collective-permute-start(bf16[2,128,640]{2,1,0:T(8,128)(2,1)S(1)} %collective-permute-done.5.refs_7_), channel_id=1, source_target_pairs={{0,448},{64,128},{128,64},{192,256},{256,192},{320,384},{384,320},... | collective-permute-start | bytes 983048 | tf_op jit(solution)/shard_map/ppermute | solution.py:118
  69.2 23.2 %copy-start.7 = (bf16[2,128,640]{2,1,0:T(8,128)(2,1)}, bf16[2,128,640]{2,1,0:T(8,128)(2,1)S(1)}, u32[]{:S(2)}) copy-start(bf16[2,128,640]{2,1,0:T(8,128)(2,1)S(1)} %collective-permute-done.2.refs_3_) | copy-start | bytes 983044
  69.2 19.1 %collective-permute-start.3 = (bf16[2,128,640]{2,1,0:T(8,128)(2,1)S(1)}, bf16[2,128,640]{2,1,0:T(8,128)(2,1)S(1)}, u32[]{:S(2)}, u32[]{:S(2)}) collective-permute-start(bf16[2,128,640]{2,1,0:T(8,128)(2,1)S(1)} %collective-permute-done.2.refs_3_), channel_id=1, source_target_pairs={{0,448},{64,128},{128,64},{192,256},{256,192},{320,384},{384,320},... | collective-permute-start | bytes 983048 | tf_op jit(solution)/shard_map/ppermute | solution.py:118
  74.0 18.4 %copy-start.8 = (bf16[2,128,640]{2,1,0:T(8,128)(2,1)}, bf16[2,128,640]{2,1,0:T(8,128)(2,1)S(1)}, u32[]{:S(2)}) copy-start(bf16[2,128,640]{2,1,0:T(8,128)(2,1)S(1)} %collective-permute-done.6.refs_8_) | copy-start | bytes 983044
  74.0 18.4 %collective-permute-start.7 = (bf16[2,128,640]{2,1,0:T(8,128)(2,1)S(1)}, bf16[2,128,640]{2,1,0:T(8,128)(2,1)}, u32[]{:S(2)}, u32[]{:S(2)}) collective-permute-start(bf16[2,128,640]{2,1,0:T(8,128)(2,1)S(1)} %collective-permute-done.6.refs_8_), channel_id=1, source_target_pairs={{0,64},{64,0},{128,192},{192,128},{256,320},{320,256},{384,448},{4... | collective-permute-start | bytes 983048 | tf_op jit(solution)/shard_map/ppermute | solution.py:118
  77.2 15.2 %copy-start = (bf16[8,256,256]{2,1,0:T(8,128)(2,1)}, bf16[8,256,256]{2,1,0:T(8,128)(2,1)S(1)}, u32[]{:S(2)}) copy-start(bf16[8,256,256]{2,1,0:T(8,128)(2,1)S(1)} %all-to-all-done.x_ref) | copy-start | bytes 3145732
  88.2 4.2 %copy-start.9 = (bf16[2,128,640]{2,1,0:T(8,128)(2,1)}, bf16[2,128,640]{2,1,0:T(8,128)(2,1)S(1)}, u32[]{:S(2)}) copy-start(bf16[2,128,640]{2,1,0:T(8,128)(2,1)S(1)} %collective-permute-done.3.refs_4_) | copy-start | bytes 983044
  114.7 4.4 %collective-permute-start.8 = (bf16[8,128,256]{2,1,0:T(8,128)(2,1)}, bf16[8,128,256]{2,1,0:T(8,128)(2,1)S(1)}, u32[]{:S(2)}, u32[]{:S(2)}) collective-permute-start(bf16[8,128,256]{2,1,0:T(8,128)(2,1)} %get-tuple-element.15), channel_id=1, source_target_pairs={{0,1},{1,0},{2,3},{3,2},{4,5},{5,4},{6,7},{7,6},{8,9},{9,8},{10,11... | collective-permute-start | bytes 1572872 | tf_op jit(solution)/shard_map/ppermute | solution.py:246
  121.1 12.9 %all-to-all-start.2 = ((bf16[4,2,128,256]{3,2,1,0:T(8,128)(2,1)}), bf16[4,2,128,256]{3,2,1,0:T(8,128)(2,1)S(1)}, u32[]{:S(2)}, u32[]{:S(2)}) async-start(bf16[4,2,128,256]{3,2,1,0:T(8,128)(2,1)} %bitcast.6), calls=%async_computation.2 | async-start | bytes 1048576 | tf_op jit(solution)/shard_map/all_to_all | solution.py:248
  156.1 17.4 %all-to-all-start.3 = ((bf16[8,128,256]{2,1,0:T(8,128)(2,1)}), bf16[8,128,256]{2,1,0:T(8,128)(2,1)S(1)}, u32[]{:S(2)}, u32[]{:S(2)}) async-start(bf16[8,128,256]{2,1,0:T(8,128)(2,1)} %ffn.1), calls=%async_computation.3 | async-start | bytes 1048576 | tf_op jit(solution)/shard_map/all_to_all | solution.py:265
  164.1 3.1 %collective-permute-start.9 = (bf16[128,256]{1,0:T(8,128)(2,1)S(1)}, bf16[128,256]{1,0:T(8,128)(2,1)S(1)}, u32[]{:S(2)}, u32[]{:S(2)}) collective-permute-start(bf16[128,256]{1,0:T(8,128)(2,1)S(1)} %dynamic-slice_bitcast_fusion), channel_id=1, source_target_pairs={{0,1},{1,0},{2,3},{3,2},{4,5},{5,4},{6,7},{7,6},{8,9},{9,8},{10,11... | collective-permute-start | bytes 196616 | tf_op jit(solution)/shard_map/ppermute | solution.py:268
Sparse Core Ops, SparseCore 0:
  10.5 115.5 all-gather.1

commit v3 on v2

--- a/solution.py
+++ b/solution.py
@@ -31,12 +31,13 @@
     return jnp.sum(jnp.where(same, row.reshape(1, n), 0.0), axis=1, keepdims=True)
 
 
-def pack_kernel(conv, blend, emis, emis_s, valve, valve_s, raising, raising_s, low, low_s, own, ffn):
+def pack_kernel(conv, blend, emis, emis_s, valve, valve_s, raising, raising_s, low, low_s, seq, own, ffn, seqs):
     emission = emis[...] * upright(emis_s[...], 32)
     packed = jnp.concatenate([conv[...], blend[...], emission, jnp.zeros((32, 64), F32)], axis=1)
     packed = packed.astype(BF)
     for k in range(8):
         own[k] = packed
+        seqs[k] = seq[...]
     gate = valve[...] * valve_s[...].reshape(1, 704)
     up = raising[...] * raising_s[...].reshape(1, 704)
     ffn[:, 0:640] = gate[:, 0:640].astype(BF)
@@ -45,29 +46,40 @@
     ffn[:, 1408:2112] = (low[...] * upright(low_s[...], 32)).astype(BF)
 
 
-def spread(order, left, right):
+def spread(order, left, right, place=0):
     found = []
     for half, refs in enumerate((left, right)):
-        place = 0
+        at = place
         for ref in refs:
             for k in range(ref.shape[0]):
-                found.append((order[half, place], half, ref, k))
-                place += 1
+                found.append((order[half, at], half, ref, k))
+                at += 1
     return found
 
 
-def project_kernel(order, x_ref, gain, conv_s, blend_s, *refs):
-    pieces, act_ref, sq_ref = refs[:10], refs[10], refs[11]
+def multiply(found, x_ref, gain, factor, prior):
+    for block, half, ref, k in found:
+        cols = pl.ds(128 * half, 128)
+        rows = (x_ref[block, :, cols].astype(F32) * factor * gain[block, :, cols]).astype(BF)
+        prior = prior + jnp.dot(rows, ref[k, :, 0:384], preferred_element_type=F32)
+    return prior
+
+
+def early_kernel(order, x_ref, gain, *refs):
+    pieces, prior_ref, factor_ref = refs[:8], refs[8], refs[9]
     total = jnp.zeros((256, 1), F32)
     for k in range(8):
         v = x_ref[k].astype(F32)
         total = total + jnp.sum(v * v, axis=1, keepdims=True)
     factor = lax.rsqrt(total / 2048.0 + EPS)
-    prior = jnp.zeros((256, 384), F32)
-    for block, half, ref, k in spread(order, pieces[:5], pieces[5:]):
-        cols = pl.ds(128 * half, 128)
-        rows = (x_ref[block, :, cols].astype(F32) * factor * gain[block, :, cols]).astype(BF)
-        prior = prior + jnp.dot(rows, ref[k, :, 0:384], preferred_element_type=F32)
+    factor_ref[...] = jnp.broadcast_to(factor, (256, 128))
+    found = spread(order, pieces[:4], pieces[4:])
+    prior_ref[...] = multiply(found, x_ref, gain, factor, jnp.zeros((256, 384), F32))
+
+
+def project_kernel(order, x_ref, gain, conv_s, blend_s, prior, factor, left, right, act_ref, sq_ref):
+    found = spread(order, [left], [right], 6)
+    prior = multiply(found, x_ref, gain, factor[:, 0:1], prior[...])
     scales = jnp.concatenate([conv_s[...].reshape(1, 192), blend_s[...].reshape(1, 192)], axis=1)
     act = gelu(prior * scales)
     act_ref[...] = act
@@ -127,11 +139,14 @@
 
 
 def ffn_kernel(mid_ref, gain, w_ref, out_ref, w, acc, hid, sems):
-    def fetch(k):
-        return pltpu.make_async_copy(w_ref.at[k], w.at[k], sems.at[k])
-
-    for k in range(8):
-        fetch(k).start()
+    def fetch(k, part):
+        cols = pl.ds(1408 * part, 1408 - 704 * part)
+        at = (k, slice(None), slice(None), slice(None), cols)
+        return pltpu.make_async_copy(w_ref.at[at], w.at[at], sems.at[part, k])
+
+    for part in range(2):
+        for k in range(8):
+            fetch(k, part).start()
     total = jnp.zeros((128, 1), F32)
     for k in range(8):
         v = mid_ref[k].astype(F32)
@@ -139,7 +154,7 @@
     factor = lax.rsqrt(total / 2048.0 + EPS)
     for k in range(8):
         rows = (mid_ref[k].astype(F32) * factor * gain[k]).astype(BF)
-        fetch(k).wait()
+        fetch(k, 0).wait()
         for c in range(2):
             piece = w[k, :, c, :, 0:1408].reshape(256, 1408)
             part = jnp.dot(rows, piece, preferred_element_type=F32)
@@ -155,6 +170,7 @@
         u = acc[c, :, 1344:1408]
         hid[c, :, 640:704] = (g * jax.nn.sigmoid(g) * u).astype(BF)
     for k in range(8):
+        fetch(k, 1).wait()
         part = jnp.zeros((128, 256), F32)
         for c in range(2):
             piece = w[k, :, c, :, 1408:2112].reshape(256, 704)
@@ -184,11 +200,15 @@
 ):
     z, x, c = lax.axis_index("z"), lax.axis_index("x"), lax.axis_index("c")
     swap = [(0, 1), (1, 0)]
-    own, ffn_own = pl.pallas_call(
+    own, ffn_own, seqs = pl.pallas_call(
         pack_kernel,
-        in_specs=[VM] * 10,
-        out_specs=[VM, VM],
-        out_shape=[jax.ShapeDtypeStruct((8, 32, 640), BF), jax.ShapeDtypeStruct((32, 2112), BF)],
+        in_specs=[VM] * 11,
+        out_specs=[VM] * 3,
+        out_shape=[
+            jax.ShapeDtypeStruct((8, 32, 640), BF),
+            jax.ShapeDtypeStruct((32, 2112), BF),
+            jax.ShapeDtypeStruct((8, 256, 256), BF),
+        ],
         name="pack",
     )(
         conveyor_matrix,
@@ -201,30 +221,32 @@
         raising_rescalers,
         lowering_matrix.T,
         lowering_rescalers,
+        sequence_entries,
     )
     ffn_all = lax.all_gather(ffn_own, ("z", "y", "c"), axis=0, tiled=True)
 
     first = lax.all_to_all(own, "y", 0, 0, tiled=True)
-    rows = from_everyone(sequence_entries, TP)
+    rows = lax.all_to_all(seqs, TP, 0, 0, tiled=True)
     left = exchange(first[:4].reshape(1, 128, 640), 0)
     right = exchange(first[4:].reshape(1, 128, 640), 1)
     pieces = left + right
     order = blocks(z)
 
+    gain = former_norm_factor.reshape(8, 1, 256)
+    prior, factor = pl.pallas_call(
+        early_kernel,
+        in_specs=[SM] + [VM] * 10,
+        out_specs=[VM, VM],
+        out_shape=[jax.ShapeDtypeStruct((256, 384), F32), jax.ShapeDtypeStruct((256, 128), F32)],
+        name="early",
+    )(order, rows, gain, *left[:4], *right[:4])
     act, own_sq = pl.pallas_call(
         project_kernel,
-        in_specs=[SM] + [VM] * 14,
+        in_specs=[SM] + [VM] * 8,
         out_specs=[VM, VM],
         out_shape=[jax.ShapeDtypeStruct((256, 384), F32), jax.ShapeDtypeStruct((1, 1, 256), F32)],
         name="project",
-    )(
-        order,
-        rows,
-        former_norm_factor.reshape(8, 1, 256),
-        conveyor_rescalers,
-        blend_rescalers,
-        *pieces,
-    )
+    )(order, rows, gain, conveyor_rescalers, blend_rescalers, prior, factor, left[4], right[4])
     all_sq = lax.all_gather(own_sq, TP, axis=0, tiled=True)
     kept, sent = pl.pallas_call(
         gate_kernel,
@@ -248,7 +270,7 @@
     shares = lax.all_to_all(both, "x", 0, 0, tiled=True)
     base = lax.dynamic_slice(rows, (2 * x, 128 * c, 0), (2, 128, 256))
     mid_own = (base.astype(F32) + jnp.sum(shares.astype(F32), axis=0)).astype(BF)
-    mid = lax.all_gather(mid_own, "x", axis=0, tiled=True)
+    mid = from_everyone(mid_own, "x").reshape(8, 128, 256)
     outs = pl.pallas_call(
         ffn_kernel,
         in_specs=[VM, VM, ANY],
@@ -258,7 +280,7 @@
             pltpu.VMEM((8, 8, 2, 32, 2112), BF),
             pltpu.VMEM((2, 128, 1408), F32),
             pltpu.VMEM((2, 128, 704), BF),
-            pltpu.SemaphoreType.DMA((8,)),
+            pltpu.SemaphoreType.DMA((2, 8)),
         ],
         name="ffn",
     )(mid, latter_norm_factor.reshape(8, 1, 256), ffn_all.reshape(8, 8, 2, 32, 2112))

time: 182 us -> 181 us (level)
  starting transfers between devices: 58.6 us -> 52.5 us
  Pallas kernels: 21.5 us -> 24.7 us
    all_to_all x0 -> x1, blocking collectives: none -> 11.5 us  [from_everyone(): return lax.all_to_all(copies, axis, split_axis=0, concat_axis=0, tiled=True)]
    all_gather x1 -> x0, blocking collectives: 10.6 us -> none  [on_device(): mid = lax.all_gather(mid_own, 'x', axis=0, tiled=True)]
    ppermute x6, starting transfers between devices: 20.7 us -> 16.4 us  [exchange(): batch = lax.ppermute(batch, 'z', turn)]
    ppermute x2, waiting for transfers between devices: 0.01 us -> 2.92 us  [exchange(): got = lax.ppermute(own, 'z', to_pair)]
    all_to_all x1, starting transfers between devices: 7.99 us -> 5.38 us  [on_device(): lax.all_to_all(outs, TP, 0, 0, tiled=True).reshape(4, 2, 128, 256)]
    pallas_call x2 -> x3, Pallas kernels: 6.86 us -> 9.36 us  [the longest x1 3.86 us: on_device(): pl.pallas_call(early_kernel, in_specs=[SM] + [VM] * 10, out_specs=[VM, VM...]
    ppermute x6, waiting for transfers between devices: 19.5 us -> 17.4 us  [exchange(): batch = lax.ppermute(batch, 'z', turn)]
    broadcast_in_dim x1, local copies, waits for them, and re-layouts: 1.94 us -> 0.04 us  [from_everyone(): copies = jnp.broadcast_to(x, (lax.axis_size(axis), *x.shape))]
  transfers between devices with their start and end apart: 14 -> 14, of which waited for: 7 -> 10; matrix products, arithmetic and copies ran while one was open for 4% -> 3% of each run, Pallas kernels for 5% -> 6%
where the time goes in v3:
time: 181 us; the launch traced here: 180 us
  starting transfers between devices  52.5 us (29%)
  blocking collectives  42.9 us (24%)
  waiting for transfers between devices  39 us (22%)
  Pallas kernels  24.7 us (14%)
  between operations  13.6 us (8%)
  other arithmetic  5.27 us (3%)
    all_to_all x1, blocking collectives, on_device(): first = lax.all_to_all(own, 'y', 0, 0, tiled=True)  17.6 us
    ppermute x6, waiting for transfers between devices, exchange(): batch = lax.ppermute(batch, 'z', turn)  17.4 us
    ppermute x6, starting transfers between devices, exchange(): batch = lax.ppermute(batch, 'z', turn)  16.4 us
    ppermute x2, starting transfers between devices, exchange(): got = lax.ppermute(own, 'z', to_pair)  14.3 us
    all_gather x1, blocking collectives, on_device(): all_sq = lax.all_gather(own_sq, TP, axis=0, tiled=True)  13.7 us
    all_to_all x1, blocking collectives, from_everyone(): return lax.all_to_all(copies, axis, split_axis=0, concat_axis=0, tiled=True)  11.5 us
    pallas_call x1, Pallas kernels, on_device(): pl.pallas_call(ffn_kernel, in_specs=[VM, VM, ANY], out_specs=VM, out_shap...  11.3 us
    all_to_all x1, waiting for transfers between devices, on_device(): shares = lax.all_to_all(both, 'x', 0, 0, tiled=True)  9.27 us
  transfers between devices with their start and end apart: 14, of which 10 were waited for; matrix products, arithmetic and copies ran while one was open for 3% of the time, Pallas kernels for 6%

profile of v3, /device:TPU:1, one launch (start us, length us, event | category | flops | bytes accessed | tf_op | source)
XLA Modules:
  0.0 179.9 jit_solution(15036396953603206920)
XLA Ops:
  6.5 2.4 %pack.1 = (bf16[8,32,640]{2,1,0:T(8,128)(2,1)}, bf16[32,2112]{1,0:T(8,128)(2,1)}, bf16[8,256,256]{2,1,0:T(8,128)(2,1)}) custom-call(f32[32,192]{1,0:T(8,128)} %conv.1, f32[32,192]{1,0:T(8,128)} %blend.1, f32[32,192]{1,0:T(8,128)} %bitcast.40, f32[32]{0:T(128)} %emis_s.1, f32[32,704]{1,0:T(8,128)} %valve.1, f32[704]{0:T(1024)} %valve_s.1, f32[32,704]{1,0:T(8,128)} %raising.1, ...), custom_call_target="tpu_custom_call" | custom-call | tf_op jit(solution)/shard_map/pack/pallas_call | solution.py:203
  9.0 17.6 %all_to_all.25 = bf16[8,32,640]{2,1,0:T(8,128)(2,1)S(1)} all-to-all(bf16[8,32,640]{2,1,0:T(8,128)(2,1)} %get-tuple-element.15), channel_id=1, replica_groups=mesh['z'=8,'y'=8,'x'=4,'c'=2] {'y'}, dimensions={0} | all-to-all | bytes 655360 | tf_op jit(solution)/shard_map/all_to_all | solution.py:228
  26.7 12.4 %collective-permute-start.3 = (bf16[1,128,640]{2,1,0:T(8,128)(2,1)S(1)}, bf16[1,128,640]{2,1,0:T(8,128)(2,1)S(1)}, u32[]{:S(2)}, u32[]{:S(2)}) collective-permute-start(bf16[1,128,640]{2,1,0:T(8,128)(2,1)S(1)} %bitcast.27), channel_id=1, source_target_pairs={{0,448},{64,128},{128,64},{192,256},{256,192},{320,384},{384,320},... | collective-permute-start | bytes 491528 | tf_op jit(solution)/shard_map/ppermute | solution.py:126
  39.1 1.9 %collective-permute-start = (bf16[1,128,640]{2,1,0:T(8,128)(2,1)S(1)}, bf16[1,128,640]{2,1,0:T(8,128)(2,1)S(1)}, u32[]{:S(2)}, u32[]{:S(2)}) collective-permute-start(bf16[1,128,640]{2,1,0:T(8,128)(2,1)S(1)} %bitcast.31), channel_id=1, source_target_pairs={{0,64},{64,0},{128,192},{192,128},{256,320},{320,256},{384,448},{4... | collective-permute-start | bytes 491528 | tf_op jit(solution)/shard_map/ppermute | solution.py:126
  41.0 1.9 %collective-permute-done.3.refs_5_.refs_6_ = bf16[1,128,640]{2,1,0:T(8,128)(2,1)S(1)} collective-permute-done((bf16[1,128,640]{2,1,0:T(8,128)(2,1)S(1)}, bf16[1,128,640]{2,1,0:T(8,128)(2,1)S(1)}, u32[]{:S(2)}, u32[]{:S(2)}) %collective-permute-start.3) | collective-permute-done | bytes 163872 | tf_op jit(solution)/shard_map/ppermute | solution.py:126
  42.9 1.9 %collective-permute-start.4 = (bf16[2,128,640]{2,1,0:T(8,128)(2,1)S(1)}, bf16[2,128,640]{2,1,0:T(8,128)(2,1)S(1)}, u32[]{:S(2)}, u32[]{:S(2)}) collective-permute-start(bf16[2,128,640]{2,1,0:T(8,128)(2,1)S(1)} %pad_maximum_fusion.1), channel_id=1, source_target_pairs={{0,64},{64,0},{128,192},{192,128},{256,320},{320,256},{384,448},{4... | collective-permute-start | bytes 983048 | tf_op jit(solution)/shard_map/ppermute | solution.py:130
  46.0 2.6 %collective-permute-start.1 = (bf16[2,128,640]{2,1,0:T(8,128)(2,1)S(1)}, bf16[2,128,640]{2,1,0:T(8,128)(2,1)S(1)}, u32[]{:S(2)}, u32[]{:S(2)}) collective-permute-start(bf16[2,128,640]{2,1,0:T(8,128)(2,1)S(1)} %pad_maximum_fusion), channel_id=1, source_target_pairs={{0,448},{64,128},{128,64},{192,256},{256,192},{320,384},{384,320},... | collective-permute-start | bytes 983048 | tf_op jit(solution)/shard_map/ppermute | solution.py:130
  48.6 8.8 %all-to-all-start = ((bf16[8,256,256]{2,1,0:T(8,128)(2,1)}), bf16[8,256,256]{2,1,0:T(8,128)(2,1)S(1)}, u32[]{:S(2)}, u32[]{:S(2)}) async-start(bf16[8,256,256]{2,1,0:T(8,128)(2,1)} %get-tuple-element.14), calls=%async_computation | async-start | bytes 2097152 | tf_op jit(solution)/shard_map/all_to_all | solution.py:229
  57.4 4.8 %collective-permute-start.5 = (bf16[2,128,640]{2,1,0:T(8,128)(2,1)S(1)}, bf16[2,128,640]{2,1,0:T(8,128)(2,1)S(1)}, u32[]{:S(2)}, u32[]{:S(2)}) collective-permute-start(bf16[2,128,640]{2,1,0:T(8,128)(2,1)S(1)} %collective-permute-done.4.refs_6_.refs_7_), channel_id=1, source_target_pairs={{0,448},{64,128},{128,64},{192,256},{256,192},{320,384},{384,320},... | collective-permute-start | bytes 983048 | tf_op jit(solution)/shard_map/ppermute | solution.py:130
  62.2 1.9 %collective-permute-start.2 = (bf16[2,128,640]{2,1,0:T(8,128)(2,1)S(1)}, bf16[2,128,640]{2,1,0:T(8,128)(2,1)}, u32[]{:S(2)}, u32[]{:S(2)}) collective-permute-start(bf16[2,128,640]{2,1,0:T(8,128)(2,1)S(1)} %collective-permute-done.1.refs_2_), channel_id=1, source_target_pairs={{0,64},{64,0},{128,192},{192,128},{256,320},{320,256},{384,448},{4... | collective-permute-start | bytes 983048 | tf_op jit(solution)/shard_map/ppermute | solution.py:130
  64.1 5.1 %collective-permute-done.5.refs_7_.refs_8_ = bf16[2,128,640]{2,1,0:T(8,128)(2,1)S(1)} collective-permute-done((bf16[2,128,640]{2,1,0:T(8,128)(2,1)S(1)}, bf16[2,128,640]{2,1,0:T(8,128)(2,1)S(1)}, u32[]{:S(2)}, u32[]{:S(2)}) %collective-permute-start.5) | collective-permute-done | bytes 327712 | tf_op jit(solution)/shard_map/ppermute | solution.py:130
  69.2 1.9 %collective-permute-start.7 = (bf16[2,128,640]{2,1,0:T(8,128)(2,1)S(1)}, bf16[2,128,640]{2,1,0:T(8,128)(2,1)S(1)}, u32[]{:S(2)}, u32[]{:S(2)}) collective-permute-start(bf16[2,128,640]{2,1,0:T(8,128)(2,1)S(1)} %collective-permute-done.5.refs_7_.refs_8_), channel_id=1, source_target_pairs={{0,64},{64,0},{128,192},{192,128},{256,320},{320,256},{384,448},{4... | collective-permute-start | bytes 983048 | tf_op jit(solution)/shard_map/ppermute | solution.py:130
  71.1 2.0 %collective-permute-done.2.refs_3_ = bf16[2,128,640]{2,1,0:T(8,128)(2,1)} collective-permute-done((bf16[2,128,640]{2,1,0:T(8,128)(2,1)S(1)}, bf16[2,128,640]{2,1,0:T(8,128)(2,1)}, u32[]{:S(2)}, u32[]{:S(2)}) %collective-permute-start.2) | collective-permute-done | bytes 327712 | tf_op jit(solution)/shard_map/ppermute | solution.py:130
  73.2 3.3 %collective-permute-start.6 = (bf16[2,128,640]{2,1,0:T(8,128)(2,1)}, bf16[2,128,640]{2,1,0:T(8,128)(2,1)S(1)}, u32[]{:S(2)}, u32[]{:S(2)}) collective-permute-start(bf16[2,128,640]{2,1,0:T(8,128)(2,1)} %collective-permute-done.2.refs_3_), channel_id=1, source_target_pairs={{0,448},{64,128},{128,64},{192,256},{256,192},{320,384},{384,320},... | collective-permute-start | bytes 983048 | tf_op jit(solution)/shard_map/ppermute | solution.py:130
  76.5 1.3 add_and_fusion.order
  78.7 3.9 %early.1 = (f32[256,384]{1,0:T(8,128)}, f32[256,128]{1,0:T(8,128)}) custom-call(s32[2,8]{1,0:T(2,128)} %add_and_fusion.order, bf16[8,256,256]{2,1,0:T(8,128)(2,1)} %copy-done, f32[8,1,256]{2,1,0:T(1,128)} %bitcast.38, bf16[1,128,640]{2,1,0:T(8,128)(2,1)} %bitcast.33, bf16[1,128,640]{2,1,0:T(8,128)(2,1)} %copy-done.4, bf16[2,128,640]{2,1,0:T(8,128)(2,1)} %copy-done.8, ...), custom_call_target="tpu_custom_call" | custom-call | tf_op jit(solution)/shard_map/early/pallas_call | solution.py:236
  82.6 4.6 %collective-permute-done.7.right.refs_9_ = bf16[2,128,640]{2,1,0:T(8,128)(2,1)S(1)} collective-permute-done((bf16[2,128,640]{2,1,0:T(8,128)(2,1)S(1)}, bf16[2,128,640]{2,1,0:T(8,128)(2,1)S(1)}, u32[]{:S(2)}, u32[]{:S(2)}) %collective-permute-start.7) | collective-permute-done | bytes 327712 | tf_op jit(solution)/shard_map/ppermute | solution.py:130
  87.2 5.7 %collective-permute-done.6.left.refs_4_ = bf16[2,128,640]{2,1,0:T(8,128)(2,1)S(1)} collective-permute-done((bf16[2,128,640]{2,1,0:T(8,128)(2,1)}, bf16[2,128,640]{2,1,0:T(8,128)(2,1)S(1)}, u32[]{:S(2)}, u32[]{:S(2)}) %collective-permute-start.6) | collective-permute-done | bytes 327712 | tf_op jit(solution)/shard_map/ppermute | solution.py:130
  93.6 3.1 %project.1 = (f32[256,384]{1,0:T(8,128)}, f32[1,1,256]{2,1,0:T(1,128)}) custom-call(s32[2,8]{1,0:T(2,128)} %add_and_fusion.order, bf16[8,256,256]{2,1,0:T(8,128)(2,1)} %copy-done, f32[8,1,256]{2,1,0:T(1,128)} %bitcast.39, f32[192]{0:T(256)} %conv_s.1, f32[192]{0:T(256)} %blend_s.1, f32[256,384]{1,0:T(8,128)} %get-tuple-element.16.prior, ...), custom_call_target="tpu_custom_call" | custom-call | tf_op jit(solution)/shard_map/project/pallas_call | solution.py:243
  96.7 13.7 %all_gather.6.sq_ref = f32[8,1,256]{2,1,0:T(1,128)} all-gather(f32[1,1,256]{2,1,0:T(1,128)} %get-tuple-element.19), channel_id=1, replica_groups=mesh['z'=8,'y'=8,'x'=4,'c'=2] {'x','c'}, dimensions={0}, use_global_device_ids=true | all-gather | bytes 9216 | tf_op jit(solution)/shard_map/all_gather | solution.py:250
  110.5 4.1 %gating.1 = (bf16[8,128,256]{2,1,0:T(8,128)(2,1)}, bf16[8,128,256]{2,1,0:T(8,128)(2,1)}) custom-call(s32[2,8]{1,0:T(2,128)} %add_and_fusion.order, s32[1]{0:T(128)} %bitcast.2.core, f32[256,384]{1,0:T(8,128)} %get-tuple-element.18.act_ref, f32[8,1,256]{2,1,0:T(1,128)} %all_gather.6.sq_ref, bf16[3,128,128]{2,1,0:T(8,128)(2,1)} %mats.1, f32[3,128]{1,0:T(4,128)} %offs.1, ...), custom_call_target="tpu_custom_call" | custom-call | tf_op jit(solution)/shard_map/gating/pallas_call | solution.py:251
  114.6 2.1 %collective-permute-start.8 = (bf16[8,128,256]{2,1,0:T(8,128)(2,1)}, bf16[8,128,256]{2,1,0:T(8,128)(2,1)S(1)}, u32[]{:S(2)}, u32[]{:S(2)}) collective-permute-start(bf16[8,128,256]{2,1,0:T(8,128)(2,1)} %get-tuple-element.21), channel_id=1, source_target_pairs={{0,1},{1,0},{2,3},{3,2},{4,5},{5,4},{6,7},{7,6},{8,9},{9,8},{10,11... | collective-permute-start | bytes 1572872 | tf_op jit(solution)/shard_map/ppermute | solution.py:268
  116.7 2.1 %collective-permute-done.8 = bf16[8,128,256]{2,1,0:T(8,128)(2,1)S(1)} collective-permute-done((bf16[8,128,256]{2,1,0:T(8,128)(2,1)}, bf16[8,128,256]{2,1,0:T(8,128)(2,1)S(1)}, u32[]{:S(2)}, u32[]{:S(2)}) %collective-permute-start.8) | collective-permute-done | bytes 524320 | tf_op jit(solution)/shard_map/ppermute | solution.py:268
  118.8 2.1 %add_convert_fusion = bf16[8,128,256]{2,1,0:T(8,128)(2,1)} fusion(bf16[8,128,256]{2,1,0:T(8,128)(2,1)S(1)} %collective-permute-done.8, bf16[8,128,256]{2,1,0:T(8,128)(2,1)} %get-tuple-element.20), kind=kLoop, calls=%fused_computation.2 | loop fusion | flops 1048576 | bytes 1572864 | tf_op jit(solution)/shard_map/convert_element_type | solution.py:269
  120.9 3.5 %all-to-all-start.2 = ((bf16[4,2,128,256]{3,2,1,0:T(8,128)(2,1)}), bf16[4,2,128,256]{3,2,1,0:T(8,128)(2,1)S(1)}, u32[]{:S(2)}, u32[]{:S(2)}) async-start(bf16[4,2,128,256]{3,2,1,0:T(8,128)(2,1)} %bitcast.6), calls=%async_computation.2 | async-start | bytes 1048576 | tf_op jit(solution)/shard_map/all_to_all | solution.py:270
  124.4 9.3 %all-to-all-done.2 = bf16[4,2,128,256]{3,2,1,0:T(8,128)(2,1)S(1)} async-done(((bf16[4,2,128,256]{3,2,1,0:T(8,128)(2,1)}), bf16[4,2,128,256]{3,2,1,0:T(8,128)(2,1)S(1)}, u32[]{:S(2)}, u32[]{:S(2)}) %all-to-all-start.2) | async-done | bytes 524320 | tf_op jit(solution)/shard_map/all_to_all | solution.py:270
  134.7 11.5 %all_to_all.26 = bf16[4,2,128,256]{3,2,1,0:T(8,128)(2,1)} all-to-all(bf16[4,2,128,256]{3,2,1,0:T(8,128)(2,1)S(1)} %broadcast_in_dim.2), channel_id=1, replica_groups=mesh['z'=8,'y'=8,'x'=4,'c'=2] {'x'}, dimensions={0} | all-to-all | bytes 1048576 | tf_op jit(solution)/shard_map/all_to_all | solution.py:22
  146.2 11.3 %ffn.1 = bf16[8,128,256]{2,1,0:T(8,128)(2,1)} custom-call(bf16[8,128,256]{2,1,0:T(8,128)(2,1)} %bitcast.35, f32[8,1,256]{2,1,0:T(1,128)} %bitcast.41, bf16[8,8,2,32,2112]{4,3,2,1,0:T(8,128)(2,1)} %bitcast.26), custom_call_target="tpu_custom_call" | custom-call | tf_op jit(solution)/shard_map/ffn/pallas_call | solution.py:274
  157.5 5.4 %all-to-all-start.4 = ((bf16[8,128,256]{2,1,0:T(8,128)(2,1)}), bf16[8,128,256]{2,1,0:T(8,128)(2,1)S(1)}, u32[]{:S(2)}, u32[]{:S(2)}) async-start(bf16[8,128,256]{2,1,0:T(8,128)(2,1)} %ffn.1), calls=%async_computation.4 | async-start | bytes 1048576 | tf_op jit(solution)/shard_map/all_to_all | solution.py:287
  162.9 2.0 %collective-permute-start.9 = (bf16[128,256]{1,0:T(8,128)(2,1)S(1)}, bf16[128,256]{1,0:T(8,128)(2,1)S(1)}, u32[]{:S(2)}, u32[]{:S(2)}) collective-permute-start(bf16[128,256]{1,0:T(8,128)(2,1)S(1)} %dynamic-slice_bitcast_fusion), channel_id=1, source_target_pairs={{0,1},{1,0},{2,3},{3,2},{4,5},{5,4},{6,7},{7,6},{8,9},{9,8},{10,11... | collective-permute-start | bytes 196616 | tf_op jit(solution)/shard_map/ppermute | solution.py:290
  164.9 1.1 collective-permute-done.9
  166.1 6.2 %all-to-all-done.4 = bf16[8,128,256]{2,1,0:T(8,128)(2,1)S(1)} async-done(((bf16[8,128,256]{2,1,0:T(8,128)(2,1)}), bf16[8,128,256]{2,1,0:T(8,128)(2,1)S(1)}, u32[]{:S(2)}, u32[]{:S(2)}) %all-to-all-start.4) | async-done | bytes 524320 | tf_op jit(solution)/shard_map/all_to_all | solution.py:287
  (38 shorter events, 4.7 us)
Async XLA Ops:
  6.5 139.7 %all-gather.2.cloned.1.call-start = ((), (), s32[]{:S(2)}) async-start(), calls=%async_computation.5 | async-start | bytes 17965056 | tf_op jit(solution)/shard_map/all_gather | solution.py:226
  26.7 51.1 %copy-start.1 = (bf16[4,32,640]{2,1,0:T(8,128)(2,1)}, bf16[4,32,640]{2,1,0:T(8,128)(2,1)S(1)}, u32[]{:S(2)}) copy-start(bf16[4,32,640]{2,1,0:T(8,128)(2,1)S(1)} %get-tuple-element.23) | copy-start | bytes 491524
  26.7 51.1 %copy-start.2 = (bf16[4,32,640]{2,1,0:T(8,128)(2,1)}, bf16[4,32,640]{2,1,0:T(8,128)(2,1)S(1)}, u32[]{:S(2)}) copy-start(bf16[4,32,640]{2,1,0:T(8,128)(2,1)S(1)} %get-tuple-element.24) | copy-start | bytes 491524
  26.7 16.2 %collective-permute-start.3 = (bf16[1,128,640]{2,1,0:T(8,128)(2,1)S(1)}, bf16[1,128,640]{2,1,0:T(8,128)(2,1)S(1)}, u32[]{:S(2)}, u32[]{:S(2)}) collective-permute-start(bf16[1,128,640]{2,1,0:T(8,128)(2,1)S(1)} %bitcast.27), channel_id=1, source_target_pairs={{0,448},{64,128},{128,64},{192,256},{256,192},{320,384},{384,320},... | collective-permute-start | bytes 491528 | tf_op jit(solution)/shard_map/ppermute | solution.py:126
  39.1 6.8 %collective-permute-start = (bf16[1,128,640]{2,1,0:T(8,128)(2,1)S(1)}, bf16[1,128,640]{2,1,0:T(8,128)(2,1)S(1)}, u32[]{:S(2)}, u32[]{:S(2)}) collective-permute-start(bf16[1,128,640]{2,1,0:T(8,128)(2,1)S(1)} %bitcast.31), channel_id=1, source_target_pairs={{0,64},{64,0},{128,192},{192,128},{256,320},{320,256},{384,448},{4... | collective-permute-start | bytes 491528 | tf_op jit(solution)/shard_map/ppermute | solution.py:126
  42.9 34.9 %copy-start.3 = (bf16[1,128,640]{2,1,0:T(8,128)(2,1)}, bf16[1,128,640]{2,1,0:T(8,128)(2,1)S(1)}, u32[]{:S(2)}) copy-start(bf16[1,128,640]{2,1,0:T(8,128)(2,1)S(1)} %collective-permute-done.3.refs_5_.refs_6_) | copy-start | bytes 491524
  42.9 14.5 %collective-permute-start.4 = (bf16[2,128,640]{2,1,0:T(8,128)(2,1)S(1)}, bf16[2,128,640]{2,1,0:T(8,128)(2,1)S(1)}, u32[]{:S(2)}, u32[]{:S(2)}) collective-permute-start(bf16[2,128,640]{2,1,0:T(8,128)(2,1)S(1)} %pad_maximum_fusion.1), channel_id=1, source_target_pairs={{0,64},{64,0},{128,192},{192,128},{256,320},{320,256},{384,448},{4... | collective-permute-start | bytes 983048 | tf_op jit(solution)/shard_map/ppermute | solution.py:130
  45.9 31.9 %copy-start.4 = (bf16[1,128,640]{2,1,0:T(8,128)(2,1)}, bf16[1,128,640]{2,1,0:T(8,128)(2,1)S(1)}, u32[]{:S(2)}) copy-start(bf16[1,128,640]{2,1,0:T(8,128)(2,1)S(1)} %collective-permute-done.refs_1_) | copy-start | bytes 491524
  46.0 16.2 %collective-permute-start.1 = (bf16[2,128,640]{2,1,0:T(8,128)(2,1)S(1)}, bf16[2,128,640]{2,1,0:T(8,128)(2,1)S(1)}, u32[]{:S(2)}, u32[]{:S(2)}) collective-permute-start(bf16[2,128,640]{2,1,0:T(8,128)(2,1)S(1)} %pad_maximum_fusion), channel_id=1, source_target_pairs={{0,448},{64,128},{128,64},{192,256},{256,192},{320,384},{384,320},... | collective-permute-start | bytes 983048 | tf_op jit(solution)/shard_map/ppermute | solution.py:130
  48.6 29.2 %all-to-all-start = ((bf16[8,256,256]{2,1,0:T(8,128)(2,1)}), bf16[8,256,256]{2,1,0:T(8,128)(2,1)S(1)}, u32[]{:S(2)}, u32[]{:S(2)}) async-start(bf16[8,256,256]{2,1,0:T(8,128)(2,1)} %get-tuple-element.14), calls=%async_computation | async-start | bytes 2097152 | tf_op jit(solution)/shard_map/all_to_all | solution.py:229
  57.4 20.4 %copy-start.7 = (bf16[2,128,640]{2,1,0:T(8,128)(2,1)}, bf16[2,128,640]{2,1,0:T(8,128)(2,1)S(1)}, u32[]{:S(2)}) copy-start(bf16[2,128,640]{2,1,0:T(8,128)(2,1)S(1)} %collective-permute-done.4.refs_6_.refs_7_) | copy-start | bytes 983044
  57.4 11.8 %collective-permute-start.5 = (bf16[2,128,640]{2,1,0:T(8,128)(2,1)S(1)}, bf16[2,128,640]{2,1,0:T(8,128)(2,1)S(1)}, u32[]{:S(2)}, u32[]{:S(2)}) collective-permute-start(bf16[2,128,640]{2,1,0:T(8,128)(2,1)S(1)} %collective-permute-done.4.refs_6_.refs_7_), channel_id=1, source_target_pairs={{0,448},{64,128},{128,64},{192,256},{256,192},{320,384},{384,320},... | collective-permute-start | bytes 983048 | tf_op jit(solution)/shard_map/ppermute | solution.py:130
  62.2 15.6 %copy-start.8 = (bf16[2,128,640]{2,1,0:T(8,128)(2,1)}, bf16[2,128,640]{2,1,0:T(8,128)(2,1)S(1)}, u32[]{:S(2)}) copy-start(bf16[2,128,640]{2,1,0:T(8,128)(2,1)S(1)} %collective-permute-done.1.refs_2_) | copy-start | bytes 983044
  62.2 11.0 %collective-permute-start.2 = (bf16[2,128,640]{2,1,0:T(8,128)(2,1)S(1)}, bf16[2,128,640]{2,1,0:T(8,128)(2,1)}, u32[]{:S(2)}, u32[]{:S(2)}) collective-permute-start(bf16[2,128,640]{2,1,0:T(8,128)(2,1)S(1)} %collective-permute-done.1.refs_2_), channel_id=1, source_target_pairs={{0,64},{64,0},{128,192},{192,128},{256,320},{320,256},{384,448},{4... | collective-permute-start | bytes 983048 | tf_op jit(solution)/shard_map/ppermute | solution.py:130
  69.2 8.6 %copy-start.9 = (bf16[2,128,640]{2,1,0:T(8,128)(2,1)}, bf16[2,128,640]{2,1,0:T(8,128)(2,1)S(1)}, u32[]{:S(2)}) copy-start(bf16[2,128,640]{2,1,0:T(8,128)(2,1)S(1)} %collective-permute-done.5.refs_7_.refs_8_) | copy-start | bytes 983044
  69.2 18.0 %collective-permute-start.7 = (bf16[2,128,640]{2,1,0:T(8,128)(2,1)S(1)}, bf16[2,128,640]{2,1,0:T(8,128)(2,1)S(1)}, u32[]{:S(2)}, u32[]{:S(2)}) collective-permute-start(bf16[2,128,640]{2,1,0:T(8,128)(2,1)S(1)} %collective-permute-done.5.refs_7_.refs_8_), channel_id=1, source_target_pairs={{0,64},{64,0},{128,192},{192,128},{256,320},{320,256},{384,448},{4... | collective-permute-start | bytes 983048 | tf_op jit(solution)/shard_map/ppermute | solution.py:130
  73.2 19.7 %collective-permute-start.6 = (bf16[2,128,640]{2,1,0:T(8,128)(2,1)}, bf16[2,128,640]{2,1,0:T(8,128)(2,1)S(1)}, u32[]{:S(2)}, u32[]{:S(2)}) collective-permute-start(bf16[2,128,640]{2,1,0:T(8,128)(2,1)} %collective-permute-done.2.refs_3_), channel_id=1, source_target_pairs={{0,448},{64,128},{128,64},{192,256},{256,192},{320,384},{384,320},... | collective-permute-start | bytes 983048 | tf_op jit(solution)/shard_map/ppermute | solution.py:130
  77.8 1.0 copy-start
  87.2 5.7 %copy-start.5 = (bf16[2,128,640]{2,1,0:T(8,128)(2,1)}, bf16[2,128,640]{2,1,0:T(8,128)(2,1)S(1)}, u32[]{:S(2)}) copy-start(bf16[2,128,640]{2,1,0:T(8,128)(2,1)S(1)} %collective-permute-done.7.right.refs_9_) | copy-start | bytes 983044
  92.9 0.7 copy-start.6
  114.6 4.2 %collective-permute-start.8 = (bf16[8,128,256]{2,1,0:T(8,128)(2,1)}, bf16[8,128,256]{2,1,0:T(8,128)(2,1)S(1)}, u32[]{:S(2)}, u32[]{:S(2)}) collective-permute-start(bf16[8,128,256]{2,1,0:T(8,128)(2,1)} %get-tuple-element.21), channel_id=1, source_target_pairs={{0,1},{1,0},{2,3},{3,2},{4,5},{5,4},{6,7},{7,6},{8,9},{9,8},{10,11... | collective-permute-start | bytes 1572872 | tf_op jit(solution)/shard_map/ppermute | solution.py:268
  120.9 12.8 %all-to-all-start.2 = ((bf16[4,2,128,256]{3,2,1,0:T(8,128)(2,1)}), bf16[4,2,128,256]{3,2,1,0:T(8,128)(2,1)S(1)}, u32[]{:S(2)}, u32[]{:S(2)}) async-start(bf16[4,2,128,256]{3,2,1,0:T(8,128)(2,1)} %bitcast.6), calls=%async_computation.2 | async-start | bytes 1048576 | tf_op jit(solution)/shard_map/all_to_all | solution.py:270
  157.5 14.8 %all-to-all-start.4 = ((bf16[8,128,256]{2,1,0:T(8,128)(2,1)}), bf16[8,128,256]{2,1,0:T(8,128)(2,1)S(1)}, u32[]{:S(2)}, u32[]{:S(2)}) async-start(bf16[8,128,256]{2,1,0:T(8,128)(2,1)} %ffn.1), calls=%async_computation.4 | async-start | bytes 1048576 | tf_op jit(solution)/shard_map/all_to_all | solution.py:287
  162.9 3.1 %collective-permute-start.9 = (bf16[128,256]{1,0:T(8,128)(2,1)S(1)}, bf16[128,256]{1,0:T(8,128)(2,1)S(1)}, u32[]{:S(2)}, u32[]{:S(2)}) collective-permute-start(bf16[128,256]{1,0:T(8,128)(2,1)S(1)} %dynamic-slice_bitcast_fusion), channel_id=1, source_target_pairs={{0,1},{1,0},{2,3},{3,2},{4,5},{5,4},{6,7},{7,6},{8,9},{9,8},{10,11... | collective-permute-start | bytes 196616 | tf_op jit(solution)/shard_map/ppermute | solution.py:290
Sparse Core Ops, SparseCore 0:
  10.5 116.3 all-gather.1

commit v4 on v3

--- a/solution.py
+++ b/solution.py
@@ -31,7 +31,12 @@
     return jnp.sum(jnp.where(same, row.reshape(1, n), 0.0), axis=1, keepdims=True)
 
 
-def pack_kernel(conv, blend, emis, emis_s, valve, valve_s, raising, raising_s, low, low_s, seq, own, ffn, seqs):
+def pack_kernel(conv, blend, emis, emis_s, valve, valve_s, raising, raising_s, low, low_s, seq, *refs):
+    own, ffn, seqs, scales = refs[7:11]
+    scales[:, 0:192] = refs[0][...].reshape(1, 192)
+    scales[:, 192:384] = refs[1][...].reshape(1, 192)
+    for here, there in zip(refs[2:7], refs[11:]):
+        there[...] = here[...]
     emission = emis[...] * upright(emis_s[...], 32)
     packed = jnp.concatenate([conv[...], blend[...], emission, jnp.zeros((32, 64), F32)], axis=1)
     packed = packed.astype(BF)
@@ -77,11 +82,10 @@
     prior_ref[...] = multiply(found, x_ref, gain, factor, jnp.zeros((256, 384), F32))
 
 
-def project_kernel(order, x_ref, gain, conv_s, blend_s, prior, factor, left, right, act_ref, sq_ref):
+def project_kernel(order, x_ref, gain, scales, prior, factor, left, right, act_ref, sq_ref):
     found = spread(order, [left], [right], 6)
     prior = multiply(found, x_ref, gain, factor[:, 0:1], prior[...])
-    scales = jnp.concatenate([conv_s[...].reshape(1, 192), blend_s[...].reshape(1, 192)], axis=1)
-    act = gelu(prior * scales)
+    act = gelu(prior * scales[...])
     act_ref[...] = act
     signal = act[:, 192:384]
     ones = jnp.ones((8, 192), F32)
@@ -98,7 +102,7 @@
     rows = lax.broadcasted_iota(jnp.int32, (128, 128), 0)
     cols = lax.broadcasted_iota(jnp.int32, (128, 128), 1)
     lower = cols <= rows
-    gains = gain[...].reshape(1, 192)
+    gains = gain[...]
     for g in range(3):
         mat = jnp.where(lower, mats[g].astype(F32), 0.0)
         for b in range(2):
@@ -139,14 +143,20 @@
 
 
 def ffn_kernel(mid_ref, gain, w_ref, out_ref, w, acc, hid, sems):
-    def fetch(k, part):
+    def fetch(n):
+        part, k = divmod(n, 8)
         cols = pl.ds(1408 * part, 1408 - 704 * part)
         at = (k, slice(None), slice(None), slice(None), cols)
-        return pltpu.make_async_copy(w_ref.at[at], w.at[at], sems.at[part, k])
-
-    for part in range(2):
-        for k in range(8):
-            fetch(k, part).start()
+        return pltpu.make_async_copy(w_ref.at[at], w.at[at], sems.at[n])
+
+    for n in range(3):
+        fetch(n).start()
+
+    def arrive(n):
+        fetch(n).wait()
+        if n + 3 < 16:
+            fetch(n + 3).start()
+
     total = jnp.zeros((128, 1), F32)
     for k in range(8):
         v = mid_ref[k].astype(F32)
@@ -154,7 +164,7 @@
     factor = lax.rsqrt(total / 2048.0 + EPS)
     for k in range(8):
         rows = (mid_ref[k].astype(F32) * factor * gain[k]).astype(BF)
-        fetch(k, 0).wait()
+        arrive(k)
         for c in range(2):
             piece = w[k, :, c, :, 0:1408].reshape(256, 1408)
             part = jnp.dot(rows, piece, preferred_element_type=F32)
@@ -170,7 +180,7 @@
         u = acc[c, :, 1344:1408]
         hid[c, :, 640:704] = (g * jax.nn.sigmoid(g) * u).astype(BF)
     for k in range(8):
-        fetch(k, 1).wait()
+        arrive(8 + k)
         part = jnp.zeros((128, 256), F32)
         for c in range(2):
             piece = w[k, :, c, :, 1408:2112].reshape(256, 704)
@@ -200,14 +210,20 @@
 ):
     z, x, c = lax.axis_index("z"), lax.axis_index("x"), lax.axis_index("c")
     swap = [(0, 1), (1, 0)]
-    own, ffn_own, seqs = pl.pallas_call(
+    own, ffn_own, seqs, scales, gain, latter_gain, mats, offs, blend_gain = pl.pallas_call(
         pack_kernel,
-        in_specs=[VM] * 11,
-        out_specs=[VM] * 3,
+        in_specs=[VM] * 18,
+        out_specs=[VM] * 9,
         out_shape=[
             jax.ShapeDtypeStruct((8, 32, 640), BF),
             jax.ShapeDtypeStruct((32, 2112), BF),
             jax.ShapeDtypeStruct((8, 256, 256), BF),
+            pltpu.VMEM((1, 384), F32),
+            pltpu.VMEM((8, 1, 256), F32),
+            pltpu.VMEM((8, 1, 256), F32),
+            pltpu.VMEM((3, 128, 128), BF),
+            pltpu.VMEM((3, 128), F32),
+            pltpu.VMEM((1, 192), F32),
         ],
         name="pack",
     )(
@@ -222,31 +238,40 @@
         lowering_matrix.T,
         lowering_rescalers,
         sequence_entries,
+        conveyor_rescalers,
+        blend_rescalers,
+        former_norm_factor.reshape(8, 1, 256),
+        latter_norm_factor.reshape(8, 1, 256),
+        location_matrices,
+        location_offsets,
+        blend_norm_factor.reshape(1, 192),
     )
     ffn_all = lax.all_gather(ffn_own, ("z", "y", "c"), axis=0, tiled=True)
 
     first = lax.all_to_all(own, "y", 0, 0, tiled=True)
     rows = lax.all_to_all(seqs, TP, 0, 0, tiled=True)
-    left = exchange(first[:4].reshape(1, 128, 640), 0)
-    right = exchange(first[4:].reshape(1, 128, 640), 1)
+    left = [vmem(p) for p in exchange(first[:4].reshape(1, 128, 640), 0)]
+    right = [vmem(p) for p in exchange(first[4:].reshape(1, 128, 640), 1)]
     pieces = left + right
     order = blocks(z)
-
-    gain = former_norm_factor.reshape(8, 1, 256)
+    near = vmem(rows)
+
     prior, factor = pl.pallas_call(
         early_kernel,
         in_specs=[SM] + [VM] * 10,
         out_specs=[VM, VM],
-        out_shape=[jax.ShapeDtypeStruct((256, 384), F32), jax.ShapeDtypeStruct((256, 128), F32)],
+        out_shape=[pltpu.VMEM((256, 384), F32), pltpu.VMEM((256, 128), F32)],
+        compiler_params=limit(4),
         name="early",
-    )(order, rows, gain, *left[:4], *right[:4])
+    )(order, near, gain, *left[:4], *right[:4])
     act, own_sq = pl.pallas_call(
         project_kernel,
-        in_specs=[SM] + [VM] * 8,
+        in_specs=[SM] + [VM] * 7,
         out_specs=[VM, VM],
-        out_shape=[jax.ShapeDtypeStruct((256, 384), F32), jax.ShapeDtypeStruct((1, 1, 256), F32)],
+        out_shape=[pltpu.VMEM((256, 384), F32), jax.ShapeDtypeStruct((1, 1, 256), F32)],
+        compiler_params=limit(4),
         name="project",
-    )(order, rows, gain, conveyor_rescalers, blend_rescalers, prior, factor, left[4], right[4])
+    )(order, near, gain, scales, prior, factor, left[4], right[4])
     all_sq = lax.all_gather(own_sq, TP, axis=0, tiled=True)
     kept, sent = pl.pallas_call(
         gate_kernel,
@@ -254,15 +279,16 @@
         out_specs=[VM, VM],
         out_shape=[jax.ShapeDtypeStruct((8, 128, 256), BF)] * 2,
         scratch_shapes=[pltpu.VMEM((2, 128, 192), BF)],
+        compiler_params=limit(6),
         name="gating",
     )(
         order,
         c.astype(jnp.int32).reshape(1),
         act,
         all_sq,
-        location_matrices,
-        location_offsets,
-        blend_norm_factor,
+        mats,
+        offs,
+        blend_gain,
         *pieces,
     )
     got = lax.ppermute(sent, "c", swap)
@@ -273,17 +299,17 @@
     mid = from_everyone(mid_own, "x").reshape(8, 128, 256)
     outs = pl.pallas_call(
         ffn_kernel,
-        in_specs=[VM, VM, ANY],
+        in_specs=[VM, VM, pl.BlockSpec(memory_space=pltpu.HBM)],
         out_specs=VM,
         out_shape=jax.ShapeDtypeStruct((8, 128, 256), BF),
         scratch_shapes=[
             pltpu.VMEM((8, 8, 2, 32, 2112), BF),
             pltpu.VMEM((2, 128, 1408), F32),
             pltpu.VMEM((2, 128, 704), BF),
-            pltpu.SemaphoreType.DMA((2, 8)),
+            pltpu.SemaphoreType.DMA((16,)),
         ],
         name="ffn",
-    )(mid, latter_norm_factor.reshape(8, 1, 256), ffn_all.reshape(8, 8, 2, 32, 2112))
+    )(vmem(mid), latter_gain, ffn_all.reshape(8, 8, 2, 32, 2112))
     ffn_shares = lax.all_to_all(outs, TP, 0, 0, tiled=True).reshape(4, 2, 128, 256)
     mid_kept = lax.dynamic_index_in_dim(mid_own, c, 0, keepdims=False)
     mid_sent = lax.dynamic_index_in_dim(mid_own, 1 - c, 0, keepdims=False)
@@ -295,6 +321,14 @@
     return out.astype(BF).reshape(256, 256)
 
 
+def limit(mib):
+    return pltpu.CompilerParams(vmem_limit_bytes=mib << 20)
+
+
+def vmem(x):
+    return pltpu.with_memory_space_constraint(x, pltpu.VMEM)
+
+
 def solution(mesh):
     finer = Mesh(mesh.devices.reshape(8, 8, 4, 2), ("z", "y", "x", "c"))
     return jax.shard_map(

time: 181 us -> 173 us (0.956)
  Pallas kernels: 24.7 us -> 19.6 us
  waiting for transfers between devices: 39 us -> 42.3 us
  other arithmetic: 5.27 us -> 2.65 us
    ppermute x6, waiting for transfers between devices: 17.4 us -> 20.6 us  [exchange(): batch = lax.ppermute(batch, 'z', turn)]
    pallas_call x1, Pallas kernels: 3.86 us -> 1.61 us  [on_device(): pl.pallas_call(early_kernel, in_specs=[SM] + [VM] * 10, out_specs=[VM, VM...]
    pallas_call x1, Pallas kernels: 4.12 us -> 2.08 us  [on_device(): pl.pallas_call(gate_kernel, in_specs=[SM, SM] + [VM] * 15, out_specs=[VM,...]
  transfers between devices with their start and end apart: 14 -> 14, of which waited for: 10 -> 10; matrix products, arithmetic and copies ran while one was open for 3% -> 1% of each run, Pallas kernels for 6% -> 3%
where the time goes in v4:
time: 173 us
  starting transfers between devices  52.6 us (30%)
  waiting for transfers between devices  42.3 us (24%)
  blocking collectives  41.8 us (24%)
  Pallas kernels  19.6 us (11%)
  between operations  13.6 us (8%)
  other arithmetic  2.65 us (2%)
    ppermute x6, waiting for transfers between devices, exchange(): batch = lax.ppermute(batch, 'z', turn)  20.6 us
    all_to_all x1, blocking collectives, on_device(): first = lax.all_to_all(own, 'y', 0, 0, tiled=True)  17.6 us
    ppermute x6, starting transfers between devices, exchange(): batch = lax.ppermute(batch, 'z', turn)  16.6 us
    ppermute x2, starting transfers between devices, exchange(): got = lax.ppermute(own, 'z', to_pair)  14.3 us
    all_gather x1, blocking collectives, on_device(): all_sq = lax.all_gather(own_sq, TP, axis=0, tiled=True)  13.1 us
    pallas_call x1, Pallas kernels, on_device(): pl.pallas_call(ffn_kernel, in_specs=[VM, VM, pl.BlockSpec(memory_space=pl...  11.5 us
    all_to_all x1, blocking collectives, from_everyone(): return lax.all_to_all(copies, axis, split_axis=0, concat_axis=0, tiled=True)  11 us
    all_to_all x1, waiting for transfers between devices, on_device(): shares = lax.all_to_all(both, 'x', 0, 0, tiled=True)  9.4 us
  transfers between devices with their start and end apart: 14, of which 10 were waited for; matrix products, arithmetic and copies ran while one was open for 1% of the time, Pallas kernels for 3%

profile of v4, /device:TPU:1, one launch (start us, length us, event | category | flops | bytes accessed | tf_op | source)
XLA Modules:
  0.0 172.5 jit_solution(15269884554133006532)
XLA Ops:
  6.5 2.5 %pack.1 = (bf16[8,32,640]{2,1,0:T(8,128)(2,1)}, bf16[32,2112]{1,0:T(8,128)(2,1)}, bf16[8,256,256]{2,1,0:T(8,128)(2,1)}, f32[1,384]{1,0:T(1,128)S(1)}, f32[8,1,25...) custom-call(f32[32,192]{1,0:T(8,128)} %conv.1, ...), custom_call_target="tpu_custom_call" | custom-call | tf_op jit(solution)/shard_map/pack/pallas_call | solution.py:213
  9.1 17.6 %all_to_all.25 = bf16[8,32,640]{2,1,0:T(8,128)(2,1)S(1)} all-to-all(bf16[8,32,640]{2,1,0:T(8,128)(2,1)} %get-tuple-element.23), channel_id=1, replica_groups=mesh['z'=8,'y'=8,'x'=4,'c'=2] {'y'}, dimensions={0} | all-to-all | bytes 655360 | tf_op jit(solution)/shard_map/all_to_all | solution.py:251
  26.8 12.4 %collective-permute-start.3 = (bf16[1,128,640]{2,1,0:T(8,128)(2,1)S(1)}, bf16[1,128,640]{2,1,0:T(8,128)(2,1)S(1)}, u32[]{:S(2)}, u32[]{:S(2)}) collective-permute-start(bf16[1,128,640]{2,1,0:T(8,128)(2,1)S(1)} %bitcast.27), channel_id=1, source_target_pairs={{0,448},{64,128},{128,64},{192,256},{256,192},{320,384},{384,320},... | collective-permute-start | bytes 491528 | tf_op jit(solution)/shard_map/ppermute | solution.py:130
  39.2 1.9 %collective-permute-start = (bf16[1,128,640]{2,1,0:T(8,128)(2,1)S(1)}, bf16[1,128,640]{2,1,0:T(8,128)(2,1)S(1)}, u32[]{:S(2)}, u32[]{:S(2)}) collective-permute-start(bf16[1,128,640]{2,1,0:T(8,128)(2,1)S(1)} %bitcast.31), channel_id=1, source_target_pairs={{0,64},{64,0},{128,192},{192,128},{256,320},{320,256},{384,448},{4... | collective-permute-start | bytes 491528 | tf_op jit(solution)/shard_map/ppermute | solution.py:130
  41.1 1.8 %collective-permute-done.3.refs_5_.refs_6_ = bf16[1,128,640]{2,1,0:T(8,128)(2,1)S(1)} collective-permute-done((bf16[1,128,640]{2,1,0:T(8,128)(2,1)S(1)}, bf16[1,128,640]{2,1,0:T(8,128)(2,1)S(1)}, u32[]{:S(2)}, u32[]{:S(2)}) %collective-permute-start.3) | collective-permute-done | bytes 163872 | tf_op jit(solution)/shard_map/ppermute | solution.py:130
  42.9 1.9 %collective-permute-start.4 = (bf16[2,128,640]{2,1,0:T(8,128)(2,1)S(1)}, bf16[2,128,640]{2,1,0:T(8,128)(2,1)S(1)}, u32[]{:S(2)}, u32[]{:S(2)}) collective-permute-start(bf16[2,128,640]{2,1,0:T(8,128)(2,1)S(1)} %pad_maximum_fusion.1), channel_id=1, source_target_pairs={{0,64},{64,0},{128,192},{192,128},{256,320},{320,256},{384,448},{4... | collective-permute-start | bytes 983048 | tf_op jit(solution)/shard_map/ppermute | solution.py:134
  44.9 1.1 collective-permute-done.refs_1_
  46.0 2.6 %collective-permute-start.1 = (bf16[2,128,640]{2,1,0:T(8,128)(2,1)S(1)}, bf16[2,128,640]{2,1,0:T(8,128)(2,1)S(1)}, u32[]{:S(2)}, u32[]{:S(2)}) collective-permute-start(bf16[2,128,640]{2,1,0:T(8,128)(2,1)S(1)} %pad_maximum_fusion), channel_id=1, source_target_pairs={{0,448},{64,128},{128,64},{192,256},{256,192},{320,384},{384,320},... | collective-permute-start | bytes 983048 | tf_op jit(solution)/shard_map/ppermute | solution.py:134
  48.7 8.8 %all-to-all-start = ((bf16[8,256,256]{2,1,0:T(8,128)(2,1)}), bf16[8,256,256]{2,1,0:T(8,128)(2,1)S(1)}, u32[]{:S(2)}, u32[]{:S(2)}) async-start(bf16[8,256,256]{2,1,0:T(8,128)(2,1)} %get-tuple-element.20), calls=%async_computation | async-start | bytes 2097152 | tf_op jit(solution)/shard_map/all_to_all | solution.py:252
  57.5 4.8 %collective-permute-start.5 = (bf16[2,128,640]{2,1,0:T(8,128)(2,1)S(1)}, bf16[2,128,640]{2,1,0:T(8,128)(2,1)S(1)}, u32[]{:S(2)}, u32[]{:S(2)}) collective-permute-start(bf16[2,128,640]{2,1,0:T(8,128)(2,1)S(1)} %collective-permute-done.4.refs_6_.refs_7_), channel_id=1, source_target_pairs={{0,448},{64,128},{128,64},{192,256},{256,192},{320,384},{384,320},... | collective-permute-start | bytes 983048 | tf_op jit(solution)/shard_map/ppermute | solution.py:134
  62.3 1.9 %collective-permute-start.2 = (bf16[2,128,640]{2,1,0:T(8,128)(2,1)S(1)}, bf16[2,128,640]{2,1,0:T(8,128)(2,1)S(1)}, u32[]{:S(2)}, u32[]{:S(2)}) collective-permute-start(bf16[2,128,640]{2,1,0:T(8,128)(2,1)S(1)} %collective-permute-done.1.refs_2_), channel_id=1, source_target_pairs={{0,64},{64,0},{128,192},{192,128},{256,320},{320,256},{384,448},{4... | collective-permute-start | bytes 983048 | tf_op jit(solution)/shard_map/ppermute | solution.py:134
  64.3 5.2 %collective-permute-done.5.refs_7_.refs_8_ = bf16[2,128,640]{2,1,0:T(8,128)(2,1)S(1)} collective-permute-done((bf16[2,128,640]{2,1,0:T(8,128)(2,1)S(1)}, bf16[2,128,640]{2,1,0:T(8,128)(2,1)S(1)}, u32[]{:S(2)}, u32[]{:S(2)}) %collective-permute-start.5) | collective-permute-done | bytes 327712 | tf_op jit(solution)/shard_map/ppermute | solution.py:134
  69.4 1.9 %collective-permute-start.7 = (bf16[2,128,640]{2,1,0:T(8,128)(2,1)S(1)}, bf16[2,128,640]{2,1,0:T(8,128)(2,1)S(1)}, u32[]{:S(2)}, u32[]{:S(2)}) collective-permute-start(bf16[2,128,640]{2,1,0:T(8,128)(2,1)S(1)} %collective-permute-done.5.refs_7_.refs_8_), channel_id=1, source_target_pairs={{0,64},{64,0},{128,192},{192,128},{256,320},{320,256},{384,448},{4... | collective-permute-start | bytes 983048 | tf_op jit(solution)/shard_map/ppermute | solution.py:134
  71.4 1.8 %collective-permute-done.2.refs_3_ = bf16[2,128,640]{2,1,0:T(8,128)(2,1)S(1)} collective-permute-done((bf16[2,128,640]{2,1,0:T(8,128)(2,1)S(1)}, bf16[2,128,640]{2,1,0:T(8,128)(2,1)S(1)}, u32[]{:S(2)}, u32[]{:S(2)}) %collective-permute-start.2) | collective-permute-done | bytes 327712 | tf_op jit(solution)/shard_map/ppermute | solution.py:134
  73.2 3.4 %collective-permute-start.6 = (bf16[2,128,640]{2,1,0:T(8,128)(2,1)S(1)}, bf16[2,128,640]{2,1,0:T(8,128)(2,1)}, u32[]{:S(2)}, u32[]{:S(2)}) collective-permute-start(bf16[2,128,640]{2,1,0:T(8,128)(2,1)S(1)} %collective-permute-done.2.refs_3_), channel_id=1, source_target_pairs={{0,448},{64,128},{128,64},{192,256},{256,192},{320,384},{384,320},... | collective-permute-start | bytes 983048 | tf_op jit(solution)/shard_map/ppermute | solution.py:134
  77.3 1.6 early.1
  79.0 8.5 %collective-permute-done.7.right.refs_9_ = bf16[2,128,640]{2,1,0:T(8,128)(2,1)S(1)} collective-permute-done((bf16[2,128,640]{2,1,0:T(8,128)(2,1)S(1)}, bf16[2,128,640]{2,1,0:T(8,128)(2,1)S(1)}, u32[]{:S(2)}, u32[]{:S(2)}) %collective-permute-start.7) | collective-permute-done | bytes 327712 | tf_op jit(solution)/shard_map/ppermute | solution.py:134
  87.5 5.1 %collective-permute-done.6.left.refs_4_ = bf16[2,128,640]{2,1,0:T(8,128)(2,1)} collective-permute-done((bf16[2,128,640]{2,1,0:T(8,128)(2,1)S(1)}, bf16[2,128,640]{2,1,0:T(8,128)(2,1)}, u32[]{:S(2)}, u32[]{:S(2)}) %collective-permute-start.6) | collective-permute-done | bytes 327712 | tf_op jit(solution)/shard_map/ppermute | solution.py:134
  92.6 1.9 %project.1 = (f32[256,384]{1,0:T(8,128)S(1)}, f32[1,1,256]{2,1,0:T(1,128)S(1)}) custom-call(s32[2,8]{1,0:T(2,128)S(1)} %add_and_fusion.order, bf16[8,256,256]{2,1,0:T(8,128)(2,1)S(1)} %all-to-all-done.x_ref, f32[8,1,256]{2,1,0:T(1,128)S(1)} %get-tuple-element.21.gain, f32[1,384]{1,0:T(1,128)S(1)} %get-tuple-element.22.scales, ...), custom_call_target="tpu_custom_call" | custom-call | tf_op jit(solution)/shard_map/project/pallas_call | solution.py:267
  94.4 13.1 %all_gather.6.sq_ref = f32[8,1,256]{2,1,0:T(1,128)S(1)} all-gather(f32[1,1,256]{2,1,0:T(1,128)S(1)} %get-tuple-element.27), channel_id=1, replica_groups=mesh['z'=8,'y'=8,'x'=4,'c'=2] {'x','c'}, dimensions={0}, use_global_device_ids=true | all-gather | bytes 9216 | tf_op jit(solution)/shard_map/all_gather | solution.py:275
  107.6 2.1 %gating.1 = (bf16[8,128,256]{2,1,0:T(8,128)(2,1)S(1)}, bf16[8,128,256]{2,1,0:T(8,128)(2,1)S(1)}) custom-call(s32[2,8]{1,0:T(2,128)S(1)} %add_and_fusion.order, s32[1]{0:T(128)} %bitcast.5.core, f32[256,384]{1,0:T(8,128)S(1)} %get-tuple-element.26.act_ref, f32[8,1,256]{2,1,0:T(1,128)S(1)} %all_gather.6.sq_ref, ...), custom_call_target="tpu_custom_call" | custom-call | tf_op jit(solution)/shard_map/gating/pallas_call | solution.py:276
  109.7 2.1 %collective-permute-start.8 = (bf16[8,128,256]{2,1,0:T(8,128)(2,1)S(1)}, bf16[8,128,256]{2,1,0:T(8,128)(2,1)S(1)}, u32[]{:S(2)}, u32[]{:S(2)}) collective-permute-start(bf16[8,128,256]{2,1,0:T(8,128)(2,1)S(1)} %get-tuple-element.32), channel_id=1, source_target_pairs={{0,1},{1,0},{2,3},{3,2},{4,5},{5,4},{6,7},{7,6},{8,9},{9,8},{10,11... | collective-permute-start | bytes 1572872 | tf_op jit(solution)/shard_map/ppermute | solution.py:294
  111.7 2.0 %collective-permute-done.8 = bf16[8,128,256]{2,1,0:T(8,128)(2,1)S(1)} collective-permute-done((bf16[8,128,256]{2,1,0:T(8,128)(2,1)S(1)}, bf16[8,128,256]{2,1,0:T(8,128)(2,1)S(1)}, u32[]{:S(2)}, u32[]{:S(2)}) %collective-permute-start.8) | collective-permute-done | bytes 524320 | tf_op jit(solution)/shard_map/ppermute | solution.py:294
  113.8 0.9 add_convert_fusion
  114.7 3.5 %all-to-all-start.2 = ((bf16[4,2,128,256]{3,2,1,0:T(8,128)(2,1)}), bf16[4,2,128,256]{3,2,1,0:T(8,128)(2,1)S(1)}, u32[]{:S(2)}, u32[]{:S(2)}) async-start(bf16[4,2,128,256]{3,2,1,0:T(8,128)(2,1)} %bitcast.8), calls=%async_computation.2 | async-start | bytes 1048576 | tf_op jit(solution)/shard_map/all_to_all | solution.py:296
  118.2 9.4 %all-to-all-done.2 = bf16[4,2,128,256]{3,2,1,0:T(8,128)(2,1)S(1)} async-done(((bf16[4,2,128,256]{3,2,1,0:T(8,128)(2,1)}), bf16[4,2,128,256]{3,2,1,0:T(8,128)(2,1)S(1)}, u32[]{:S(2)}, u32[]{:S(2)}) %all-to-all-start.2) | async-done | bytes 524320 | tf_op jit(solution)/shard_map/all_to_all | solution.py:296
  127.8 11.0 %all_to_all.26 = bf16[4,2,128,256]{3,2,1,0:T(8,128)(2,1)S(1)} all-to-all(bf16[4,2,128,256]{3,2,1,0:T(8,128)(2,1)S(1)} %broadcast_in_dim.2), channel_id=1, replica_groups=mesh['z'=8,'y'=8,'x'=4,'c'=2] {'x'}, dimensions={0} | all-to-all | bytes 1048576 | tf_op jit(solution)/shard_map/all_to_all | solution.py:22
  138.7 11.5 %ffn.1 = bf16[8,128,256]{2,1,0:T(8,128)(2,1)} custom-call(bf16[8,128,256]{2,1,0:T(8,128)(2,1)S(1)} %bitcast.35, f32[8,1,256]{2,1,0:T(1,128)} %copy-done, bf16[8,8,2,32,2112]{4,3,2,1,0:T(8,128)(2,1)} %bitcast.36), custom_call_target="tpu_custom_call" | custom-call | tf_op jit(solution)/shard_map/ffn/pallas_call | solution.py:300
  150.3 5.3 %all-to-all-start.4 = ((bf16[8,128,256]{2,1,0:T(8,128)(2,1)}), bf16[8,128,256]{2,1,0:T(8,128)(2,1)S(1)}, u32[]{:S(2)}, u32[]{:S(2)}) async-start(bf16[8,128,256]{2,1,0:T(8,128)(2,1)} %ffn.1), calls=%async_computation.4 | async-start | bytes 1048576 | tf_op jit(solution)/shard_map/all_to_all | solution.py:313
  155.5 2.0 %collective-permute-start.9 = (bf16[128,256]{1,0:T(8,128)(2,1)S(1)}, bf16[128,256]{1,0:T(8,128)(2,1)S(1)}, u32[]{:S(2)}, u32[]{:S(2)}) collective-permute-start(bf16[128,256]{1,0:T(8,128)(2,1)S(1)} %dynamic-slice_bitcast_fusion), channel_id=1, source_target_pairs={{0,1},{1,0},{2,3},{3,2},{4,5},{5,4},{6,7},{7,6},{8,9},{9,8},{10,11... | collective-permute-start | bytes 196616 | tf_op jit(solution)/shard_map/ppermute | solution.py:316
  157.6 1.1 collective-permute-done.9
  158.7 6.2 %all-to-all-done.4 = bf16[8,128,256]{2,1,0:T(8,128)(2,1)S(1)} async-done(((bf16[8,128,256]{2,1,0:T(8,128)(2,1)}), bf16[8,128,256]{2,1,0:T(8,128)(2,1)S(1)}, u32[]{:S(2)}, u32[]{:S(2)}) %all-to-all-start.4) | async-done | bytes 524320 | tf_op jit(solution)/shard_map/all_to_all | solution.py:313
  (20 shorter events, 1.8 us)
Async XLA Ops:
  6.5 132.2 %all-gather.2.cloned.1.call-start = ((), (), s32[]{:S(2)}) async-start(), calls=%async_computation.5 | async-start | bytes 17965056 | tf_op jit(solution)/shard_map/all_gather | solution.py:249
  9.0 39.6 %copy-start = (f32[8,1,256]{2,1,0:T(1,128)}, f32[8,1,256]{2,1,0:T(1,128)S(1)}, u32[]{:S(2)}) copy-start(f32[8,1,256]{2,1,0:T(1,128)S(1)} %get-tuple-element.33.gain) | copy-start | bytes 24580
  26.8 16.1 %collective-permute-start.3 = (bf16[1,128,640]{2,1,0:T(8,128)(2,1)S(1)}, bf16[1,128,640]{2,1,0:T(8,128)(2,1)S(1)}, u32[]{:S(2)}, u32[]{:S(2)}) collective-permute-start(bf16[1,128,640]{2,1,0:T(8,128)(2,1)S(1)} %bitcast.27), channel_id=1, source_target_pairs={{0,448},{64,128},{128,64},{192,256},{256,192},{320,384},{384,320},... | collective-permute-start | bytes 491528 | tf_op jit(solution)/shard_map/ppermute | solution.py:130
  39.2 6.8 %collective-permute-start = (bf16[1,128,640]{2,1,0:T(8,128)(2,1)S(1)}, bf16[1,128,640]{2,1,0:T(8,128)(2,1)S(1)}, u32[]{:S(2)}, u32[]{:S(2)}) collective-permute-start(bf16[1,128,640]{2,1,0:T(8,128)(2,1)S(1)} %bitcast.31), channel_id=1, source_target_pairs={{0,64},{64,0},{128,192},{192,128},{256,320},{320,256},{384,448},{4... | collective-permute-start | bytes 491528 | tf_op jit(solution)/shard_map/ppermute | solution.py:130
  42.9 14.5 %collective-permute-start.4 = (bf16[2,128,640]{2,1,0:T(8,128)(2,1)S(1)}, bf16[2,128,640]{2,1,0:T(8,128)(2,1)S(1)}, u32[]{:S(2)}, u32[]{:S(2)}) collective-permute-start(bf16[2,128,640]{2,1,0:T(8,128)(2,1)S(1)} %pad_maximum_fusion.1), channel_id=1, source_target_pairs={{0,64},{64,0},{128,192},{192,128},{256,320},{320,256},{384,448},{4... | collective-permute-start | bytes 983048 | tf_op jit(solution)/shard_map/ppermute | solution.py:134
  46.0 16.3 %collective-permute-start.1 = (bf16[2,128,640]{2,1,0:T(8,128)(2,1)S(1)}, bf16[2,128,640]{2,1,0:T(8,128)(2,1)S(1)}, u32[]{:S(2)}, u32[]{:S(2)}) collective-permute-start(bf16[2,128,640]{2,1,0:T(8,128)(2,1)S(1)} %pad_maximum_fusion), channel_id=1, source_target_pairs={{0,448},{64,128},{128,64},{192,256},{256,192},{320,384},{384,320},... | collective-permute-start | bytes 983048 | tf_op jit(solution)/shard_map/ppermute | solution.py:134
  48.7 28.7 %all-to-all-start = ((bf16[8,256,256]{2,1,0:T(8,128)(2,1)}), bf16[8,256,256]{2,1,0:T(8,128)(2,1)S(1)}, u32[]{:S(2)}, u32[]{:S(2)}) async-start(bf16[8,256,256]{2,1,0:T(8,128)(2,1)} %get-tuple-element.20), calls=%async_computation | async-start | bytes 2097152 | tf_op jit(solution)/shard_map/all_to_all | solution.py:252
  57.5 12.0 %collective-permute-start.5 = (bf16[2,128,640]{2,1,0:T(8,128)(2,1)S(1)}, bf16[2,128,640]{2,1,0:T(8,128)(2,1)S(1)}, u32[]{:S(2)}, u32[]{:S(2)}) collective-permute-start(bf16[2,128,640]{2,1,0:T(8,128)(2,1)S(1)} %collective-permute-done.4.refs_6_.refs_7_), channel_id=1, source_target_pairs={{0,448},{64,128},{128,64},{192,256},{256,192},{320,384},{384,320},... | collective-permute-start | bytes 983048 | tf_op jit(solution)/shard_map/ppermute | solution.py:134
  62.3 10.9 %collective-permute-start.2 = (bf16[2,128,640]{2,1,0:T(8,128)(2,1)S(1)}, bf16[2,128,640]{2,1,0:T(8,128)(2,1)S(1)}, u32[]{:S(2)}, u32[]{:S(2)}) collective-permute-start(bf16[2,128,640]{2,1,0:T(8,128)(2,1)S(1)} %collective-permute-done.1.refs_2_), channel_id=1, source_target_pairs={{0,64},{64,0},{128,192},{192,128},{256,320},{320,256},{384,448},{4... | collective-permute-start | bytes 983048 | tf_op jit(solution)/shard_map/ppermute | solution.py:134
  69.4 18.0 %collective-permute-start.7 = (bf16[2,128,640]{2,1,0:T(8,128)(2,1)S(1)}, bf16[2,128,640]{2,1,0:T(8,128)(2,1)S(1)}, u32[]{:S(2)}, u32[]{:S(2)}) collective-permute-start(bf16[2,128,640]{2,1,0:T(8,128)(2,1)S(1)} %collective-permute-done.5.refs_7_.refs_8_), channel_id=1, source_target_pairs={{0,64},{64,0},{128,192},{192,128},{256,320},{320,256},{384,448},{4... | collective-permute-start | bytes 983048 | tf_op jit(solution)/shard_map/ppermute | solution.py:134
  73.2 19.4 %collective-permute-start.6 = (bf16[2,128,640]{2,1,0:T(8,128)(2,1)S(1)}, bf16[2,128,640]{2,1,0:T(8,128)(2,1)}, u32[]{:S(2)}, u32[]{:S(2)}) collective-permute-start(bf16[2,128,640]{2,1,0:T(8,128)(2,1)S(1)} %collective-permute-done.2.refs_3_), channel_id=1, source_target_pairs={{0,448},{64,128},{128,64},{192,256},{256,192},{320,384},{384,320},... | collective-permute-start | bytes 983048 | tf_op jit(solution)/shard_map/ppermute | solution.py:134
  109.7 4.1 %collective-permute-start.8 = (bf16[8,128,256]{2,1,0:T(8,128)(2,1)S(1)}, bf16[8,128,256]{2,1,0:T(8,128)(2,1)S(1)}, u32[]{:S(2)}, u32[]{:S(2)}) collective-permute-start(bf16[8,128,256]{2,1,0:T(8,128)(2,1)S(1)} %get-tuple-element.32), channel_id=1, source_target_pairs={{0,1},{1,0},{2,3},{3,2},{4,5},{5,4},{6,7},{7,6},{8,9},{9,8},{10,11... | collective-permute-start | bytes 1572872 | tf_op jit(solution)/shard_map/ppermute | solution.py:294
  114.7 12.9 %all-to-all-start.2 = ((bf16[4,2,128,256]{3,2,1,0:T(8,128)(2,1)}), bf16[4,2,128,256]{3,2,1,0:T(8,128)(2,1)S(1)}, u32[]{:S(2)}, u32[]{:S(2)}) async-start(bf16[4,2,128,256]{3,2,1,0:T(8,128)(2,1)} %bitcast.8), calls=%async_computation.2 | async-start | bytes 1048576 | tf_op jit(solution)/shard_map/all_to_all | solution.py:296
  150.3 14.6 %all-to-all-start.4 = ((bf16[8,128,256]{2,1,0:T(8,128)(2,1)}), bf16[8,128,256]{2,1,0:T(8,128)(2,1)S(1)}, u32[]{:S(2)}, u32[]{:S(2)}) async-start(bf16[8,128,256]{2,1,0:T(8,128)(2,1)} %ffn.1), calls=%async_computation.4 | async-start | bytes 1048576 | tf_op jit(solution)/shard_map/all_to_all | solution.py:313
  155.5 3.1 %collective-permute-start.9 = (bf16[128,256]{1,0:T(8,128)(2,1)S(1)}, bf16[128,256]{1,0:T(8,128)(2,1)S(1)}, u32[]{:S(2)}, u32[]{:S(2)}) collective-permute-start(bf16[128,256]{1,0:T(8,128)(2,1)S(1)} %dynamic-slice_bitcast_fusion), channel_id=1, source_target_pairs={{0,1},{1,0},{2,3},{3,2},{4,5},{5,4},{6,7},{7,6},{8,9},{9,8},{10,11... | collective-permute-start | bytes 196616 | tf_op jit(solution)/shard_map/ppermute | solution.py:316
Sparse Core Ops, SparseCore 0:
  10.5 116.3 all-gather.1

commit v5 on v4

--- a/solution.py
+++ b/solution.py
@@ -71,14 +71,14 @@
 
 
 def early_kernel(order, x_ref, gain, *refs):
-    pieces, prior_ref, factor_ref = refs[:8], refs[8], refs[9]
+    pieces, prior_ref, factor_ref = refs[:6], refs[6], refs[7]
     total = jnp.zeros((256, 1), F32)
     for k in range(8):
         v = x_ref[k].astype(F32)
         total = total + jnp.sum(v * v, axis=1, keepdims=True)
     factor = lax.rsqrt(total / 2048.0 + EPS)
     factor_ref[...] = jnp.broadcast_to(factor, (256, 128))
-    found = spread(order, pieces[:4], pieces[4:])
+    found = spread(order, pieces[:3], pieces[3:])
     prior_ref[...] = multiply(found, x_ref, gain, factor, jnp.zeros((256, 384), F32))
 
 
@@ -96,7 +96,7 @@
 
 
 def gate_kernel(order, core, act_ref, sq_ref, mats, offs, gain, *refs):
-    pieces, kept, sent, gated = refs[:10], refs[10], refs[11], refs[12]
+    pieces, kept, sent, gated = refs[:8], refs[8], refs[9], refs[10]
     total = jnp.sum(sq_ref[...], axis=0)
     factor = lax.rsqrt(total / 1536.0 + EPS)
     rows = lax.broadcasted_iota(jnp.int32, (128, 128), 0)
@@ -115,8 +115,8 @@
             ).astype(BF)
     here = core[0]
     mine, other = gated[here], gated[1 - here]
-    for block, half, ref, k in spread(order, pieces[:5], pieces[5:]):
-        piece = ref[k, :, 384:576]
+    for block, half, ref, k in spread(order, pieces[:4], pieces[4:]):
+        piece = ref[k, :, 0:192]
         cols = pl.ds(128 * half, 128)
         part = lax.dot_general(mine, piece, NT, preferred_element_type=F32)
         kept[block, :, cols] = part.astype(BF)
@@ -129,7 +129,7 @@
     to_next = [(i, (((i + 1 - flip) ^ 1) - 1 + flip) % 8) for i in range(8)]
     got = lax.ppermute(own, "z", to_pair)
     batch = jnp.concatenate([own, got])
-    pieces = [own, got]
+    pieces = [batch]
     for turn in (to_next, to_pair, to_next):
         batch = lax.ppermute(batch, "z", turn)
         pieces.append(batch)
@@ -250,20 +250,24 @@
 
     first = lax.all_to_all(own, "y", 0, 0, tiled=True)
     rows = lax.all_to_all(seqs, TP, 0, 0, tiled=True)
-    left = [vmem(p) for p in exchange(first[:4].reshape(1, 128, 640), 0)]
-    right = [vmem(p) for p in exchange(first[4:].reshape(1, 128, 640), 1)]
-    pieces = left + right
+    streams = {}
+    for name, cols in (("cb", slice(0, 384)), ("em", slice(384, 640))):
+        for flip in range(2):
+            half = first[4 * flip : 4 * flip + 4, :, cols].reshape(1, 128, -1)
+            streams[name, flip] = [vmem(p) for p in exchange(half, flip)]
+    left, right = streams["cb", 0], streams["cb", 1]
+    pieces = streams["em", 0] + streams["em", 1]
     order = blocks(z)
     near = vmem(rows)
 
     prior, factor = pl.pallas_call(
         early_kernel,
-        in_specs=[SM] + [VM] * 10,
+        in_specs=[SM] + [VM] * 8,
         out_specs=[VM, VM],
         out_shape=[pltpu.VMEM((256, 384), F32), pltpu.VMEM((256, 128), F32)],
         compiler_params=limit(4),
         name="early",
-    )(order, near, gain, *left[:4], *right[:4])
+    )(order, near, gain, *left[:3], *right[:3])
     act, own_sq = pl.pallas_call(
         project_kernel,
         in_specs=[SM] + [VM] * 7,
@@ -271,11 +275,11 @@
         out_shape=[pltpu.VMEM((256, 384), F32), jax.ShapeDtypeStruct((1, 1, 256), F32)],
         compiler_params=limit(4),
         name="project",
-    )(order, near, gain, scales, prior, factor, left[4], right[4])
+    )(order, near, gain, scales, prior, factor, left[3], right[3])
     all_sq = lax.all_gather(own_sq, TP, axis=0, tiled=True)
     kept, sent = pl.pallas_call(
         gate_kernel,
-        in_specs=[SM, SM] + [VM] * 15,
+        in_specs=[SM, SM] + [VM] * 13,
         out_specs=[VM, VM],
         out_shape=[jax.ShapeDtypeStruct((8, 128, 256), BF)] * 2,
         scratch_shapes=[pltpu.VMEM((2, 128, 192), BF)],

time: 173 us -> 191 us (1.10)
  starting transfers between devices: 52.6 us -> 73.4 us
  waiting for transfers between devices: 42.3 us -> 35.1 us
  local copies, waits for them, and re-layouts: 0.07 us -> 2.35 us
  blocking collectives: 41.8 us -> 43.9 us
    ppermute x6 -> x12, starting transfers between devices: 16.6 us -> 34.1 us  [exchange(): batch = lax.ppermute(batch, 'z', turn)]
    ppermute x6 -> x12, waiting for transfers between devices: 20.6 us -> 16.5 us  [exchange(): batch = lax.ppermute(batch, 'z', turn)]
    ppermute x2 -> x4, starting transfers between devices: 14.3 us -> 17.9 us  [exchange(): got = lax.ppermute(own, 'z', to_pair)]
    ppermute x2 -> x4, waiting for transfers between devices: 2.9 us -> 0.01 us  [exchange(): got = lax.ppermute(own, 'z', to_pair)]
    unnamed x2 -> x14, local copies, waits for them, and re-layouts: 0.01 us -> 2.28 us
    all_gather x1, blocking collectives: 13.1 us -> 15.3 us  [on_device(): all_sq = lax.all_gather(own_sq, TP, axis=0, tiled=True)]
  transfers between devices with their start and end apart: 14 -> 22, of which waited for: 10 -> 7; matrix products, arithmetic and copies ran while one was open for 1% -> 1% of each run, Pallas kernels for 3% -> 3%
where the time goes in v5:
time: 191 us; the launch traced here: 190 us
  starting transfers between devices  73.4 us (38%)
  blocking collectives  43.9 us (23%)
  waiting for transfers between devices  35.1 us (18%)
  Pallas kernels  19 us (10%)
  between operations  13.8 us (7%)
  other arithmetic  2.63 us (1%)
  local copies, waits for them, and re-layouts  2.35 us (1%)
    ppermute x12, starting transfers between devices, exchange(): batch = lax.ppermute(batch, 'z', turn)  34.1 us
    ppermute x4, starting transfers between devices, exchange(): got = lax.ppermute(own, 'z', to_pair)  17.9 us
    all_to_all x1, blocking collectives, on_device(): first = lax.all_to_all(own, 'y', 0, 0, tiled=True)  17.6 us
    ppermute x12, waiting for transfers between devices, exchange(): batch = lax.ppermute(batch, 'z', turn)  16.5 us
    all_gather x1, blocking collectives, on_device(): all_sq = lax.all_gather(own_sq, TP, axis=0, tiled=True)  15.3 us
    pallas_call x1, Pallas kernels, on_device(): pl.pallas_call(ffn_kernel, in_specs=[VM, VM, pl.BlockSpec(memory_space=pl...  11.5 us
    all_to_all x1, blocking collectives, from_everyone(): return lax.all_to_all(copies, axis, split_axis=0, concat_axis=0, tiled=True)  11 us
    all_to_all x1, waiting for transfers between devices, on_device(): shares = lax.all_to_all(both, 'x', 0, 0, tiled=True)  9.4 us
  transfers between devices with their start and end apart: 22, of which 7 were waited for; matrix products, arithmetic and copies ran while one was open for 1% of the time, Pallas kernels for 3%

profile of v5, /device:TPU:1, one launch (start us, length us, event | category | flops | bytes accessed | tf_op | source)
XLA Modules:
  0.0 190.2 jit_solution(7217902712953503866)
XLA Ops:
  6.5 2.5 %pack.1 = (bf16[8,32,640]{2,1,0:T(8,128)(2,1)}, bf16[32,2112]{1,0:T(8,128)(2,1)}, bf16[8,256,256]{2,1,0:T(8,128)(2,1)}, f32[1,384]{1,0:T(1,128)S(1)}, f32[8,1,25...) custom-call(f32[32,192]{1,0:T(8,128)} %conv.1, ...), custom_call_target="tpu_custom_call" | custom-call | tf_op jit(solution)/shard_map/pack/pallas_call | solution.py:213
  9.1 17.6 %all_to_all.25 = bf16[8,32,640]{2,1,0:T(8,128)(2,1)S(1)} all-to-all(bf16[8,32,640]{2,1,0:T(8,128)(2,1)} %get-tuple-element.23), channel_id=1, replica_groups=mesh['z'=8,'y'=8,'x'=4,'c'=2] {'y'}, dimensions={0} | all-to-all | bytes 655360 | tf_op jit(solution)/shard_map/all_to_all | solution.py:251
  26.7 8.5 %all-to-all-start = ((bf16[8,256,256]{2,1,0:T(8,128)(2,1)}), bf16[8,256,256]{2,1,0:T(8,128)(2,1)S(1)}, u32[]{:S(2)}, u32[]{:S(2)}) async-start(bf16[8,256,256]{2,1,0:T(8,128)(2,1)} %get-tuple-element.20), calls=%async_computation | async-start | bytes 2097152 | tf_op jit(solution)/shard_map/all_to_all | solution.py:252
  35.3 10.7 %collective-permute-start.3 = (bf16[1,128,384]{2,1,0:T(8,128)(2,1)S(1)}, bf16[1,128,384]{2,1,0:T(8,128)(2,1)S(1)}, u32[]{:S(2)}, u32[]{:S(2)}) collective-permute-start(bf16[1,128,384]{2,1,0:T(8,128)(2,1)S(1)} %bitcast.34), channel_id=1, source_target_pairs={{0,448},{64,128},{128,64},{192,256},{256,192},{320,384},{384,320},... | collective-permute-start | bytes 294920 | tf_op jit(solution)/shard_map/ppermute | solution.py:130
  46.0 1.9 %collective-permute-start = (bf16[1,128,384]{2,1,0:T(8,128)(2,1)S(1)}, bf16[1,128,384]{2,1,0:T(8,128)(2,1)S(1)}, u32[]{:S(2)}, u32[]{:S(2)}) collective-permute-start(bf16[1,128,384]{2,1,0:T(8,128)(2,1)S(1)} %bitcast.32), channel_id=1, source_target_pairs={{0,64},{64,0},{128,192},{192,128},{256,320},{320,256},{384,448},{4... | collective-permute-start | bytes 294920 | tf_op jit(solution)/shard_map/ppermute | solution.py:130
  47.9 3.4 %collective-permute-start.8 = (bf16[1,128,256]{2,1,0:T(8,128)(2,1)S(1)}, bf16[1,128,256]{2,1,0:T(8,128)(2,1)S(1)}, u32[]{:S(2)}, u32[]{:S(2)}) collective-permute-start(bf16[1,128,256]{2,1,0:T(8,128)(2,1)S(1)} %bitcast.38), channel_id=1, source_target_pairs={{0,64},{64,0},{128,192},{192,128},{256,320},{320,256},{384,448},{4... | collective-permute-start | bytes 196616 | tf_op jit(solution)/shard_map/ppermute | solution.py:130
  51.3 1.9 %collective-permute-start.12 = (bf16[1,128,256]{2,1,0:T(8,128)(2,1)S(1)}, bf16[1,128,256]{2,1,0:T(8,128)(2,1)S(1)}, u32[]{:S(2)}, u32[]{:S(2)}) collective-permute-start(bf16[1,128,256]{2,1,0:T(8,128)(2,1)S(1)} %bitcast.36), channel_id=1, source_target_pairs={{0,448},{64,128},{128,64},{192,256},{256,192},{320,384},{384,320},... | collective-permute-start | bytes 196616 | tf_op jit(solution)/shard_map/ppermute | solution.py:130
  53.3 1.9 %collective-permute-start.4 = (bf16[2,128,384]{2,1,0:T(8,128)(2,1)S(1)}, bf16[2,128,384]{2,1,0:T(8,128)(2,1)S(1)}, u32[]{:S(2)}, u32[]{:S(2)}) collective-permute-start(bf16[2,128,384]{2,1,0:T(8,128)(2,1)S(1)} %pad_maximum_fusion.1.refs_3_), channel_id=1, source_target_pairs={{0,64},{64,0},{128,192},{192,128},{256,320},{320,256},{384,448},{4... | collective-permute-start | bytes 589832 | tf_op jit(solution)/shard_map/ppermute | solution.py:134
  55.2 4.6 %collective-permute-start.1 = (bf16[2,128,384]{2,1,0:T(8,128)(2,1)S(1)}, bf16[2,128,384]{2,1,0:T(8,128)(2,1)S(1)}, u32[]{:S(2)}, u32[]{:S(2)}) collective-permute-start(bf16[2,128,384]{2,1,0:T(8,128)(2,1)S(1)} %pad_maximum_fusion.refs_0_), channel_id=1, source_target_pairs={{0,448},{64,128},{128,64},{192,256},{256,192},{320,384},{384,320},... | collective-permute-start | bytes 589832 | tf_op jit(solution)/shard_map/ppermute | solution.py:134
  59.9 1.9 %collective-permute-start.9 = (bf16[2,128,256]{2,1,0:T(8,128)(2,1)S(1)}, bf16[2,128,256]{2,1,0:T(8,128)(2,1)S(1)}, u32[]{:S(2)}, u32[]{:S(2)}) collective-permute-start(bf16[2,128,256]{2,1,0:T(8,128)(2,1)S(1)} %pad_maximum_fusion.2.refs_0_), channel_id=1, source_target_pairs={{0,448},{64,128},{128,64},{192,256},{256,192},{320,384},{384,320},... | collective-permute-start | bytes 393224 | tf_op jit(solution)/shard_map/ppermute | solution.py:134
  61.8 2.2 %collective-permute-start.13 = (bf16[2,128,256]{2,1,0:T(8,128)(2,1)S(1)}, bf16[2,128,256]{2,1,0:T(8,128)(2,1)S(1)}, u32[]{:S(2)}, u32[]{:S(2)}) collective-permute-start(bf16[2,128,256]{2,1,0:T(8,128)(2,1)S(1)} %pad_maximum_fusion.3.refs_4_), channel_id=1, source_target_pairs={{0,64},{64,0},{128,192},{192,128},{256,320},{320,256},{384,448},{4... | collective-permute-start | bytes 393224 | tf_op jit(solution)/shard_map/ppermute | solution.py:134
  64.0 4.6 %collective-permute-start.5 = (bf16[2,128,384]{2,1,0:T(8,128)(2,1)S(1)}, bf16[2,128,384]{2,1,0:T(8,128)(2,1)S(1)}, u32[]{:S(2)}, u32[]{:S(2)}) collective-permute-start(bf16[2,128,384]{2,1,0:T(8,128)(2,1)S(1)} %collective-permute-done.4.refs_4_), channel_id=1, source_target_pairs={{0,448},{64,128},{128,64},{192,256},{256,192},{320,384},{384,320},... | collective-permute-start | bytes 589832 | tf_op jit(solution)/shard_map/ppermute | solution.py:134
  68.6 1.9 %collective-permute-start.2 = (bf16[2,128,384]{2,1,0:T(8,128)(2,1)S(1)}, bf16[2,128,384]{2,1,0:T(8,128)(2,1)S(1)}, u32[]{:S(2)}, u32[]{:S(2)}) collective-permute-start(bf16[2,128,384]{2,1,0:T(8,128)(2,1)S(1)} %collective-permute-done.1.refs_1_), channel_id=1, source_target_pairs={{0,64},{64,0},{128,192},{192,128},{256,320},{320,256},{384,448},{4... | collective-permute-start | bytes 589832 | tf_op jit(solution)/shard_map/ppermute | solution.py:134
  70.5 3.4 %collective-permute-start.10 = (bf16[2,128,256]{2,1,0:T(8,128)(2,1)S(1)}, bf16[2,128,256]{2,1,0:T(8,128)(2,1)S(1)}, u32[]{:S(2)}, u32[]{:S(2)}) collective-permute-start(bf16[2,128,256]{2,1,0:T(8,128)(2,1)S(1)} %collective-permute-done.9.refs_1_), channel_id=1, source_target_pairs={{0,64},{64,0},{128,192},{192,128},{256,320},{320,256},{384,448},{4... | collective-permute-start | bytes 393224 | tf_op jit(solution)/shard_map/ppermute | solution.py:134
  73.9 1.9 %collective-permute-start.14 = (bf16[2,128,256]{2,1,0:T(8,128)(2,1)S(1)}, bf16[2,128,256]{2,1,0:T(8,128)(2,1)S(1)}, u32[]{:S(2)}, u32[]{:S(2)}) collective-permute-start(bf16[2,128,256]{2,1,0:T(8,128)(2,1)S(1)} %collective-permute-done.13.refs_5_), channel_id=1, source_target_pairs={{0,448},{64,128},{128,64},{192,256},{256,192},{320,384},{384,320},... | collective-permute-start | bytes 393224 | tf_op jit(solution)/shard_map/ppermute | solution.py:134
  75.9 10.1 %collective-permute-done.10.refs_2_ = bf16[2,128,256]{2,1,0:T(8,128)(2,1)S(1)} collective-permute-done((bf16[2,128,256]{2,1,0:T(8,128)(2,1)S(1)}, bf16[2,128,256]{2,1,0:T(8,128)(2,1)S(1)}, u32[]{:S(2)}, u32[]{:S(2)}) %collective-permute-start.10) | collective-permute-done | bytes 131104 | tf_op jit(solution)/shard_map/ppermute | solution.py:134
  85.9 1.9 %collective-permute-start.11 = (bf16[2,128,256]{2,1,0:T(8,128)(2,1)S(1)}, bf16[2,128,256]{2,1,0:T(8,128)(2,1)S(1)}, u32[]{:S(2)}, u32[]{:S(2)}) collective-permute-start(bf16[2,128,256]{2,1,0:T(8,128)(2,1)S(1)} %collective-permute-done.10.refs_2_), channel_id=1, source_target_pairs={{0,448},{64,128},{128,64},{192,256},{256,192},{320,384},{384,320},... | collective-permute-start | bytes 393224 | tf_op jit(solution)/shard_map/ppermute | solution.py:134
  87.9 1.9 %collective-permute-start.15 = (bf16[2,128,256]{2,1,0:T(8,128)(2,1)S(1)}, bf16[2,128,256]{2,1,0:T(8,128)(2,1)}, u32[]{:S(2)}, u32[]{:S(2)}) collective-permute-start(bf16[2,128,256]{2,1,0:T(8,128)(2,1)S(1)} %collective-permute-done.14.refs_6_), channel_id=1, source_target_pairs={{0,64},{64,0},{128,192},{192,128},{256,320},{320,256},{384,448},{4... | collective-permute-start | bytes 393224 | tf_op jit(solution)/shard_map/ppermute | solution.py:134
  89.8 3.4 %collective-permute-start.7 = (bf16[2,128,384]{2,1,0:T(8,128)(2,1)S(1)}, bf16[2,128,384]{2,1,0:T(8,128)(2,1)S(1)}, u32[]{:S(2)}, u32[]{:S(2)}) collective-permute-start(bf16[2,128,384]{2,1,0:T(8,128)(2,1)S(1)} %collective-permute-done.5.refs_5_), channel_id=1, source_target_pairs={{0,64},{64,0},{128,192},{192,128},{256,320},{320,256},{384,448},{4... | collective-permute-start | bytes 589832 | tf_op jit(solution)/shard_map/ppermute | solution.py:134
  93.2 4.6 %collective-permute-start.6 = (bf16[2,128,384]{2,1,0:T(8,128)(2,1)S(1)}, bf16[2,128,384]{2,1,0:T(8,128)(2,1)S(1)}, u32[]{:S(2)}, u32[]{:S(2)}) collective-permute-start(bf16[2,128,384]{2,1,0:T(8,128)(2,1)S(1)} %collective-permute-done.2.refs_2_), channel_id=1, source_target_pairs={{0,448},{64,128},{128,64},{192,256},{256,192},{320,384},{384,320},... | collective-permute-start | bytes 589832 | tf_op jit(solution)/shard_map/ppermute | solution.py:134
  100.1 5.3 %collective-permute-done.7.right = bf16[2,128,384]{2,1,0:T(8,128)(2,1)S(1)} collective-permute-done((bf16[2,128,384]{2,1,0:T(8,128)(2,1)S(1)}, bf16[2,128,384]{2,1,0:T(8,128)(2,1)S(1)}, u32[]{:S(2)}, u32[]{:S(2)}) %collective-permute-start.7) | collective-permute-done | bytes 196640 | tf_op jit(solution)/shard_map/ppermute | solution.py:134
  108.6 15.3 %all_gather.6.sq_ref = f32[8,1,256]{2,1,0:T(1,128)S(1)} all-gather(f32[1,1,256]{2,1,0:T(1,128)S(1)} %get-tuple-element.27), channel_id=1, replica_groups=mesh['z'=8,'y'=8,'x'=4,'c'=2] {'x','c'}, dimensions={0}, use_global_device_ids=true | all-gather | bytes 9216 | tf_op jit(solution)/shard_map/all_gather | solution.py:279
  125.5 2.0 %gating.1 = (bf16[8,128,256]{2,1,0:T(8,128)(2,1)S(1)}, bf16[8,128,256]{2,1,0:T(8,128)(2,1)S(1)}) custom-call(s32[2,8]{1,0:T(2,128)S(1)} %add_and_fusion.order, s32[1]{0:T(128)} %bitcast.5.core, f32[256,384]{1,0:T(8,128)S(1)} %get-tuple-element.26.act_ref, f32[8,1,256]{2,1,0:T(1,128)S(1)} %all_gather.6.sq_ref, bf16[3,128,128]{2,1,0:T(8,128)(2,1)S(1)} %copy-done.1, ...), custom_call_target="tpu_custom_call" | custom-call | tf_op jit(solution)/shard_map/gating/pallas_call | solution.py:280
  127.5 2.1 %collective-permute-start.16 = (bf16[8,128,256]{2,1,0:T(8,128)(2,1)S(1)}, bf16[8,128,256]{2,1,0:T(8,128)(2,1)S(1)}, u32[]{:S(2)}, u32[]{:S(2)}) collective-permute-start(bf16[8,128,256]{2,1,0:T(8,128)(2,1)S(1)} %get-tuple-element.32), channel_id=1, source_target_pairs={{0,1},{1,0},{2,3},{3,2},{4,5},{5,4},{6,7},{7,6},{8,9},{9,8},{10,11... | collective-permute-start | bytes 1572872 | tf_op jit(solution)/shard_map/ppermute | solution.py:298
  129.6 1.9 collective-permute-done.16
  132.4 3.5 %all-to-all-start.2 = ((bf16[4,2,128,256]{3,2,1,0:T(8,128)(2,1)}), bf16[4,2,128,256]{3,2,1,0:T(8,128)(2,1)S(1)}, u32[]{:S(2)}, u32[]{:S(2)}) async-start(bf16[4,2,128,256]{3,2,1,0:T(8,128)(2,1)} %bitcast.10), calls=%async_computation.2 | async-start | bytes 1048576 | tf_op jit(solution)/shard_map/all_to_all | solution.py:300
  135.9 9.4 %all-to-all-done.2 = bf16[4,2,128,256]{3,2,1,0:T(8,128)(2,1)S(1)} async-done(((bf16[4,2,128,256]{3,2,1,0:T(8,128)(2,1)}), bf16[4,2,128,256]{3,2,1,0:T(8,128)(2,1)S(1)}, u32[]{:S(2)}, u32[]{:S(2)}) %all-to-all-start.2) | async-done | bytes 524320 | tf_op jit(solution)/shard_map/all_to_all | solution.py:300
  145.4 11.0 %all_to_all.26 = bf16[4,2,128,256]{3,2,1,0:T(8,128)(2,1)S(1)} all-to-all(bf16[4,2,128,256]{3,2,1,0:T(8,128)(2,1)S(1)} %broadcast_in_dim.2), channel_id=1, replica_groups=mesh['z'=8,'y'=8,'x'=4,'c'=2] {'x'}, dimensions={0} | all-to-all | bytes 1048576 | tf_op jit(solution)/shard_map/all_to_all | solution.py:22
  156.4 11.5 %ffn.1 = bf16[8,128,256]{2,1,0:T(8,128)(2,1)} custom-call(bf16[8,128,256]{2,1,0:T(8,128)(2,1)S(1)} %bitcast.29, f32[8,1,256]{2,1,0:T(1,128)} %copy-done.2, bf16[8,8,2,32,2112]{4,3,2,1,0:T(8,128)(2,1)} %bitcast.30), custom_call_target="tpu_custom_call" | custom-call | tf_op jit(solution)/shard_map/ffn/pallas_call | solution.py:304
  167.9 5.2 %all-to-all-start.4 = ((bf16[8,128,256]{2,1,0:T(8,128)(2,1)}), bf16[8,128,256]{2,1,0:T(8,128)(2,1)S(1)}, u32[]{:S(2)}, u32[]{:S(2)}) async-start(bf16[8,128,256]{2,1,0:T(8,128)(2,1)} %ffn.1), calls=%async_computation.4 | async-start | bytes 1048576 | tf_op jit(solution)/shard_map/all_to_all | solution.py:317
  173.2 2.0 %collective-permute-start.17 = (bf16[128,256]{1,0:T(8,128)(2,1)S(1)}, bf16[128,256]{1,0:T(8,128)(2,1)S(1)}, u32[]{:S(2)}, u32[]{:S(2)}) collective-permute-start(bf16[128,256]{1,0:T(8,128)(2,1)S(1)} %dynamic-slice_bitcast_fusion), channel_id=1, source_target_pairs={{0,1},{1,0},{2,3},{3,2},{4,5},{5,4},{6,7},{7,6},{8,9},{9,8},{10,11... | collective-permute-start | bytes 196616 | tf_op jit(solution)/shard_map/ppermute | solution.py:320
  176.4 6.2 %all-to-all-done.4 = bf16[8,128,256]{2,1,0:T(8,128)(2,1)S(1)} async-done(((bf16[8,128,256]{2,1,0:T(8,128)(2,1)}), bf16[8,128,256]{2,1,0:T(8,128)(2,1)S(1)}, u32[]{:S(2)}, u32[]{:S(2)}) %all-to-all-start.4) | async-done | bytes 524320 | tf_op jit(solution)/shard_map/all_to_all | solution.py:317
  (51 shorter events, 10.2 us)
Async XLA Ops:
  6.5 149.9 %all-gather.2.cloned.1.call-start = ((), (), s32[]{:S(2)}) async-start(), calls=%async_computation.5 | async-start | bytes 17965056 | tf_op jit(solution)/shard_map/all_gather | solution.py:249
  9.0 17.7 %copy-start = (bf16[3,128,128]{2,1,0:T(8,128)(2,1)}, bf16[3,128,128]{2,1,0:T(8,128)(2,1)S(1)}, u32[]{:S(2)}) copy-start(bf16[3,128,128]{2,1,0:T(8,128)(2,1)S(1)} %get-tuple-element.28.mats) | copy-start | bytes 294916
  9.0 17.7 %copy-start.2 = (f32[8,1,256]{2,1,0:T(1,128)}, f32[8,1,256]{2,1,0:T(1,128)S(1)}, u32[]{:S(2)}) copy-start(f32[8,1,256]{2,1,0:T(1,128)S(1)} %get-tuple-element.33.gain) | copy-start | bytes 24580
  9.0 17.7 %copy-start.3 = (f32[1,384]{1,0:T(1,128)}, f32[1,384]{1,0:T(1,128)S(1)}, u32[]{:S(2)}) copy-start(f32[1,384]{1,0:T(1,128)S(1)} %get-tuple-element.22.scales) | copy-start | bytes 4612
  9.0 84.1 %copy-start.5 = (f32[1,192]{1,0:T(1,128)}, f32[1,192]{1,0:T(1,128)S(1)}, u32[]{:S(2)}) copy-start(f32[1,192]{1,0:T(1,128)S(1)} %get-tuple-element.30.gain) | copy-start | bytes 2308
  26.7 71.8 %all-to-all-start = ((bf16[8,256,256]{2,1,0:T(8,128)(2,1)}), bf16[8,256,256]{2,1,0:T(8,128)(2,1)S(1)}, u32[]{:S(2)}, u32[]{:S(2)}) async-start(bf16[8,256,256]{2,1,0:T(8,128)(2,1)} %get-tuple-element.20), calls=%async_computation | async-start | bytes 2097152 | tf_op jit(solution)/shard_map/all_to_all | solution.py:252
  35.3 17.9 %collective-permute-start.3 = (bf16[1,128,384]{2,1,0:T(8,128)(2,1)S(1)}, bf16[1,128,384]{2,1,0:T(8,128)(2,1)S(1)}, u32[]{:S(2)}, u32[]{:S(2)}) collective-permute-start(bf16[1,128,384]{2,1,0:T(8,128)(2,1)S(1)} %bitcast.34), channel_id=1, source_target_pairs={{0,448},{64,128},{128,64},{192,256},{256,192},{320,384},{384,320},... | collective-permute-start | bytes 294920 | tf_op jit(solution)/shard_map/ppermute | solution.py:130
  46.0 9.2 %collective-permute-start = (bf16[1,128,384]{2,1,0:T(8,128)(2,1)S(1)}, bf16[1,128,384]{2,1,0:T(8,128)(2,1)S(1)}, u32[]{:S(2)}, u32[]{:S(2)}) collective-permute-start(bf16[1,128,384]{2,1,0:T(8,128)(2,1)S(1)} %bitcast.32), channel_id=1, source_target_pairs={{0,64},{64,0},{128,192},{192,128},{256,320},{320,256},{384,448},{4... | collective-permute-start | bytes 294920 | tf_op jit(solution)/shard_map/ppermute | solution.py:130
  47.9 11.9 %collective-permute-start.8 = (bf16[1,128,256]{2,1,0:T(8,128)(2,1)S(1)}, bf16[1,128,256]{2,1,0:T(8,128)(2,1)S(1)}, u32[]{:S(2)}, u32[]{:S(2)}) collective-permute-start(bf16[1,128,256]{2,1,0:T(8,128)(2,1)S(1)} %bitcast.38), channel_id=1, source_target_pairs={{0,64},{64,0},{128,192},{192,128},{256,320},{320,256},{384,448},{4... | collective-permute-start | bytes 196616 | tf_op jit(solution)/shard_map/ppermute | solution.py:130
  51.3 10.5 %collective-permute-start.12 = (bf16[1,128,256]{2,1,0:T(8,128)(2,1)S(1)}, bf16[1,128,256]{2,1,0:T(8,128)(2,1)S(1)}, u32[]{:S(2)}, u32[]{:S(2)}) collective-permute-start(bf16[1,128,256]{2,1,0:T(8,128)(2,1)S(1)} %bitcast.36), channel_id=1, source_target_pairs={{0,448},{64,128},{128,64},{192,256},{256,192},{320,384},{384,320},... | collective-permute-start | bytes 196616 | tf_op jit(solution)/shard_map/ppermute | solution.py:130
  53.3 10.7 %collective-permute-start.4 = (bf16[2,128,384]{2,1,0:T(8,128)(2,1)S(1)}, bf16[2,128,384]{2,1,0:T(8,128)(2,1)S(1)}, u32[]{:S(2)}, u32[]{:S(2)}) collective-permute-start(bf16[2,128,384]{2,1,0:T(8,128)(2,1)S(1)} %pad_maximum_fusion.1.refs_3_), channel_id=1, source_target_pairs={{0,64},{64,0},{128,192},{192,128},{256,320},{320,256},{384,448},{4... | collective-permute-start | bytes 589832 | tf_op jit(solution)/shard_map/ppermute | solution.py:134
  55.2 13.3 %collective-permute-start.1 = (bf16[2,128,384]{2,1,0:T(8,128)(2,1)S(1)}, bf16[2,128,384]{2,1,0:T(8,128)(2,1)S(1)}, u32[]{:S(2)}, u32[]{:S(2)}) collective-permute-start(bf16[2,128,384]{2,1,0:T(8,128)(2,1)S(1)} %pad_maximum_fusion.refs_0_), channel_id=1, source_target_pairs={{0,448},{64,128},{128,64},{192,256},{256,192},{320,384},{384,320},... | collective-permute-start | bytes 589832 | tf_op jit(solution)/shard_map/ppermute | solution.py:134
  59.9 10.7 %collective-permute-start.9 = (bf16[2,128,256]{2,1,0:T(8,128)(2,1)S(1)}, bf16[2,128,256]{2,1,0:T(8,128)(2,1)S(1)}, u32[]{:S(2)}, u32[]{:S(2)}) collective-permute-start(bf16[2,128,256]{2,1,0:T(8,128)(2,1)S(1)} %pad_maximum_fusion.2.refs_0_), channel_id=1, source_target_pairs={{0,448},{64,128},{128,64},{192,256},{256,192},{320,384},{384,320},... | collective-permute-start | bytes 393224 | tf_op jit(solution)/shard_map/ppermute | solution.py:134
  61.8 12.1 %collective-permute-start.13 = (bf16[2,128,256]{2,1,0:T(8,128)(2,1)S(1)}, bf16[2,128,256]{2,1,0:T(8,128)(2,1)S(1)}, u32[]{:S(2)}, u32[]{:S(2)}) collective-permute-start(bf16[2,128,256]{2,1,0:T(8,128)(2,1)S(1)} %pad_maximum_fusion.3.refs_4_), channel_id=1, source_target_pairs={{0,64},{64,0},{128,192},{192,128},{256,320},{320,256},{384,448},{4... | collective-permute-start | bytes 393224 | tf_op jit(solution)/shard_map/ppermute | solution.py:134
  64.0 25.8 %collective-permute-start.5 = (bf16[2,128,384]{2,1,0:T(8,128)(2,1)S(1)}, bf16[2,128,384]{2,1,0:T(8,128)(2,1)S(1)}, u32[]{:S(2)}, u32[]{:S(2)}) collective-permute-start(bf16[2,128,384]{2,1,0:T(8,128)(2,1)S(1)} %collective-permute-done.4.refs_4_), channel_id=1, source_target_pairs={{0,448},{64,128},{128,64},{192,256},{256,192},{320,384},{384,320},... | collective-permute-start | bytes 589832 | tf_op jit(solution)/shard_map/ppermute | solution.py:134
  68.6 24.6 %collective-permute-start.2 = (bf16[2,128,384]{2,1,0:T(8,128)(2,1)S(1)}, bf16[2,128,384]{2,1,0:T(8,128)(2,1)S(1)}, u32[]{:S(2)}, u32[]{:S(2)}) collective-permute-start(bf16[2,128,384]{2,1,0:T(8,128)(2,1)S(1)} %collective-permute-done.1.refs_1_), channel_id=1, source_target_pairs={{0,64},{64,0},{128,192},{192,128},{256,320},{320,256},{384,448},{4... | collective-permute-start | bytes 589832 | tf_op jit(solution)/shard_map/ppermute | solution.py:134
  70.5 15.4 %collective-permute-start.10 = (bf16[2,128,256]{2,1,0:T(8,128)(2,1)S(1)}, bf16[2,128,256]{2,1,0:T(8,128)(2,1)S(1)}, u32[]{:S(2)}, u32[]{:S(2)}) collective-permute-start(bf16[2,128,256]{2,1,0:T(8,128)(2,1)S(1)} %collective-permute-done.9.refs_1_), channel_id=1, source_target_pairs={{0,64},{64,0},{128,192},{192,128},{256,320},{320,256},{384,448},{4... | collective-permute-start | bytes 393224 | tf_op jit(solution)/shard_map/ppermute | solution.py:134
  73.9 13.9 %collective-permute-start.14 = (bf16[2,128,256]{2,1,0:T(8,128)(2,1)S(1)}, bf16[2,128,256]{2,1,0:T(8,128)(2,1)S(1)}, u32[]{:S(2)}, u32[]{:S(2)}) collective-permute-start(bf16[2,128,256]{2,1,0:T(8,128)(2,1)S(1)} %collective-permute-done.13.refs_5_), channel_id=1, source_target_pairs={{0,448},{64,128},{128,64},{192,256},{256,192},{320,384},{384,320},... | collective-permute-start | bytes 393224 | tf_op jit(solution)/shard_map/ppermute | solution.py:134
  85.9 38.0 %collective-permute-start.11 = (bf16[2,128,256]{2,1,0:T(8,128)(2,1)S(1)}, bf16[2,128,256]{2,1,0:T(8,128)(2,1)S(1)}, u32[]{:S(2)}, u32[]{:S(2)}) collective-permute-start(bf16[2,128,256]{2,1,0:T(8,128)(2,1)S(1)} %collective-permute-done.10.refs_2_), channel_id=1, source_target_pairs={{0,448},{64,128},{128,64},{192,256},{256,192},{320,384},{384,320},... | collective-permute-start | bytes 393224 | tf_op jit(solution)/shard_map/ppermute | solution.py:134
  87.9 36.0 %collective-permute-start.15 = (bf16[2,128,256]{2,1,0:T(8,128)(2,1)S(1)}, bf16[2,128,256]{2,1,0:T(8,128)(2,1)}, u32[]{:S(2)}, u32[]{:S(2)}) collective-permute-start(bf16[2,128,256]{2,1,0:T(8,128)(2,1)S(1)} %collective-permute-done.14.refs_6_), channel_id=1, source_target_pairs={{0,64},{64,0},{128,192},{192,128},{256,320},{320,256},{384,448},{4... | collective-permute-start | bytes 393224 | tf_op jit(solution)/shard_map/ppermute | solution.py:134
  89.8 15.6 %collective-permute-start.7 = (bf16[2,128,384]{2,1,0:T(8,128)(2,1)S(1)}, bf16[2,128,384]{2,1,0:T(8,128)(2,1)S(1)}, u32[]{:S(2)}, u32[]{:S(2)}) collective-permute-start(bf16[2,128,384]{2,1,0:T(8,128)(2,1)S(1)} %collective-permute-done.5.refs_5_), channel_id=1, source_target_pairs={{0,64},{64,0},{128,192},{192,128},{256,320},{320,256},{384,448},{4... | collective-permute-start | bytes 589832 | tf_op jit(solution)/shard_map/ppermute | solution.py:134
  93.2 13.3 %collective-permute-start.6 = (bf16[2,128,384]{2,1,0:T(8,128)(2,1)S(1)}, bf16[2,128,384]{2,1,0:T(8,128)(2,1)S(1)}, u32[]{:S(2)}, u32[]{:S(2)}) collective-permute-start(bf16[2,128,384]{2,1,0:T(8,128)(2,1)S(1)} %collective-permute-done.2.refs_2_), channel_id=1, source_target_pairs={{0,448},{64,128},{128,64},{192,256},{256,192},{320,384},{384,320},... | collective-permute-start | bytes 589832 | tf_op jit(solution)/shard_map/ppermute | solution.py:134
  106.5 0.7 copy-start.4
  123.9 0.9 copy-start.1
  124.8 0.7 copy-start.6
  127.5 4.0 %collective-permute-start.16 = (bf16[8,128,256]{2,1,0:T(8,128)(2,1)S(1)}, bf16[8,128,256]{2,1,0:T(8,128)(2,1)S(1)}, u32[]{:S(2)}, u32[]{:S(2)}) collective-permute-start(bf16[8,128,256]{2,1,0:T(8,128)(2,1)S(1)} %get-tuple-element.32), channel_id=1, source_target_pairs={{0,1},{1,0},{2,3},{3,2},{4,5},{5,4},{6,7},{7,6},{8,9},{9,8},{10,11... | collective-permute-start | bytes 1572872 | tf_op jit(solution)/shard_map/ppermute | solution.py:298
  132.4 12.9 %all-to-all-start.2 = ((bf16[4,2,128,256]{3,2,1,0:T(8,128)(2,1)}), bf16[4,2,128,256]{3,2,1,0:T(8,128)(2,1)S(1)}, u32[]{:S(2)}, u32[]{:S(2)}) async-start(bf16[4,2,128,256]{3,2,1,0:T(8,128)(2,1)} %bitcast.10), calls=%async_computation.2 | async-start | bytes 1048576 | tf_op jit(solution)/shard_map/all_to_all | solution.py:300
  167.9 14.6 %all-to-all-start.4 = ((bf16[8,128,256]{2,1,0:T(8,128)(2,1)}), bf16[8,128,256]{2,1,0:T(8,128)(2,1)S(1)}, u32[]{:S(2)}, u32[]{:S(2)}) async-start(bf16[8,128,256]{2,1,0:T(8,128)(2,1)} %ffn.1), calls=%async_computation.4 | async-start | bytes 1048576 | tf_op jit(solution)/shard_map/all_to_all | solution.py:317
  173.2 3.1 %collective-permute-start.17 = (bf16[128,256]{1,0:T(8,128)(2,1)S(1)}, bf16[128,256]{1,0:T(8,128)(2,1)S(1)}, u32[]{:S(2)}, u32[]{:S(2)}) collective-permute-start(bf16[128,256]{1,0:T(8,128)(2,1)S(1)} %dynamic-slice_bitcast_fusion), channel_id=1, source_target_pairs={{0,1},{1,0},{2,3},{3,2},{4,5},{5,4},{6,7},{7,6},{8,9},{9,8},{10,11... | collective-permute-start | bytes 196616 | tf_op jit(solution)/shard_map/ppermute | solution.py:320
Sparse Core Ops, SparseCore 0:
  10.5 120.7 all-gather.1

commit v6 on v5

--- a/solution.py
+++ b/solution.py
@@ -31,17 +31,21 @@
     return jnp.sum(jnp.where(same, row.reshape(1, n), 0.0), axis=1, keepdims=True)
 
 
-def pack_kernel(conv, blend, emis, emis_s, valve, valve_s, raising, raising_s, low, low_s, seq, *refs):
-    own, ffn, seqs, scales = refs[7:11]
-    scales[:, 0:192] = refs[0][...].reshape(1, 192)
-    scales[:, 192:384] = refs[1][...].reshape(1, 192)
-    for here, there in zip(refs[2:7], refs[11:]):
-        there[...] = here[...]
+def pack_kernel(conv, blend, emis, emis_s, own):
     emission = emis[...] * upright(emis_s[...], 32)
     packed = jnp.concatenate([conv[...], blend[...], emission, jnp.zeros((32, 64), F32)], axis=1)
     packed = packed.astype(BF)
     for k in range(8):
         own[k] = packed
+
+
+def pack_later_kernel(valve, valve_s, raising, raising_s, low, low_s, seq, *refs):
+    ffn, seqs, scales = refs[7:10]
+    scales[:, 0:192] = refs[0][...].reshape(1, 192)
+    scales[:, 192:384] = refs[1][...].reshape(1, 192)
+    for here, there in zip(refs[2:7], refs[10:]):
+        there[...] = here[...]
+    for k in range(8):
         seqs[k] = seq[...]
     gate = valve[...] * valve_s[...].reshape(1, 704)
     up = raising[...] * raising_s[...].reshape(1, 704)
@@ -116,7 +120,7 @@
     here = core[0]
     mine, other = gated[here], gated[1 - here]
     for block, half, ref, k in spread(order, pieces[:4], pieces[4:]):
-        piece = ref[k, :, 0:192]
+        piece = ref[k, :, 384:576]
         cols = pl.ds(128 * half, 128)
         part = lax.dot_general(mine, piece, NT, preferred_element_type=F32)
         kept[block, :, cols] = part.astype(BF)
@@ -149,13 +153,13 @@
         at = (k, slice(None), slice(None), slice(None), cols)
         return pltpu.make_async_copy(w_ref.at[at], w.at[at], sems.at[n])
 
-    for n in range(3):
+    for n in range(8):
         fetch(n).start()
 
     def arrive(n):
         fetch(n).wait()
-        if n + 3 < 16:
-            fetch(n + 3).start()
+        if n < 8:
+            fetch(n + 8).start()
 
     total = jnp.zeros((128, 1), F32)
     for k in range(8):
@@ -180,7 +184,9 @@
         u = acc[c, :, 1344:1408]
         hid[c, :, 640:704] = (g * jax.nn.sigmoid(g) * u).astype(BF)
     for k in range(8):
-        arrive(8 + k)
+        if k % 4 == 0:
+            for n in range(8 + k, 12 + k):
+                arrive(n)
         part = jnp.zeros((128, 256), F32)
         for c in range(2):
             piece = w[k, :, c, :, 1408:2112].reshape(256, 704)
@@ -210,12 +216,18 @@
 ):
     z, x, c = lax.axis_index("z"), lax.axis_index("x"), lax.axis_index("c")
     swap = [(0, 1), (1, 0)]
-    own, ffn_own, seqs, scales, gain, latter_gain, mats, offs, blend_gain = pl.pallas_call(
+    own = pl.pallas_call(
         pack_kernel,
-        in_specs=[VM] * 18,
-        out_specs=[VM] * 9,
+        in_specs=[VM] * 4,
+        out_specs=VM,
+        out_shape=jax.ShapeDtypeStruct((8, 32, 640), BF),
+        name="pack",
+    )(conveyor_matrix, blend_value_matrix, branch_emission_matrix.T, emission_rescalers)
+    ffn_own, seqs, scales, gain, latter_gain, mats, offs, blend_gain = pl.pallas_call(
+        pack_later_kernel,
+        in_specs=[VM] * 14,
+        out_specs=[VM] * 8,
         out_shape=[
-            jax.ShapeDtypeStruct((8, 32, 640), BF),
             jax.ShapeDtypeStruct((32, 2112), BF),
             jax.ShapeDtypeStruct((8, 256, 256), BF),
             pltpu.VMEM((1, 384), F32),
@@ -225,12 +237,8 @@
             pltpu.VMEM((3, 128), F32),
             pltpu.VMEM((1, 192), F32),
         ],
-        name="pack",
+        name="pack_later",
     )(
-        conveyor_matrix,
-        blend_value_matrix,
-        branch_emission_matrix.T,
-        emission_rescalers,
         valve_matrix,
         valve_rescalers,
         raising_matrix,
@@ -250,13 +258,9 @@
 
     first = lax.all_to_all(own, "y", 0, 0, tiled=True)
     rows = lax.all_to_all(seqs, TP, 0, 0, tiled=True)
-    streams = {}
-    for name, cols in (("cb", slice(0, 384)), ("em", slice(384, 640))):
-        for flip in range(2):
-            half = first[4 * flip : 4 * flip + 4, :, cols].reshape(1, 128, -1)
-            streams[name, flip] = [vmem(p) for p in exchange(half, flip)]
-    left, right = streams["cb", 0], streams["cb", 1]
-    pieces = streams["em", 0] + streams["em", 1]
+    left = [vmem(p) for p in exchange(first[:4].reshape(1, 128, 640), 0)]
+    right = [vmem(p) for p in exchange(first[4:].reshape(1, 128, 640), 1)]
+    pieces = left + right
     order = blocks(z)
     near = vmem(rows)
 

time: 191 us -> 172 us (0.901)
  starting transfers between devices: 73.4 us -> 57.9 us
  local copies, waits for them, and re-layouts: 2.35 us -> 0.07 us
    ppermute x12 -> x6, starting transfers between devices: 34.1 us -> 21.9 us  [exchange(): batch = lax.ppermute(batch, 'z', turn)]
    ppermute x4 -> x2, starting transfers between devices: 17.9 us -> 14.6 us  [exchange(): got = lax.ppermute(own, 'z', to_pair)]
    unnamed x14 -> x2, local copies, waits for them, and re-layouts: 2.28 us -> 0.01 us
    pallas_call x1, Pallas kernels: 11.5 us -> 9.36 us  [on_device(): pl.pallas_call(ffn_kernel, in_specs=[VM, VM, pl.BlockSpec(memory_space=pl...]
    pallas_call x1 -> x2, Pallas kernels: 2.48 us -> 3.94 us  [the longest x1 2.31 us: on_device(): pl.pallas_call(pack_later_kernel, in_specs=[VM] * 14, out_specs=[VM] * 8,...]
    ppermute x12 -> x6, waiting for transfers between devices: 16.5 us -> 15.7 us  [exchange(): batch = lax.ppermute(batch, 'z', turn)]
  transfers between devices with their start and end apart: 22 -> 14, of which waited for: 7 -> 8; matrix products, arithmetic and copies ran while one was open for 1% -> 1% of each run, Pallas kernels for 3% -> 4%
where the time goes in v6:
time: 172 us; the launch traced here: 171 us
  starting transfers between devices  57.9 us (34%)
  blocking collectives  43.7 us (25%)
  waiting for transfers between devices  34.3 us (20%)
  Pallas kernels  18.9 us (11%)
  between operations  13.6 us (8%)
  other arithmetic  2.65 us (2%)
    ppermute x6, starting transfers between devices, exchange(): batch = lax.ppermute(batch, 'z', turn)  21.9 us
    all_to_all x1, blocking collectives, on_device(): first = lax.all_to_all(own, 'y', 0, 0, tiled=True)  17.6 us
    ppermute x6, waiting for transfers between devices, exchange(): batch = lax.ppermute(batch, 'z', turn)  15.7 us
    all_gather x1, blocking collectives, on_device(): all_sq = lax.all_gather(own_sq, TP, axis=0, tiled=True)  15 us
    ppermute x2, starting transfers between devices, exchange(): got = lax.ppermute(own, 'z', to_pair)  14.6 us
    all_to_all x1, blocking collectives, from_everyone(): return lax.all_to_all(copies, axis, split_axis=0, concat_axis=0, tiled=True)  11 us
    all_to_all x1, waiting for transfers between devices, on_device(): shares = lax.all_to_all(both, 'x', 0, 0, tiled=True)  9.39 us
    pallas_call x1, Pallas kernels, on_device(): pl.pallas_call(ffn_kernel, in_specs=[VM, VM, pl.BlockSpec(memory_space=pl...  9.36 us
  transfers between devices with their start and end apart: 14, of which 8 were waited for; matrix products, arithmetic and copies ran while one was open for 1% of the time, Pallas kernels for 4%

profile of v6, /device:TPU:1, one launch (start us, length us, event | category | flops | bytes accessed | tf_op | source)
XLA Modules:
  0.0 171.0 jit_solution(13711637442976593309)
XLA Ops:
  6.5 2.3 %pack_later.1 = (bf16[32,2112]{1,0:T(8,128)(2,1)}, bf16[8,256,256]{2,1,0:T(8,128)(2,1)}, f32[1,384]{1,0:T(1,128)S(1)}, f32[8,1,256]{2,1,0:T(1,128)S(1)}, f32[8,1...) custom-call(f32[32,704]{1,0:T(8,128)} %valve.1, ...), custom_call_target="tpu_custom_call" | custom-call | tf_op jit(solution)/shard_map/pack_later/pallas_call | solution.py:226
  8.9 1.6 pack.1
  10.5 17.6 %all_to_all.25 = bf16[8,32,640]{2,1,0:T(8,128)(2,1)S(1)} all-to-all(bf16[8,32,640]{2,1,0:T(8,128)(2,1)} %pack.1), channel_id=1, replica_groups=mesh['z'=8,'y'=8,'x'=4,'c'=2] {'y'}, dimensions={0} | all-to-all | bytes 655360 | tf_op jit(solution)/shard_map/all_to_all | solution.py:259
  28.2 5.8 %collective-permute-start = (bf16[1,128,640]{2,1,0:T(8,128)(2,1)S(1)}, bf16[1,128,640]{2,1,0:T(8,128)(2,1)S(1)}, u32[]{:S(2)}, u32[]{:S(2)}) collective-permute-start(bf16[1,128,640]{2,1,0:T(8,128)(2,1)S(1)} %bitcast.32), channel_id=1, source_target_pairs={{0,64},{64,0},{128,192},{192,128},{256,320},{320,256},{384,448},{4... | collective-permute-start | bytes 491528 | tf_op jit(solution)/shard_map/ppermute | solution.py:134
  33.9 8.8 %collective-permute-start.3 = (bf16[1,128,640]{2,1,0:T(8,128)(2,1)S(1)}, bf16[1,128,640]{2,1,0:T(8,128)(2,1)S(1)}, u32[]{:S(2)}, u32[]{:S(2)}) collective-permute-start(bf16[1,128,640]{2,1,0:T(8,128)(2,1)S(1)} %bitcast.30), channel_id=1, source_target_pairs={{0,448},{64,128},{128,64},{192,256},{256,192},{320,384},{384,320},... | collective-permute-start | bytes 491528 | tf_op jit(solution)/shard_map/ppermute | solution.py:134
  42.8 4.2 %collective-permute-start.1 = (bf16[2,128,640]{2,1,0:T(8,128)(2,1)S(1)}, bf16[2,128,640]{2,1,0:T(8,128)(2,1)S(1)}, u32[]{:S(2)}, u32[]{:S(2)}) collective-permute-start(bf16[2,128,640]{2,1,0:T(8,128)(2,1)S(1)} %pad_maximum_fusion.refs_0_), channel_id=1, source_target_pairs={{0,448},{64,128},{128,64},{192,256},{256,192},{320,384},{384,320},... | collective-permute-start | bytes 983048 | tf_op jit(solution)/shard_map/ppermute | solution.py:138
  47.2 1.9 %collective-permute-start.4 = (bf16[2,128,640]{2,1,0:T(8,128)(2,1)S(1)}, bf16[2,128,640]{2,1,0:T(8,128)(2,1)S(1)}, u32[]{:S(2)}, u32[]{:S(2)}) collective-permute-start(bf16[2,128,640]{2,1,0:T(8,128)(2,1)S(1)} %pad_maximum_fusion.1.refs_3_.refs_4_), channel_id=1, source_target_pairs={{0,64},{64,0},{128,192},{192,128},{256,320},{320,256},{384,448},{4... | collective-permute-start | bytes 983048 | tf_op jit(solution)/shard_map/ppermute | solution.py:138
  49.1 8.5 %all-to-all-start = ((bf16[8,256,256]{2,1,0:T(8,128)(2,1)}), bf16[8,256,256]{2,1,0:T(8,128)(2,1)S(1)}, u32[]{:S(2)}, u32[]{:S(2)}) async-start(bf16[8,256,256]{2,1,0:T(8,128)(2,1)} %get-tuple-element.19), calls=%async_computation | async-start | bytes 2097152 | tf_op jit(solution)/shard_map/all_to_all | solution.py:260
  57.6 3.6 %collective-permute-start.2 = (bf16[2,128,640]{2,1,0:T(8,128)(2,1)S(1)}, bf16[2,128,640]{2,1,0:T(8,128)(2,1)S(1)}, u32[]{:S(2)}, u32[]{:S(2)}) collective-permute-start(bf16[2,128,640]{2,1,0:T(8,128)(2,1)S(1)} %collective-permute-done.1.refs_1_), channel_id=1, source_target_pairs={{0,64},{64,0},{128,192},{192,128},{256,320},{320,256},{384,448},{4... | collective-permute-start | bytes 983048 | tf_op jit(solution)/shard_map/ppermute | solution.py:138
  61.2 5.1 %collective-permute-start.5 = (bf16[2,128,640]{2,1,0:T(8,128)(2,1)S(1)}, bf16[2,128,640]{2,1,0:T(8,128)(2,1)S(1)}, u32[]{:S(2)}, u32[]{:S(2)}) collective-permute-start(bf16[2,128,640]{2,1,0:T(8,128)(2,1)S(1)} %collective-permute-done.4.refs_4_.refs_5_), channel_id=1, source_target_pairs={{0,448},{64,128},{128,64},{192,256},{256,192},{320,384},{384,320},... | collective-permute-start | bytes 983048 | tf_op jit(solution)/shard_map/ppermute | solution.py:138
  66.3 2.2 %collective-permute-done.2.refs_2_ = bf16[2,128,640]{2,1,0:T(8,128)(2,1)S(1)} collective-permute-done((bf16[2,128,640]{2,1,0:T(8,128)(2,1)S(1)}, bf16[2,128,640]{2,1,0:T(8,128)(2,1)S(1)}, u32[]{:S(2)}, u32[]{:S(2)}) %collective-permute-start.2) | collective-permute-done | bytes 327712 | tf_op jit(solution)/shard_map/ppermute | solution.py:138
  68.5 5.2 %collective-permute-start.6 = (bf16[2,128,640]{2,1,0:T(8,128)(2,1)S(1)}, bf16[2,128,640]{2,1,0:T(8,128)(2,1)S(1)}, u32[]{:S(2)}, u32[]{:S(2)}) collective-permute-start(bf16[2,128,640]{2,1,0:T(8,128)(2,1)S(1)} %collective-permute-done.2.refs_2_), channel_id=1, source_target_pairs={{0,448},{64,128},{128,64},{192,256},{256,192},{320,384},{384,320},... | collective-permute-start | bytes 983048 | tf_op jit(solution)/shard_map/ppermute | solution.py:138
  74.2 1.9 %collective-permute-start.7 = (bf16[2,128,640]{2,1,0:T(8,128)(2,1)S(1)}, bf16[2,128,640]{2,1,0:T(8,128)(2,1)}, u32[]{:S(2)}, u32[]{:S(2)}) collective-permute-start(bf16[2,128,640]{2,1,0:T(8,128)(2,1)S(1)} %collective-permute-done.5.refs_5_.refs_6_), channel_id=1, source_target_pairs={{0,64},{64,0},{128,192},{192,128},{256,320},{320,256},{384,448},{4... | collective-permute-start | bytes 983048 | tf_op jit(solution)/shard_map/ppermute | solution.py:138
  76.1 0.7 add_and_fusion.order
  76.8 1.6 early.1
  78.5 9.8 %collective-permute-done.6.left.refs_3_ = bf16[2,128,640]{2,1,0:T(8,128)(2,1)S(1)} collective-permute-done((bf16[2,128,640]{2,1,0:T(8,128)(2,1)S(1)}, bf16[2,128,640]{2,1,0:T(8,128)(2,1)S(1)}, u32[]{:S(2)}, u32[]{:S(2)}) %collective-permute-start.6) | collective-permute-done | bytes 327712 | tf_op jit(solution)/shard_map/ppermute | solution.py:138
  88.2 3.2 %collective-permute-done.7.right.refs_7_ = bf16[2,128,640]{2,1,0:T(8,128)(2,1)} collective-permute-done((bf16[2,128,640]{2,1,0:T(8,128)(2,1)S(1)}, bf16[2,128,640]{2,1,0:T(8,128)(2,1)}, u32[]{:S(2)}, u32[]{:S(2)}) %collective-permute-start.7) | collective-permute-done | bytes 327712 | tf_op jit(solution)/shard_map/ppermute | solution.py:138
  91.4 1.9 %project.1 = (f32[256,384]{1,0:T(8,128)S(1)}, f32[1,1,256]{2,1,0:T(1,128)S(1)}) custom-call(s32[2,8]{1,0:T(2,128)S(1)} %add_and_fusion.order, bf16[8,256,256]{2,1,0:T(8,128)(2,1)S(1)} %all-to-all-done.x_ref, f32[8,1,256]{2,1,0:T(1,128)S(1)} %get-tuple-element.20.gain, f32[1,384]{1,0:T(1,128)S(1)} %get-tuple-element.21.scales, ...), custom_call_target="tpu_custom_call" | custom-call | tf_op jit(solution)/shard_map/project/pallas_call | solution.py:275
  93.3 15.0 %all_gather.6.sq_ref = f32[8,1,256]{2,1,0:T(1,128)S(1)} all-gather(f32[1,1,256]{2,1,0:T(1,128)S(1)} %get-tuple-element.25), channel_id=1, replica_groups=mesh['z'=8,'y'=8,'x'=4,'c'=2] {'x','c'}, dimensions={0}, use_global_device_ids=true | all-gather | bytes 9216 | tf_op jit(solution)/shard_map/all_gather | solution.py:283
  108.4 2.1 %gating.1 = (bf16[8,128,256]{2,1,0:T(8,128)(2,1)S(1)}, bf16[8,128,256]{2,1,0:T(8,128)(2,1)S(1)}) custom-call(s32[2,8]{1,0:T(2,128)S(1)} %add_and_fusion.order, s32[1]{0:T(128)} %bitcast.4.core, f32[256,384]{1,0:T(8,128)S(1)} %get-tuple-element.24.act_ref, f32[8,1,256]{2,1,0:T(1,128)S(1)} %all_gather.6.sq_ref, ...), custom_call_target="tpu_custom_call" | custom-call | tf_op jit(solution)/shard_map/gating/pallas_call | solution.py:284
  110.5 2.1 %collective-permute-start.8 = (bf16[8,128,256]{2,1,0:T(8,128)(2,1)S(1)}, bf16[8,128,256]{2,1,0:T(8,128)(2,1)S(1)}, u32[]{:S(2)}, u32[]{:S(2)}) collective-permute-start(bf16[8,128,256]{2,1,0:T(8,128)(2,1)S(1)} %get-tuple-element.30), channel_id=1, source_target_pairs={{0,1},{1,0},{2,3},{3,2},{4,5},{5,4},{6,7},{7,6},{8,9},{9,8},{10,11... | collective-permute-start | bytes 1572872 | tf_op jit(solution)/shard_map/ppermute | solution.py:302
  112.6 1.9 %collective-permute-done.8 = bf16[8,128,256]{2,1,0:T(8,128)(2,1)S(1)} collective-permute-done((bf16[8,128,256]{2,1,0:T(8,128)(2,1)S(1)}, bf16[8,128,256]{2,1,0:T(8,128)(2,1)S(1)}, u32[]{:S(2)}, u32[]{:S(2)}) %collective-permute-start.8) | collective-permute-done | bytes 524320 | tf_op jit(solution)/shard_map/ppermute | solution.py:302
  114.5 0.9 add_convert_fusion
  115.4 3.5 %all-to-all-start.2 = ((bf16[4,2,128,256]{3,2,1,0:T(8,128)(2,1)}), bf16[4,2,128,256]{3,2,1,0:T(8,128)(2,1)S(1)}, u32[]{:S(2)}, u32[]{:S(2)}) async-start(bf16[4,2,128,256]{3,2,1,0:T(8,128)(2,1)} %bitcast.8), calls=%async_computation.2 | async-start | bytes 1048576 | tf_op jit(solution)/shard_map/all_to_all | solution.py:304
  118.9 9.4 %all-to-all-done.2 = bf16[4,2,128,256]{3,2,1,0:T(8,128)(2,1)S(1)} async-done(((bf16[4,2,128,256]{3,2,1,0:T(8,128)(2,1)}), bf16[4,2,128,256]{3,2,1,0:T(8,128)(2,1)S(1)}, u32[]{:S(2)}, u32[]{:S(2)}) %all-to-all-start.2) | async-done | bytes 524320 | tf_op jit(solution)/shard_map/all_to_all | solution.py:304
  128.4 11.0 %all_to_all.26 = bf16[4,2,128,256]{3,2,1,0:T(8,128)(2,1)S(1)} all-to-all(bf16[4,2,128,256]{3,2,1,0:T(8,128)(2,1)S(1)} %broadcast_in_dim.2), channel_id=1, replica_groups=mesh['z'=8,'y'=8,'x'=4,'c'=2] {'x'}, dimensions={0} | all-to-all | bytes 1048576 | tf_op jit(solution)/shard_map/all_to_all | solution.py:22
  139.4 9.4 %ffn.1 = bf16[8,128,256]{2,1,0:T(8,128)(2,1)} custom-call(bf16[8,128,256]{2,1,0:T(8,128)(2,1)S(1)} %bitcast.27, f32[8,1,256]{2,1,0:T(1,128)} %copy-done, bf16[8,8,2,32,2112]{4,3,2,1,0:T(8,128)(2,1)} %bitcast.28), custom_call_target="tpu_custom_call" | custom-call | tf_op jit(solution)/shard_map/ffn/pallas_call | solution.py:308
  148.8 5.3 %all-to-all-start.4 = ((bf16[8,128,256]{2,1,0:T(8,128)(2,1)}), bf16[8,128,256]{2,1,0:T(8,128)(2,1)S(1)}, u32[]{:S(2)}, u32[]{:S(2)}) async-start(bf16[8,128,256]{2,1,0:T(8,128)(2,1)} %ffn.1), calls=%async_computation.4 | async-start | bytes 1048576 | tf_op jit(solution)/shard_map/all_to_all | solution.py:321
  154.0 2.0 %collective-permute-start.9 = (bf16[128,256]{1,0:T(8,128)(2,1)S(1)}, bf16[128,256]{1,0:T(8,128)(2,1)S(1)}, u32[]{:S(2)}, u32[]{:S(2)}) collective-permute-start(bf16[128,256]{1,0:T(8,128)(2,1)S(1)} %dynamic-slice_bitcast_fusion), channel_id=1, source_target_pairs={{0,1},{1,0},{2,3},{3,2},{4,5},{5,4},{6,7},{7,6},{8,9},{9,8},{10,11... | collective-permute-start | bytes 196616 | tf_op jit(solution)/shard_map/ppermute | solution.py:324
  156.1 1.1 collective-permute-done.9
  157.2 6.2 %all-to-all-done.4 = bf16[8,128,256]{2,1,0:T(8,128)(2,1)S(1)} async-done(((bf16[8,128,256]{2,1,0:T(8,128)(2,1)}), bf16[8,128,256]{2,1,0:T(8,128)(2,1)S(1)}, u32[]{:S(2)}, u32[]{:S(2)}) %all-to-all-start.4) | async-done | bytes 524320 | tf_op jit(solution)/shard_map/all_to_all | solution.py:321
  163.5 0.7 add_convert_fusion.1
  (21 shorter events, 0.9 us)
Async XLA Ops:
  6.5 132.9 %all-gather.2.cloned.1.call-start = ((), (), s32[]{:S(2)}) async-start(), calls=%async_computation.5 | async-start | bytes 17965056 | tf_op jit(solution)/shard_map/all_gather | solution.py:257
  8.8 40.2 %copy-start = (f32[8,1,256]{2,1,0:T(1,128)}, f32[8,1,256]{2,1,0:T(1,128)S(1)}, u32[]{:S(2)}) copy-start(f32[8,1,256]{2,1,0:T(1,128)S(1)} %get-tuple-element.31.gain) | copy-start | bytes 24580
  28.2 14.6 %collective-permute-start = (bf16[1,128,640]{2,1,0:T(8,128)(2,1)S(1)}, bf16[1,128,640]{2,1,0:T(8,128)(2,1)S(1)}, u32[]{:S(2)}, u32[]{:S(2)}) collective-permute-start(bf16[1,128,640]{2,1,0:T(8,128)(2,1)S(1)} %bitcast.32), channel_id=1, source_target_pairs={{0,64},{64,0},{128,192},{192,128},{256,320},{320,256},{384,448},{4... | collective-permute-start | bytes 491528 | tf_op jit(solution)/shard_map/ppermute | solution.py:134
  33.9 13.2 %collective-permute-start.3 = (bf16[1,128,640]{2,1,0:T(8,128)(2,1)S(1)}, bf16[1,128,640]{2,1,0:T(8,128)(2,1)S(1)}, u32[]{:S(2)}, u32[]{:S(2)}) collective-permute-start(bf16[1,128,640]{2,1,0:T(8,128)(2,1)S(1)} %bitcast.30), channel_id=1, source_target_pairs={{0,448},{64,128},{128,64},{192,256},{256,192},{320,384},{384,320},... | collective-permute-start | bytes 491528 | tf_op jit(solution)/shard_map/ppermute | solution.py:134
  42.8 14.7 %collective-permute-start.1 = (bf16[2,128,640]{2,1,0:T(8,128)(2,1)S(1)}, bf16[2,128,640]{2,1,0:T(8,128)(2,1)S(1)}, u32[]{:S(2)}, u32[]{:S(2)}) collective-permute-start(bf16[2,128,640]{2,1,0:T(8,128)(2,1)S(1)} %pad_maximum_fusion.refs_0_), channel_id=1, source_target_pairs={{0,448},{64,128},{128,64},{192,256},{256,192},{320,384},{384,320},... | collective-permute-start | bytes 983048 | tf_op jit(solution)/shard_map/ppermute | solution.py:138
  47.2 14.1 %collective-permute-start.4 = (bf16[2,128,640]{2,1,0:T(8,128)(2,1)S(1)}, bf16[2,128,640]{2,1,0:T(8,128)(2,1)S(1)}, u32[]{:S(2)}, u32[]{:S(2)}) collective-permute-start(bf16[2,128,640]{2,1,0:T(8,128)(2,1)S(1)} %pad_maximum_fusion.1.refs_3_.refs_4_), channel_id=1, source_target_pairs={{0,64},{64,0},{128,192},{192,128},{256,320},{320,256},{384,448},{4... | collective-permute-start | bytes 983048 | tf_op jit(solution)/shard_map/ppermute | solution.py:138
  49.1 27.8 %all-to-all-start = ((bf16[8,256,256]{2,1,0:T(8,128)(2,1)}), bf16[8,256,256]{2,1,0:T(8,128)(2,1)S(1)}, u32[]{:S(2)}, u32[]{:S(2)}) async-start(bf16[8,256,256]{2,1,0:T(8,128)(2,1)} %get-tuple-element.19), calls=%async_computation | async-start | bytes 2097152 | tf_op jit(solution)/shard_map/all_to_all | solution.py:260
  57.6 10.9 %collective-permute-start.2 = (bf16[2,128,640]{2,1,0:T(8,128)(2,1)S(1)}, bf16[2,128,640]{2,1,0:T(8,128)(2,1)S(1)}, u32[]{:S(2)}, u32[]{:S(2)}) collective-permute-start(bf16[2,128,640]{2,1,0:T(8,128)(2,1)S(1)} %collective-permute-done.1.refs_1_), channel_id=1, source_target_pairs={{0,64},{64,0},{128,192},{192,128},{256,320},{320,256},{384,448},{4... | collective-permute-start | bytes 983048 | tf_op jit(solution)/shard_map/ppermute | solution.py:138
  61.2 13.0 %collective-permute-start.5 = (bf16[2,128,640]{2,1,0:T(8,128)(2,1)S(1)}, bf16[2,128,640]{2,1,0:T(8,128)(2,1)S(1)}, u32[]{:S(2)}, u32[]{:S(2)}) collective-permute-start(bf16[2,128,640]{2,1,0:T(8,128)(2,1)S(1)} %collective-permute-done.4.refs_4_.refs_5_), channel_id=1, source_target_pairs={{0,448},{64,128},{128,64},{192,256},{256,192},{320,384},{384,320},... | collective-permute-start | bytes 983048 | tf_op jit(solution)/shard_map/ppermute | solution.py:138
  68.5 19.7 %collective-permute-start.6 = (bf16[2,128,640]{2,1,0:T(8,128)(2,1)S(1)}, bf16[2,128,640]{2,1,0:T(8,128)(2,1)S(1)}, u32[]{:S(2)}, u32[]{:S(2)}) collective-permute-start(bf16[2,128,640]{2,1,0:T(8,128)(2,1)S(1)} %collective-permute-done.2.refs_2_), channel_id=1, source_target_pairs={{0,448},{64,128},{128,64},{192,256},{256,192},{320,384},{384,320},... | collective-permute-start | bytes 983048 | tf_op jit(solution)/shard_map/ppermute | solution.py:138
  74.2 17.3 %collective-permute-start.7 = (bf16[2,128,640]{2,1,0:T(8,128)(2,1)S(1)}, bf16[2,128,640]{2,1,0:T(8,128)(2,1)}, u32[]{:S(2)}, u32[]{:S(2)}) collective-permute-start(bf16[2,128,640]{2,1,0:T(8,128)(2,1)S(1)} %collective-permute-done.5.refs_5_.refs_6_), channel_id=1, source_target_pairs={{0,64},{64,0},{128,192},{192,128},{256,320},{320,256},{384,448},{4... | collective-permute-start | bytes 983048 | tf_op jit(solution)/shard_map/ppermute | solution.py:138
  110.5 4.0 %collective-permute-start.8 = (bf16[8,128,256]{2,1,0:T(8,128)(2,1)S(1)}, bf16[8,128,256]{2,1,0:T(8,128)(2,1)S(1)}, u32[]{:S(2)}, u32[]{:S(2)}) collective-permute-start(bf16[8,128,256]{2,1,0:T(8,128)(2,1)S(1)} %get-tuple-element.30), channel_id=1, source_target_pairs={{0,1},{1,0},{2,3},{3,2},{4,5},{5,4},{6,7},{7,6},{8,9},{9,8},{10,11... | collective-permute-start | bytes 1572872 | tf_op jit(solution)/shard_map/ppermute | solution.py:302
  115.4 12.9 %all-to-all-start.2 = ((bf16[4,2,128,256]{3,2,1,0:T(8,128)(2,1)}), bf16[4,2,128,256]{3,2,1,0:T(8,128)(2,1)S(1)}, u32[]{:S(2)}, u32[]{:S(2)}) async-start(bf16[4,2,128,256]{3,2,1,0:T(8,128)(2,1)} %bitcast.8), calls=%async_computation.2 | async-start | bytes 1048576 | tf_op jit(solution)/shard_map/all_to_all | solution.py:304
  148.8 14.6 %all-to-all-start.4 = ((bf16[8,128,256]{2,1,0:T(8,128)(2,1)}), bf16[8,128,256]{2,1,0:T(8,128)(2,1)S(1)}, u32[]{:S(2)}, u32[]{:S(2)}) async-start(bf16[8,128,256]{2,1,0:T(8,128)(2,1)} %ffn.1), calls=%async_computation.4 | async-start | bytes 1048576 | tf_op jit(solution)/shard_map/all_to_all | solution.py:321
  154.0 3.1 %collective-permute-start.9 = (bf16[128,256]{1,0:T(8,128)(2,1)S(1)}, bf16[128,256]{1,0:T(8,128)(2,1)S(1)}, u32[]{:S(2)}, u32[]{:S(2)}) collective-permute-start(bf16[128,256]{1,0:T(8,128)(2,1)S(1)} %dynamic-slice_bitcast_fusion), channel_id=1, source_target_pairs={{0,1},{1,0},{2,3},{3,2},{4,5},{5,4},{6,7},{7,6},{8,9},{9,8},{10,11... | collective-permute-start | bytes 196616 | tf_op jit(solution)/shard_map/ppermute | solution.py:324
Sparse Core Ops, SparseCore 0:
  10.5 115.2 all-gather.1

commit v7 on v6

--- a/solution.py
+++ b/solution.py
@@ -39,20 +39,23 @@
         own[k] = packed
 
 
-def pack_later_kernel(valve, valve_s, raising, raising_s, low, low_s, seq, *refs):
-    ffn, seqs, scales = refs[7:10]
-    scales[:, 0:192] = refs[0][...].reshape(1, 192)
-    scales[:, 192:384] = refs[1][...].reshape(1, 192)
-    for here, there in zip(refs[2:7], refs[10:]):
-        there[...] = here[...]
-    for k in range(8):
-        seqs[k] = seq[...]
+def pack_ffn_kernel(valve, valve_s, raising, raising_s, low, low_s, ffn):
     gate = valve[...] * valve_s[...].reshape(1, 704)
     up = raising[...] * raising_s[...].reshape(1, 704)
     ffn[:, 0:640] = gate[:, 0:640].astype(BF)
     ffn[:, 640:1280] = up[:, 0:640].astype(BF)
     ffn[:, 1280:1408] = jnp.concatenate([gate[:, 640:704], up[:, 640:704]], axis=1).astype(BF)
     ffn[:, 1408:2112] = (low[...] * upright(low_s[...], 32)).astype(BF)
+
+
+def keep_kernel(seq, *refs):
+    seqs, scales = refs[7:9]
+    for k in range(8):
+        seqs[k] = seq[...]
+    scales[:, 0:192] = refs[0][...].reshape(1, 192)
+    scales[:, 192:384] = refs[1][...].reshape(1, 192)
+    for here, there in zip(refs[2:7], refs[9:]):
+        there[...] = here[...]
 
 
 def spread(order, left, right, place=0):
@@ -86,7 +89,8 @@
     prior_ref[...] = multiply(found, x_ref, gain, factor, jnp.zeros((256, 384), F32))
 
 
-def project_kernel(order, x_ref, gain, scales, prior, factor, left, right, act_ref, sq_ref):
+def project_kernel(order, here, x_ref, gain, scales, prior, factor, left, right, act_ref, sq_ref, base):
+    base[...] = x_ref[pl.ds(2 * here[0], 2), pl.ds(pl.multiple_of(128 * here[1], 128), 128), :]
     found = spread(order, [left], [right], 6)
     prior = multiply(found, x_ref, gain, factor[:, 0:1], prior[...])
     act = gelu(prior * scales[...])
@@ -96,10 +100,10 @@
     sums = lax.dot_general(
         ones, signal * signal, NT, precision=lax.Precision.HIGHEST, preferred_element_type=F32
     )
-    sq_ref[0] = sums[0:1]
-
-
-def gate_kernel(order, core, act_ref, sq_ref, mats, offs, gain, *refs):
+    sq_ref[...] = jnp.broadcast_to(sums[0:1].reshape(1, 1, 256), (8, 1, 256))
+
+
+def gate_kernel(order, place, act_ref, sq_ref, mats, offs, gain, *refs):
     pieces, kept, sent, gated = refs[:8], refs[8], refs[9], refs[10]
     total = jnp.sum(sq_ref[...], axis=0)
     factor = lax.rsqrt(total / 1536.0 + EPS)
@@ -117,7 +121,7 @@
             gated[b, :, 64 * g : 64 * g + 64] = (
                 act_ref[at, 64 * g : 64 * g + 64] * mixed
             ).astype(BF)
-    here = core[0]
+    here = place[1]
     mine, other = gated[here], gated[1 - here]
     for block, half, ref, k in spread(order, pieces[:4], pieces[4:]):
         piece = ref[k, :, 384:576]
@@ -223,12 +227,25 @@
         out_shape=jax.ShapeDtypeStruct((8, 32, 640), BF),
         name="pack",
     )(conveyor_matrix, blend_value_matrix, branch_emission_matrix.T, emission_rescalers)
-    ffn_own, seqs, scales, gain, latter_gain, mats, offs, blend_gain = pl.pallas_call(
-        pack_later_kernel,
-        in_specs=[VM] * 14,
-        out_specs=[VM] * 8,
+    ffn_own = pl.pallas_call(
+        pack_ffn_kernel,
+        in_specs=[VM] * 6,
+        out_specs=VM,
+        out_shape=jax.ShapeDtypeStruct((32, 2112), BF),
+        name="pack_ffn",
+    )(
+        valve_matrix,
+        valve_rescalers,
+        raising_matrix,
+        raising_rescalers,
+        lowering_matrix.T,
+        lowering_rescalers,
+    )
+    seqs, scales, gain, latter_gain, mats, offs, blend_gain = pl.pallas_call(
+        keep_kernel,
+        in_specs=[VM] * 8,
+        out_specs=[VM] * 7,
         out_shape=[
-            jax.ShapeDtypeStruct((32, 2112), BF),
             jax.ShapeDtypeStruct((8, 256, 256), BF),
             pltpu.VMEM((1, 384), F32),
             pltpu.VMEM((8, 1, 256), F32),
@@ -237,14 +254,8 @@
             pltpu.VMEM((3, 128), F32),
             pltpu.VMEM((1, 192), F32),
         ],
-        name="pack_later",
+        name="keep",
     )(
-        valve_matrix,
-        valve_rescalers,
-        raising_matrix,
-        raising_rescalers,
-        lowering_matrix.T,
-        lowering_rescalers,
         sequence_entries,
         conveyor_rescalers,
         blend_rescalers,
@@ -272,15 +283,20 @@
         compiler_params=limit(4),
         name="early",
     )(order, near, gain, *left[:3], *right[:3])
-    act, own_sq = pl.pallas_call(
+    here = jnp.stack([x, c]).astype(jnp.int32)
+    act, own_sq, base = pl.pallas_call(
         project_kernel,
-        in_specs=[SM] + [VM] * 7,
-        out_specs=[VM, VM],
-        out_shape=[pltpu.VMEM((256, 384), F32), jax.ShapeDtypeStruct((1, 1, 256), F32)],
+        in_specs=[SM, SM] + [VM] * 7,
+        out_specs=[VM] * 3,
+        out_shape=[
+            pltpu.VMEM((256, 384), F32),
+            jax.ShapeDtypeStruct((8, 1, 256), F32),
+            jax.ShapeDtypeStruct((2, 128, 256), BF),
+        ],
         compiler_params=limit(4),
         name="project",
-    )(order, near, gain, scales, prior, factor, left[3], right[3])
-    all_sq = lax.all_gather(own_sq, TP, axis=0, tiled=True)
+    )(order, here, near, gain, scales, prior, factor, left[3], right[3])
+    all_sq = lax.all_to_all(own_sq, TP, 0, 0, tiled=True)
     kept, sent = pl.pallas_call(
         gate_kernel,
         in_specs=[SM, SM] + [VM] * 13,
@@ -291,7 +307,7 @@
         name="gating",
     )(
         order,
-        c.astype(jnp.int32).reshape(1),
+        here,
         act,
         all_sq,
         mats,
@@ -302,7 +318,6 @@
     got = lax.ppermute(sent, "c", swap)
     both = (kept.astype(F32) + got.astype(F32)).astype(BF).reshape(4, 2, 128, 256)
     shares = lax.all_to_all(both, "x", 0, 0, tiled=True)
-    base = lax.dynamic_slice(rows, (2 * x, 128 * c, 0), (2, 128, 256))
     mid_own = (base.astype(F32) + jnp.sum(shares.astype(F32), axis=0)).astype(BF)
     mid = from_everyone(mid_own, "x").reshape(8, 128, 256)
     outs = pl.pallas_call(

time: 172 us -> 170 us (0.988)
  blocking collectives: 43.7 us -> 53.7 us
  waiting for transfers between devices: 34.3 us -> 25.1 us
  starting transfers between devices: 57.9 us -> 53.5 us
    all_to_all x0 -> x2, blocking collectives: none -> 25.2 us  [the longest x1 13.6 us: on_device(): all_sq = lax.all_to_all(own_sq, TP, 0, 0, tiled=True)]
    all_gather x1 -> x0, blocking collectives: 15 us -> none  [on_device(): all_sq = lax.all_gather(own_sq, TP, axis=0, tiled=True)]
    all_to_all x1 -> x0, waiting for transfers between devices: 9.39 us -> none  [on_device(): shares = lax.all_to_all(both, 'x', 0, 0, tiled=True)]
    all_to_all x1 -> x0, starting transfers between devices: 3.47 us -> none  [on_device(): shares = lax.all_to_all(both, 'x', 0, 0, tiled=True)]
    pallas_call x2 -> x3, Pallas kernels: 4.21 us -> 5.31 us  [the longest x1 2.07 us: on_device(): pl.pallas_call(keep_kernel, in_specs=[VM] * 8, out_specs=[VM] * 7, out_sh...]
  transfers between devices with their start and end apart: 14 -> 13, of which waited for: 8 -> 7; matrix products, arithmetic and copies ran while one was open for 1% -> 1% of each run, Pallas kernels for 4% -> 6%
where the time goes in v7:
time: 170 us; the launch traced here: 169 us
  blocking collectives  53.7 us (32%)
  starting transfers between devices  53.5 us (31%)
  waiting for transfers between devices  25.1 us (15%)
  Pallas kernels  20.4 us (12%)
  between operations  13.6 us (8%)
  other arithmetic  1.92 us (1%)
    ppermute x6, starting transfers between devices, exchange(): batch = lax.ppermute(batch, 'z', turn)  20.6 us
    all_to_all x1, blocking collectives, on_device(): first = lax.all_to_all(own, 'y', 0, 0, tiled=True)  17.6 us
    ppermute x6, waiting for transfers between devices, exchange(): batch = lax.ppermute(batch, 'z', turn)  16 us
    ppermute x2, starting transfers between devices, exchange(): got = lax.ppermute(own, 'z', to_pair)  14.6 us
    all_to_all x1, blocking collectives, on_device(): all_sq = lax.all_to_all(own_sq, TP, 0, 0, tiled=True)  13.6 us
    all_to_all x1, blocking collectives, on_device(): shares = lax.all_to_all(both, 'x', 0, 0, tiled=True)  11.7 us
    all_to_all x1, blocking collectives, from_everyone(): return lax.all_to_all(copies, axis, split_axis=0, concat_axis=0, tiled=True)  10.8 us
    pallas_call x1, Pallas kernels, on_device(): pl.pallas_call(ffn_kernel, in_specs=[VM, VM, pl.BlockSpec(memory_space=pl...  9.37 us
  transfers between devices with their start and end apart: 13, of which 7 were waited for; matrix products, arithmetic and copies ran while one was open for 1% of the time, Pallas kernels for 6%

profile of v7, /device:TPU:1, one launch (start us, length us, event | category | flops | bytes accessed | tf_op | source)
XLA Modules:
  0.0 168.9 jit_solution(18337813626838981769)
XLA Ops:
  6.5 1.8 %pack_ffn.1 = bf16[32,2112]{1,0:T(8,128)(2,1)} custom-call(f32[32,704]{1,0:T(8,128)} %valve.1, f32[704]{0:T(1024)} %valve_s.1, f32[32,704]{1,0:T(8,128)} %raising.1, f32[704]{0:T(1024)} %raising_s.1, f32[32,704]{1,0:T(8,128)} %bitcast.36, f32[32]{0:T(128)} %low_s.1), custom_call_target="tpu_custom_call" | custom-call | tf_op jit(solution)/shard_map/pack_ffn/pallas_call | solution.py:230
  8.3 1.6 pack.1
  10.0 17.6 %all_to_all.30 = bf16[8,32,640]{2,1,0:T(8,128)(2,1)S(1)} all-to-all(bf16[8,32,640]{2,1,0:T(8,128)(2,1)} %pack.1), channel_id=1, replica_groups=mesh['z'=8,'y'=8,'x'=4,'c'=2] {'y'}, dimensions={0} | all-to-all | bytes 655360 | tf_op jit(solution)/shard_map/all_to_all | solution.py:270
  27.6 5.8 %collective-permute-start = (bf16[1,128,640]{2,1,0:T(8,128)(2,1)S(1)}, bf16[1,128,640]{2,1,0:T(8,128)(2,1)S(1)}, u32[]{:S(2)}, u32[]{:S(2)}) collective-permute-start(bf16[1,128,640]{2,1,0:T(8,128)(2,1)S(1)} %bitcast.34), channel_id=1, source_target_pairs={{0,64},{64,0},{128,192},{192,128},{256,320},{320,256},{384,448},{4... | collective-permute-start | bytes 491528 | tf_op jit(solution)/shard_map/ppermute | solution.py:138
  33.4 8.8 %collective-permute-start.3 = (bf16[1,128,640]{2,1,0:T(8,128)(2,1)S(1)}, bf16[1,128,640]{2,1,0:T(8,128)(2,1)S(1)}, u32[]{:S(2)}, u32[]{:S(2)}) collective-permute-start(bf16[1,128,640]{2,1,0:T(8,128)(2,1)S(1)} %bitcast.32), channel_id=1, source_target_pairs={{0,448},{64,128},{128,64},{192,256},{256,192},{320,384},{384,320},... | collective-permute-start | bytes 491528 | tf_op jit(solution)/shard_map/ppermute | solution.py:138
  42.3 4.6 %collective-permute-start.1 = (bf16[2,128,640]{2,1,0:T(8,128)(2,1)S(1)}, bf16[2,128,640]{2,1,0:T(8,128)(2,1)S(1)}, u32[]{:S(2)}, u32[]{:S(2)}) collective-permute-start(bf16[2,128,640]{2,1,0:T(8,128)(2,1)S(1)} %pad_maximum_fusion.refs_0_), channel_id=1, source_target_pairs={{0,448},{64,128},{128,64},{192,256},{256,192},{320,384},{384,320},... | collective-permute-start | bytes 983048 | tf_op jit(solution)/shard_map/ppermute | solution.py:142
  47.0 1.9 %collective-permute-start.4 = (bf16[2,128,640]{2,1,0:T(8,128)(2,1)S(1)}, bf16[2,128,640]{2,1,0:T(8,128)(2,1)S(1)}, u32[]{:S(2)}, u32[]{:S(2)}) collective-permute-start(bf16[2,128,640]{2,1,0:T(8,128)(2,1)S(1)} %pad_maximum_fusion.1.refs_3_.refs_4_), channel_id=1, source_target_pairs={{0,64},{64,0},{128,192},{192,128},{256,320},{320,256},{384,448},{4... | collective-permute-start | bytes 983048 | tf_op jit(solution)/shard_map/ppermute | solution.py:142
  48.9 2.1 %keep.1 = (bf16[8,256,256]{2,1,0:T(8,128)(2,1)}, f32[1,384]{1,0:T(1,128)S(1)}, f32[8,1,256]{2,1,0:T(1,128)S(1)}, f32[8,1,256]{2,1,0:T(1,128)S(1)}, bf16[3,128,12...) custom-call(bf16[256,256]{1,0:T(8,128)(2,1)} %seq.1, f32[192]{0:T(256)} %refs_0_.1, f32[192]{0:T(256)} %refs_1_.1, ...), custom_call_target="tpu_custom_call" | custom-call | tf_op jit(solution)/shard_map/keep/pallas_call | solution.py:244
  51.6 8.3 %all-to-all-start = ((bf16[8,256,256]{2,1,0:T(8,128)(2,1)}), bf16[8,256,256]{2,1,0:T(8,128)(2,1)S(1)}, u32[]{:S(2)}, u32[]{:S(2)}) async-start(bf16[8,256,256]{2,1,0:T(8,128)(2,1)} %get-tuple-element.19), calls=%async_computation | async-start | bytes 2097152 | tf_op jit(solution)/shard_map/all_to_all | solution.py:271
  59.9 3.6 %collective-permute-start.2 = (bf16[2,128,640]{2,1,0:T(8,128)(2,1)S(1)}, bf16[2,128,640]{2,1,0:T(8,128)(2,1)S(1)}, u32[]{:S(2)}, u32[]{:S(2)}) collective-permute-start(bf16[2,128,640]{2,1,0:T(8,128)(2,1)S(1)} %collective-permute-done.1.refs_1_), channel_id=1, source_target_pairs={{0,64},{64,0},{128,192},{192,128},{256,320},{320,256},{384,448},{4... | collective-permute-start | bytes 983048 | tf_op jit(solution)/shard_map/ppermute | solution.py:142
  63.5 4.1 %collective-permute-start.5 = (bf16[2,128,640]{2,1,0:T(8,128)(2,1)S(1)}, bf16[2,128,640]{2,1,0:T(8,128)(2,1)}, u32[]{:S(2)}, u32[]{:S(2)}) collective-permute-start(bf16[2,128,640]{2,1,0:T(8,128)(2,1)S(1)} %collective-permute-done.4.refs_4_.refs_5_), channel_id=1, source_target_pairs={{0,448},{64,128},{128,64},{192,256},{256,192},{320,384},{384,320},... | collective-permute-start | bytes 983048 | tf_op jit(solution)/shard_map/ppermute | solution.py:142
  67.7 4.0 %collective-permute-done.2.refs_2_ = bf16[2,128,640]{2,1,0:T(8,128)(2,1)S(1)} collective-permute-done((bf16[2,128,640]{2,1,0:T(8,128)(2,1)S(1)}, bf16[2,128,640]{2,1,0:T(8,128)(2,1)S(1)}, u32[]{:S(2)}, u32[]{:S(2)}) %collective-permute-start.2) | collective-permute-done | bytes 327712 | tf_op jit(solution)/shard_map/ppermute | solution.py:142
  71.7 4.4 %collective-permute-start.6 = (bf16[2,128,640]{2,1,0:T(8,128)(2,1)S(1)}, bf16[2,128,640]{2,1,0:T(8,128)(2,1)S(1)}, u32[]{:S(2)}, u32[]{:S(2)}) collective-permute-start(bf16[2,128,640]{2,1,0:T(8,128)(2,1)S(1)} %collective-permute-done.2.refs_2_), channel_id=1, source_target_pairs={{0,448},{64,128},{128,64},{192,256},{256,192},{320,384},{384,320},... | collective-permute-start | bytes 983048 | tf_op jit(solution)/shard_map/ppermute | solution.py:142
  76.1 0.9 collective-permute-done.5.refs_5_.refs_6_
  77.0 1.9 %collective-permute-start.7 = (bf16[2,128,640]{2,1,0:T(8,128)(2,1)}, bf16[2,128,640]{2,1,0:T(8,128)(2,1)S(1)}, u32[]{:S(2)}, u32[]{:S(2)}) collective-permute-start(bf16[2,128,640]{2,1,0:T(8,128)(2,1)} %collective-permute-done.5.refs_5_.refs_6_), channel_id=1, source_target_pairs={{0,64},{64,0},{128,192},{192,128},{256,320},{320,256},{384,448},{4... | collective-permute-start | bytes 983048 | tf_op jit(solution)/shard_map/ppermute | solution.py:142
  79.0 0.7 add_and_fusion.order
  79.7 2.0 %early.1 = (f32[256,384]{1,0:T(8,128)S(1)}, f32[256,128]{1,0:T(8,128)S(1)}) custom-call(s32[2,8]{1,0:T(2,128)S(1)} %add_and_fusion.order, bf16[8,256,256]{2,1,0:T(8,128)(2,1)S(1)} %all-to-all-done.x_ref, f32[8,1,256]{2,1,0:T(1,128)S(1)} %get-tuple-element.20.gain, bf16[2,128,640]{2,1,0:T(8,128)(2,1)S(1)} %pad_maximum_fusion.refs_0_, ...), custom_call_target="tpu_custom_call" | custom-call | tf_op jit(solution)/shard_map/early/pallas_call | solution.py:278
  81.8 9.6 %collective-permute-done.6.left.refs_3_ = bf16[2,128,640]{2,1,0:T(8,128)(2,1)S(1)} collective-permute-done((bf16[2,128,640]{2,1,0:T(8,128)(2,1)S(1)}, bf16[2,128,640]{2,1,0:T(8,128)(2,1)S(1)}, u32[]{:S(2)}, u32[]{:S(2)}) %collective-permute-start.6) | collective-permute-done | bytes 327712 | tf_op jit(solution)/shard_map/ppermute | solution.py:142
  91.4 1.6 collective-permute-done.7.right.refs_7_
  92.9 1.5 project.1
  94.4 13.6 %all_to_all.31.sq_ref = f32[8,1,256]{2,1,0:T(1,128)S(1)} all-to-all(f32[8,1,256]{2,1,0:T(1,128)S(1)} %get-tuple-element.26), channel_id=1, replica_groups=mesh['z'=8,'y'=8,'x'=4,'c'=2] {'x','c'}, dimensions={0} | all-to-all | bytes 16384 | tf_op jit(solution)/shard_map/all_to_all | solution.py:299
  108.0 2.1 %gating.1 = (bf16[8,128,256]{2,1,0:T(8,128)(2,1)S(1)}, bf16[8,128,256]{2,1,0:T(8,128)(2,1)S(1)}) custom-call(s32[2,8]{1,0:T(2,128)S(1)} %add_and_fusion.order, s32[2]{0:T(128)S(1)} %pad_add_fusion.here.place, f32[256,384]{1,0:T(8,128)S(1)} %get-tuple-element.25.act_ref, f32[8,1,256]{2,1,0:T(1,128)S(1)} %all_to_all.31.sq_ref, ...), custom_call_target="tpu_custom_call" | custom-call | tf_op jit(solution)/shard_map/gating/pallas_call | solution.py:300
  110.0 2.5 %collective-permute-start.8 = (bf16[8,128,256]{2,1,0:T(8,128)(2,1)S(1)}, bf16[8,128,256]{2,1,0:T(8,128)(2,1)S(1)}, u32[]{:S(2)}, u32[]{:S(2)}) collective-permute-start(bf16[8,128,256]{2,1,0:T(8,128)(2,1)S(1)} %get-tuple-element.31), channel_id=1, source_target_pairs={{0,1},{1,0},{2,3},{3,2},{4,5},{5,4},{6,7},{7,6},{8,9},{9,8},{10,11... | collective-permute-start | bytes 1572872 | tf_op jit(solution)/shard_map/ppermute | solution.py:318
  112.6 1.8 %collective-permute-done.8 = bf16[8,128,256]{2,1,0:T(8,128)(2,1)S(1)} collective-permute-done((bf16[8,128,256]{2,1,0:T(8,128)(2,1)S(1)}, bf16[8,128,256]{2,1,0:T(8,128)(2,1)S(1)}, u32[]{:S(2)}, u32[]{:S(2)}) %collective-permute-start.8) | collective-permute-done | bytes 524320 | tf_op jit(solution)/shard_map/ppermute | solution.py:318
  114.5 11.7 %all_to_all.32 = bf16[4,2,128,256]{3,2,1,0:T(8,128)(2,1)S(1)} all-to-all(bf16[4,2,128,256]{3,2,1,0:T(8,128)(2,1)S(1)} %bitcast.30), channel_id=1, replica_groups=mesh['z'=8,'y'=8,'x'=4,'c'=2] {'x'}, dimensions={0} | all-to-all | bytes 1048576 | tf_op jit(solution)/shard_map/all_to_all | solution.py:320
  126.3 10.8 %all_to_all.33 = bf16[4,2,128,256]{3,2,1,0:T(8,128)(2,1)S(1)} all-to-all(bf16[4,2,128,256]{3,2,1,0:T(8,128)(2,1)S(1)} %broadcast_in_dim.2), channel_id=1, replica_groups=mesh['z'=8,'y'=8,'x'=4,'c'=2] {'x'}, dimensions={0} | all-to-all | bytes 1048576 | tf_op jit(solution)/shard_map/all_to_all | solution.py:22
  137.1 9.4 %ffn.1 = bf16[8,128,256]{2,1,0:T(8,128)(2,1)} custom-call(bf16[8,128,256]{2,1,0:T(8,128)(2,1)S(1)} %bitcast.28, f32[8,1,256]{2,1,0:T(1,128)} %copy-done, bf16[8,8,2,32,2112]{4,3,2,1,0:T(8,128)(2,1)} %bitcast.29), custom_call_target="tpu_custom_call" | custom-call | tf_op jit(solution)/shard_map/ffn/pallas_call | solution.py:323
  146.5 5.4 %all-to-all-start.5 = ((bf16[8,128,256]{2,1,0:T(8,128)(2,1)}), bf16[8,128,256]{2,1,0:T(8,128)(2,1)S(1)}, u32[]{:S(2)}, u32[]{:S(2)}) async-start(bf16[8,128,256]{2,1,0:T(8,128)(2,1)} %ffn.1), calls=%async_computation.5 | async-start | bytes 1048576 | tf_op jit(solution)/shard_map/all_to_all | solution.py:336
  151.9 2.0 %collective-permute-start.9 = (bf16[128,256]{1,0:T(8,128)(2,1)S(1)}, bf16[128,256]{1,0:T(8,128)(2,1)S(1)}, u32[]{:S(2)}, u32[]{:S(2)}) collective-permute-start(bf16[128,256]{1,0:T(8,128)(2,1)S(1)} %dynamic-slice_bitcast_fusion), channel_id=1, source_target_pairs={{0,1},{1,0},{2,3},{3,2},{4,5},{5,4},{6,7},{7,6},{8,9},{9,8},{10,11... | collective-permute-start | bytes 196616 | tf_op jit(solution)/shard_map/ppermute | solution.py:339
  154.0 1.1 collective-permute-done.9
  155.1 6.2 %all-to-all-done.5 = bf16[8,128,256]{2,1,0:T(8,128)(2,1)S(1)} async-done(((bf16[8,128,256]{2,1,0:T(8,128)(2,1)}), bf16[8,128,256]{2,1,0:T(8,128)(2,1)S(1)}, u32[]{:S(2)}, u32[]{:S(2)}) %all-to-all-start.5) | async-done | bytes 524320 | tf_op jit(solution)/shard_map/all_to_all | solution.py:336
  161.4 0.7 add_convert_fusion.1
  (22 shorter events, 1.2 us)
Async XLA Ops:
  6.5 130.6 %all-gather.2.cloned.1.call-start = ((), (), s32[]{:S(2)}) async-start(), calls=%async_computation.6 | async-start | bytes 17965056 | tf_op jit(solution)/shard_map/all_gather | solution.py:268
  27.6 14.6 %collective-permute-start = (bf16[1,128,640]{2,1,0:T(8,128)(2,1)S(1)}, bf16[1,128,640]{2,1,0:T(8,128)(2,1)S(1)}, u32[]{:S(2)}, u32[]{:S(2)}) collective-permute-start(bf16[1,128,640]{2,1,0:T(8,128)(2,1)S(1)} %bitcast.34), channel_id=1, source_target_pairs={{0,64},{64,0},{128,192},{192,128},{256,320},{320,256},{384,448},{4... | collective-permute-start | bytes 491528 | tf_op jit(solution)/shard_map/ppermute | solution.py:138
  33.4 13.5 %collective-permute-start.3 = (bf16[1,128,640]{2,1,0:T(8,128)(2,1)S(1)}, bf16[1,128,640]{2,1,0:T(8,128)(2,1)S(1)}, u32[]{:S(2)}, u32[]{:S(2)}) collective-permute-start(bf16[1,128,640]{2,1,0:T(8,128)(2,1)S(1)} %bitcast.32), channel_id=1, source_target_pairs={{0,448},{64,128},{128,64},{192,256},{256,192},{320,384},{384,320},... | collective-permute-start | bytes 491528 | tf_op jit(solution)/shard_map/ppermute | solution.py:138
  42.3 17.6 %collective-permute-start.1 = (bf16[2,128,640]{2,1,0:T(8,128)(2,1)S(1)}, bf16[2,128,640]{2,1,0:T(8,128)(2,1)S(1)}, u32[]{:S(2)}, u32[]{:S(2)}) collective-permute-start(bf16[2,128,640]{2,1,0:T(8,128)(2,1)S(1)} %pad_maximum_fusion.refs_0_), channel_id=1, source_target_pairs={{0,448},{64,128},{128,64},{192,256},{256,192},{320,384},{384,320},... | collective-permute-start | bytes 983048 | tf_op jit(solution)/shard_map/ppermute | solution.py:142
  47.0 16.6 %collective-permute-start.4 = (bf16[2,128,640]{2,1,0:T(8,128)(2,1)S(1)}, bf16[2,128,640]{2,1,0:T(8,128)(2,1)S(1)}, u32[]{:S(2)}, u32[]{:S(2)}) collective-permute-start(bf16[2,128,640]{2,1,0:T(8,128)(2,1)S(1)} %pad_maximum_fusion.1.refs_3_.refs_4_), channel_id=1, source_target_pairs={{0,64},{64,0},{128,192},{192,128},{256,320},{320,256},{384,448},{4... | collective-permute-start | bytes 983048 | tf_op jit(solution)/shard_map/ppermute | solution.py:142
  51.0 0.6 copy-start
  51.6 28.2 %all-to-all-start = ((bf16[8,256,256]{2,1,0:T(8,128)(2,1)}), bf16[8,256,256]{2,1,0:T(8,128)(2,1)S(1)}, u32[]{:S(2)}, u32[]{:S(2)}) async-start(bf16[8,256,256]{2,1,0:T(8,128)(2,1)} %get-tuple-element.19), calls=%async_computation | async-start | bytes 2097152 | tf_op jit(solution)/shard_map/all_to_all | solution.py:271
  59.9 11.8 %collective-permute-start.2 = (bf16[2,128,640]{2,1,0:T(8,128)(2,1)S(1)}, bf16[2,128,640]{2,1,0:T(8,128)(2,1)S(1)}, u32[]{:S(2)}, u32[]{:S(2)}) collective-permute-start(bf16[2,128,640]{2,1,0:T(8,128)(2,1)S(1)} %collective-permute-done.1.refs_1_), channel_id=1, source_target_pairs={{0,64},{64,0},{128,192},{192,128},{256,320},{320,256},{384,448},{4... | collective-permute-start | bytes 983048 | tf_op jit(solution)/shard_map/ppermute | solution.py:142
  63.5 13.5 %collective-permute-start.5 = (bf16[2,128,640]{2,1,0:T(8,128)(2,1)S(1)}, bf16[2,128,640]{2,1,0:T(8,128)(2,1)}, u32[]{:S(2)}, u32[]{:S(2)}) collective-permute-start(bf16[2,128,640]{2,1,0:T(8,128)(2,1)S(1)} %collective-permute-done.4.refs_4_.refs_5_), channel_id=1, source_target_pairs={{0,448},{64,128},{128,64},{192,256},{256,192},{320,384},{384,320},... | collective-permute-start | bytes 983048 | tf_op jit(solution)/shard_map/ppermute | solution.py:142
  71.7 19.7 %collective-permute-start.6 = (bf16[2,128,640]{2,1,0:T(8,128)(2,1)S(1)}, bf16[2,128,640]{2,1,0:T(8,128)(2,1)S(1)}, u32[]{:S(2)}, u32[]{:S(2)}) collective-permute-start(bf16[2,128,640]{2,1,0:T(8,128)(2,1)S(1)} %collective-permute-done.2.refs_2_), channel_id=1, source_target_pairs={{0,448},{64,128},{128,64},{192,256},{256,192},{320,384},{384,320},... | collective-permute-start | bytes 983048 | tf_op jit(solution)/shard_map/ppermute | solution.py:142
  77.0 15.9 %collective-permute-start.7 = (bf16[2,128,640]{2,1,0:T(8,128)(2,1)}, bf16[2,128,640]{2,1,0:T(8,128)(2,1)S(1)}, u32[]{:S(2)}, u32[]{:S(2)}) collective-permute-start(bf16[2,128,640]{2,1,0:T(8,128)(2,1)} %collective-permute-done.5.refs_5_.refs_6_), channel_id=1, source_target_pairs={{0,64},{64,0},{128,192},{192,128},{256,320},{320,256},{384,448},{4... | collective-permute-start | bytes 983048 | tf_op jit(solution)/shard_map/ppermute | solution.py:142
  110.0 4.3 %collective-permute-start.8 = (bf16[8,128,256]{2,1,0:T(8,128)(2,1)S(1)}, bf16[8,128,256]{2,1,0:T(8,128)(2,1)S(1)}, u32[]{:S(2)}, u32[]{:S(2)}) collective-permute-start(bf16[8,128,256]{2,1,0:T(8,128)(2,1)S(1)} %get-tuple-element.31), channel_id=1, source_target_pairs={{0,1},{1,0},{2,3},{3,2},{4,5},{5,4},{6,7},{7,6},{8,9},{9,8},{10,11... | collective-permute-start | bytes 1572872 | tf_op jit(solution)/shard_map/ppermute | solution.py:318
  146.5 14.8 %all-to-all-start.5 = ((bf16[8,128,256]{2,1,0:T(8,128)(2,1)}), bf16[8,128,256]{2,1,0:T(8,128)(2,1)S(1)}, u32[]{:S(2)}, u32[]{:S(2)}) async-start(bf16[8,128,256]{2,1,0:T(8,128)(2,1)} %ffn.1), calls=%async_computation.5 | async-start | bytes 1048576 | tf_op jit(solution)/shard_map/all_to_all | solution.py:336
  151.9 3.1 %collective-permute-start.9 = (bf16[128,256]{1,0:T(8,128)(2,1)S(1)}, bf16[128,256]{1,0:T(8,128)(2,1)S(1)}, u32[]{:S(2)}, u32[]{:S(2)}) collective-permute-start(bf16[128,256]{1,0:T(8,128)(2,1)S(1)} %dynamic-slice_bitcast_fusion), channel_id=1, source_target_pairs={{0,1},{1,0},{2,3},{3,2},{4,5},{5,4},{6,7},{7,6},{8,9},{9,8},{10,11... | collective-permute-start | bytes 196616 | tf_op jit(solution)/shard_map/ppermute | solution.py:339
Sparse Core Ops, SparseCore 0:
  10.5 116.7 all-gather.1

commit v8 on v7

--- a/solution.py
+++ b/solution.py
@@ -48,14 +48,22 @@
     ffn[:, 1408:2112] = (low[...] * upright(low_s[...], 32)).astype(BF)
 
 
-def keep_kernel(seq, *refs):
-    seqs, scales = refs[7:9]
+def keep_kernel(seq, conv_s, blend_s, gain1, gain2, mats, offs, blend_gain, seqs, scales, keep1, keep2, group):
     for k in range(8):
         seqs[k] = seq[...]
-    scales[:, 0:192] = refs[0][...].reshape(1, 192)
-    scales[:, 192:384] = refs[1][...].reshape(1, 192)
-    for here, there in zip(refs[2:7], refs[9:]):
-        there[...] = here[...]
+    scales[:, 0:192] = conv_s[...].reshape(1, 192)
+    scales[:, 192:384] = blend_s[...].reshape(1, 192)
+    keep1[...] = gain1[...]
+    keep2[...] = gain2[...]
+    for g in range(3):
+        group[128 * g : 128 * g + 128] = mats[g].astype(F32)
+    group[384:387] = offs[...]
+    gains = blend_gain[...]
+    for g in range(3):
+        group[392 + g : 393 + g, 0:64] = gains[:, 64 * g : 64 * g + 64]
+        group[392 + g : 393 + g, 64:128] = jnp.zeros((1, 64), F32)
+    group[387:392] = jnp.zeros((5, 128), F32)
+    group[395:400] = jnp.zeros((5, 128), F32)
 
 
 def spread(order, left, right, place=0):
@@ -89,47 +97,44 @@
     prior_ref[...] = multiply(found, x_ref, gain, factor, jnp.zeros((256, 384), F32))
 
 
-def project_kernel(order, here, x_ref, gain, scales, prior, factor, left, right, act_ref, sq_ref, base):
+def project_kernel(order, here, x_ref, gain, scales, prior, factor, *refs):
+    pieces, (mine, yours, sq_ref, base, emis) = refs[:8], refs[8:]
     base[...] = x_ref[pl.ds(2 * here[0], 2), pl.ds(pl.multiple_of(128 * here[1], 128), 128), :]
-    found = spread(order, [left], [right], 6)
-    prior = multiply(found, x_ref, gain, factor[:, 0:1], prior[...])
-    act = gelu(prior * scales[...])
-    act_ref[...] = act
+    for block, half, ref, k in spread(order, pieces[:4], pieces[4:]):
+        emis[block, pl.ds(128 * half, 128), :] = ref[k, :, 384:640]
+    found = spread(order, pieces[3:4], pieces[7:8], 6)
+    sums = multiply(found, x_ref, gain, factor[:, 0:1], prior[...])
+    act = gelu(sums * scales[...])
+    first = here[1] == 0
+    mine[...] = jnp.where(first, act[0:128], act[128:256])
+    yours[...] = jnp.where(first, act[128:256], act[0:128])
     signal = act[:, 192:384]
     ones = jnp.ones((8, 192), F32)
-    sums = lax.dot_general(
+    squares = lax.dot_general(
         ones, signal * signal, NT, precision=lax.Precision.HIGHEST, preferred_element_type=F32
     )
-    sq_ref[...] = jnp.broadcast_to(sums[0:1].reshape(1, 1, 256), (8, 1, 256))
-
-
-def gate_kernel(order, place, act_ref, sq_ref, mats, offs, gain, *refs):
-    pieces, kept, sent, gated = refs[:8], refs[8], refs[9], refs[10]
+    sq_ref[...] = jnp.broadcast_to(squares[0:1].reshape(1, 1, 256), (8, 1, 256))
+
+
+def gate_kernel(place, mine, theirs, sq_ref, my_group, their_group, my_emis, their_emis, out_ref, gated):
     total = jnp.sum(sq_ref[...], axis=0)
     factor = lax.rsqrt(total / 1536.0 + EPS)
+    factor = jnp.where(place[1] == 0, factor[:, 0:128], factor[:, 128:256])
     rows = lax.broadcasted_iota(jnp.int32, (128, 128), 0)
     cols = lax.broadcasted_iota(jnp.int32, (128, 128), 1)
     lower = cols <= rows
-    gains = gain[...]
-    for g in range(3):
-        mat = jnp.where(lower, mats[g].astype(F32), 0.0)
-        for b in range(2):
-            at = pl.ds(128 * b, 128)
-            mix = (mat * factor[:, 128 * b : 128 * b + 128]).astype(BF)
-            sig = (act_ref[at, 192 + 64 * g : 256 + 64 * g] * gains[:, 64 * g : 64 * g + 64]).astype(BF)
-            mixed = jnp.dot(mix, sig, preferred_element_type=F32) + upright(offs[g], 128)
-            gated[b, :, 64 * g : 64 * g + 64] = (
-                act_ref[at, 64 * g : 64 * g + 64] * mixed
-            ).astype(BF)
-    here = place[1]
-    mine, other = gated[here], gated[1 - here]
-    for block, half, ref, k in spread(order, pieces[:4], pieces[4:]):
-        piece = ref[k, :, 384:576]
-        cols = pl.ds(128 * half, 128)
-        part = lax.dot_general(mine, piece, NT, preferred_element_type=F32)
-        kept[block, :, cols] = part.astype(BF)
-        part = lax.dot_general(other, piece, NT, preferred_element_type=F32)
-        sent[block, :, cols] = part.astype(BF)
+    for side, (act, group) in enumerate(((mine, my_group), (theirs, their_group))):
+        for g in range(3):
+            mat = jnp.where(lower, group[128 * g : 128 * g + 128], 0.0)
+            mix = (mat * factor).astype(BF)
+            gains = group[392 + g : 393 + g, 0:64]
+            sig = (act[:, 192 + 64 * g : 256 + 64 * g] * gains).astype(BF)
+            mixed = jnp.dot(mix, sig, preferred_element_type=F32) + upright(group[384 + g], 128)
+            gated[side, :, 64 * g : 64 * g + 64] = (act[:, 64 * g : 64 * g + 64] * mixed).astype(BF)
+    for k in range(8):
+        part = lax.dot_general(gated[0], my_emis[k, :, 0:192], NT, preferred_element_type=F32)
+        more = lax.dot_general(gated[1], their_emis[k, :, 0:192], NT, preferred_element_type=F32)
+        out_ref[k] = (part + more).astype(BF)
 
 
 def exchange(own, flip):
@@ -241,18 +246,16 @@
         lowering_matrix.T,
         lowering_rescalers,
     )
-    seqs, scales, gain, latter_gain, mats, offs, blend_gain = pl.pallas_call(
+    seqs, scales, gain, latter_gain, group = pl.pallas_call(
         keep_kernel,
         in_specs=[VM] * 8,
-        out_specs=[VM] * 7,
+        out_specs=[VM] * 5,
         out_shape=[
             jax.ShapeDtypeStruct((8, 256, 256), BF),
             pltpu.VMEM((1, 384), F32),
             pltpu.VMEM((8, 1, 256), F32),
             pltpu.VMEM((8, 1, 256), F32),
-            pltpu.VMEM((3, 128, 128), BF),
-            pltpu.VMEM((3, 128), F32),
-            pltpu.VMEM((1, 192), F32),
+            jax.ShapeDtypeStruct((400, 128), F32),
         ],
         name="keep",
     )(
@@ -265,13 +268,13 @@
         location_offsets,
         blend_norm_factor.reshape(1, 192),
     )
+    other_group = lax.ppermute(group, "c", swap)
     ffn_all = lax.all_gather(ffn_own, ("z", "y", "c"), axis=0, tiled=True)
 
     first = lax.all_to_all(own, "y", 0, 0, tiled=True)
     rows = lax.all_to_all(seqs, TP, 0, 0, tiled=True)
     left = [vmem(p) for p in exchange(first[:4].reshape(1, 128, 640), 0)]
     right = [vmem(p) for p in exchange(first[4:].reshape(1, 128, 640), 1)]
-    pieces = left + right
     order = blocks(z)
     near = vmem(rows)
 
@@ -284,39 +287,32 @@
         name="early",
     )(order, near, gain, *left[:3], *right[:3])
     here = jnp.stack([x, c]).astype(jnp.int32)
-    act, own_sq, base = pl.pallas_call(
+    mine, yours, own_sq, base, emis = pl.pallas_call(
         project_kernel,
-        in_specs=[SM, SM] + [VM] * 7,
-        out_specs=[VM] * 3,
+        in_specs=[SM, SM] + [VM] * 13,
+        out_specs=[VM] * 5,
         out_shape=[
-            pltpu.VMEM((256, 384), F32),
+            jax.ShapeDtypeStruct((128, 384), F32),
+            jax.ShapeDtypeStruct((128, 384), F32),
             jax.ShapeDtypeStruct((8, 1, 256), F32),
             jax.ShapeDtypeStruct((2, 128, 256), BF),
+            jax.ShapeDtypeStruct((8, 256, 256), BF),
         ],
-        compiler_params=limit(4),
+        compiler_params=limit(52),
         name="project",
-    )(order, here, near, gain, scales, prior, factor, left[3], right[3])
+    )(order, here, near, gain, scales, prior, factor, *left, *right)
     all_sq = lax.all_to_all(own_sq, TP, 0, 0, tiled=True)
-    kept, sent = pl.pallas_call(
+    theirs = lax.ppermute(yours, "c", swap)
+    other_emis = lax.ppermute(emis, "c", swap)
+    both = pl.pallas_call(
         gate_kernel,
-        in_specs=[SM, SM] + [VM] * 13,
-        out_specs=[VM, VM],
-        out_shape=[jax.ShapeDtypeStruct((8, 128, 256), BF)] * 2,
+        in_specs=[SM] + [VM] * 7,
+        out_specs=VM,
+        out_shape=jax.ShapeDtypeStruct((8, 128, 256), BF),
         scratch_shapes=[pltpu.VMEM((2, 128, 192), BF)],
-        compiler_params=limit(6),
         name="gating",
-    )(
-        order,
-        here,
-        act,
-        all_sq,
-        mats,
-        offs,
-        blend_gain,
-        *pieces,
-    )
-    got = lax.ppermute(sent, "c", swap)
-    both = (kept.astype(F32) + got.astype(F32)).astype(BF).reshape(4, 2, 128, 256)
+    )(here, mine, theirs, all_sq, group, other_group, emis, other_emis)
+    both = both.reshape(4, 2, 128, 256)
     shares = lax.all_to_all(both, "x", 0, 0, tiled=True)
     mid_own = (base.astype(F32) + jnp.sum(shares.astype(F32), axis=0)).astype(BF)
     mid = from_everyone(mid_own, "x").reshape(8, 128, 256)

time: 170 us -> 178 us (1.047)
  blocking collectives: 53.7 us -> 39.7 us
  starting transfers between devices: 53.5 us -> 66.9 us
  Pallas kernels: 20.4 us -> 23.8 us
  waiting for transfers between devices: 25.1 us -> 27.4 us
  local copies, waits for them, and re-layouts: 0.67 us -> 2.52 us
    all_to_all x1 -> x0, blocking collectives: 13.6 us -> none  [on_device(): all_sq = lax.all_to_all(own_sq, TP, 0, 0, tiled=True)]
    ppermute x1 -> x3, starting transfers between devices: 2.52 us -> 10.5 us  [the longest x1 6.21 us: on_device(): other_emis = lax.ppermute(emis, 'c', swap)]
    all_to_all x0 -> x1, starting transfers between devices: none -> 4.72 us  [on_device(): all_sq = lax.all_to_all(own_sq, TP, 0, 0, tiled=True)]
    all_to_all x0 -> x1, waiting for transfers between devices: none -> 4.7 us  [on_device(): all_sq = lax.all_to_all(own_sq, TP, 0, 0, tiled=True)]
    pallas_call x3, Pallas kernels: 5.63 us -> 9.39 us  [the longest x1 4.05 us: on_device(): pl.pallas_call(gate_kernel, in_specs=[SM] + [VM] * 7, out_specs=VM, out_s...]
    unnamed x2 -> x20, local copies, waits for them, and re-layouts: 0.6 us -> 2.45 us
    ppermute x1 -> x3, waiting for transfers between devices: 1.79 us -> 0.01 us  [the longest x1 0.01 us: on_device(): other_group = lax.ppermute(group, 'c', swap)]
  transfers between devices with their start and end apart: 13 -> 16, of which waited for: 7 -> 7; matrix products, arithmetic and copies ran while one was open for 1% -> 1% of each run, Pallas kernels for 6% -> 7%
where the time goes in v8:
time: 178 us; the launch traced here: 177 us
  starting transfers between devices  66.9 us (38%)
  blocking collectives  39.7 us (22%)
  waiting for transfers between devices  27.4 us (15%)
  Pallas kernels  23.8 us (13%)
  between operations  13.6 us (8%)
  other arithmetic  3.2 us (2%)
  local copies, waits for them, and re-layouts  2.52 us (1%)
    ppermute x6, starting transfers between devices, exchange(): batch = lax.ppermute(batch, 'z', turn)  20.6 us
    all_to_all x1, blocking collectives, on_device(): first = lax.all_to_all(own, 'y', 0, 0, tiled=True)  17.6 us
    ppermute x6, waiting for transfers between devices, exchange(): batch = lax.ppermute(batch, 'z', turn)  15.4 us
    ppermute x2, starting transfers between devices, exchange(): got = lax.ppermute(own, 'z', to_pair)  14.6 us
    all_to_all x1, blocking collectives, on_device(): shares = lax.all_to_all(both, 'x', 0, 0, tiled=True)  12 us
    all_to_all x1, blocking collectives, from_everyone(): return lax.all_to_all(copies, axis, split_axis=0, concat_axis=0, tiled=True)  10.1 us
    pallas_call x1, Pallas kernels, on_device(): pl.pallas_call(ffn_kernel, in_specs=[VM, VM, pl.BlockSpec(memory_space=pl...  9.37 us
    all_to_all x1, starting transfers between devices, on_device(): rows = lax.all_to_all(seqs, TP, 0, 0, tiled=True)  8.23 us
  transfers between devices with their start and end apart: 16, of which 7 were waited for; matrix products, arithmetic and copies ran while one was open for 1% of the time, Pallas kernels for 7%

profile of v8, /device:TPU:1, one launch (start us, length us, event | category | flops | bytes accessed | tf_op | source)
XLA Modules:
  0.0 177.2 jit_solution(15105722259926237275)
XLA Ops:
  6.5 1.8 pack_ffn.1
  8.3 1.6 pack.1
  9.9 17.6 %all_to_all.30 = bf16[8,32,640]{2,1,0:T(8,128)(2,1)S(1)} all-to-all(bf16[8,32,640]{2,1,0:T(8,128)(2,1)} %pack.1), channel_id=1, replica_groups=mesh['z'=8,'y'=8,'x'=4,'c'=2] {'y'}, dimensions={0} | all-to-all | bytes 655360 | tf_op jit(solution)/shard_map/all_to_all | solution.py:274
  27.6 5.8 %collective-permute-start = (bf16[1,128,640]{2,1,0:T(8,128)(2,1)S(1)}, bf16[1,128,640]{2,1,0:T(8,128)(2,1)S(1)}, u32[]{:S(2)}, u32[]{:S(2)}) collective-permute-start(bf16[1,128,640]{2,1,0:T(8,128)(2,1)S(1)} %bitcast.34), channel_id=1, source_target_pairs={{0,64},{64,0},{128,192},{192,128},{256,320},{320,256},{384,448},{4... | collective-permute-start | bytes 491528 | tf_op jit(solution)/shard_map/ppermute | solution.py:143
  33.4 8.8 %collective-permute-start.3 = (bf16[1,128,640]{2,1,0:T(8,128)(2,1)S(1)}, bf16[1,128,640]{2,1,0:T(8,128)(2,1)S(1)}, u32[]{:S(2)}, u32[]{:S(2)}) collective-permute-start(bf16[1,128,640]{2,1,0:T(8,128)(2,1)S(1)} %bitcast.32), channel_id=1, source_target_pairs={{0,448},{64,128},{128,64},{192,256},{256,192},{320,384},{384,320},... | collective-permute-start | bytes 491528 | tf_op jit(solution)/shard_map/ppermute | solution.py:143
  42.3 4.6 %collective-permute-start.1 = (bf16[2,128,640]{2,1,0:T(8,128)(2,1)S(1)}, bf16[2,128,640]{2,1,0:T(8,128)(2,1)S(1)}, u32[]{:S(2)}, u32[]{:S(2)}) collective-permute-start(bf16[2,128,640]{2,1,0:T(8,128)(2,1)S(1)} %pad_maximum_fusion.refs_0_), channel_id=1, source_target_pairs={{0,448},{64,128},{128,64},{192,256},{256,192},{320,384},{384,320},... | collective-permute-start | bytes 983048 | tf_op jit(solution)/shard_map/ppermute | solution.py:147
  47.0 1.9 %collective-permute-start.4 = (bf16[2,128,640]{2,1,0:T(8,128)(2,1)S(1)}, bf16[2,128,640]{2,1,0:T(8,128)(2,1)S(1)}, u32[]{:S(2)}, u32[]{:S(2)}) collective-permute-start(bf16[2,128,640]{2,1,0:T(8,128)(2,1)S(1)} %pad_maximum_fusion.1.refs_3_.refs_4_), channel_id=1, source_target_pairs={{0,64},{64,0},{128,192},{192,128},{256,320},{320,256},{384,448},{4... | collective-permute-start | bytes 983048 | tf_op jit(solution)/shard_map/ppermute | solution.py:147
  48.9 2.1 %keep.1 = (bf16[8,256,256]{2,1,0:T(8,128)(2,1)}, f32[1,384]{1,0:T(1,128)S(1)}, f32[8,1,256]{2,1,0:T(1,128)S(1)}, f32[8,1,256]{2,1,0:T(1,128)S(1)}, f32[400,128]{1,0:T(8,128)}) custom-call(bf16[256,256]{1,0:T(8,128)(2,1)} %seq.1, f32[192]{0:T(256)} %conv_s.1, f32[192]{0:T(256)} %blend_s.1, f32[8,1,256]{2,1,0:T(1,128)} %bitcast.38, f32[8,1,256]{2,1,0:T(1,128)} %bitcast.39, ...), custom_call_target="tpu_custom_call" | custom-call | tf_op jit(solution)/shard_map/keep/pallas_call | solution.py:249
  51.0 8.2 %all-to-all-start = ((bf16[8,256,256]{2,1,0:T(8,128)(2,1)}), bf16[8,256,256]{2,1,0:T(8,128)(2,1)S(1)}, u32[]{:S(2)}, u32[]{:S(2)}) async-start(bf16[8,256,256]{2,1,0:T(8,128)(2,1)} %get-tuple-element.17), calls=%async_computation | async-start | bytes 2097152 | tf_op jit(solution)/shard_map/all_to_all | solution.py:275
  59.2 3.6 %collective-permute-start.2 = (bf16[2,128,640]{2,1,0:T(8,128)(2,1)S(1)}, bf16[2,128,640]{2,1,0:T(8,128)(2,1)S(1)}, u32[]{:S(2)}, u32[]{:S(2)}) collective-permute-start(bf16[2,128,640]{2,1,0:T(8,128)(2,1)S(1)} %collective-permute-done.1.refs_1_), channel_id=1, source_target_pairs={{0,64},{64,0},{128,192},{192,128},{256,320},{320,256},{384,448},{4... | collective-permute-start | bytes 983048 | tf_op jit(solution)/shard_map/ppermute | solution.py:147
  62.9 4.2 %collective-permute-start.5 = (bf16[2,128,640]{2,1,0:T(8,128)(2,1)S(1)}, bf16[2,128,640]{2,1,0:T(8,128)(2,1)S(1)}, u32[]{:S(2)}, u32[]{:S(2)}) collective-permute-start(bf16[2,128,640]{2,1,0:T(8,128)(2,1)S(1)} %collective-permute-done.4.refs_4_.refs_5_), channel_id=1, source_target_pairs={{0,448},{64,128},{128,64},{192,256},{256,192},{320,384},{384,320},... | collective-permute-start | bytes 983048 | tf_op jit(solution)/shard_map/ppermute | solution.py:147
  67.1 3.8 %collective-permute-done.2.refs_2_ = bf16[2,128,640]{2,1,0:T(8,128)(2,1)S(1)} collective-permute-done((bf16[2,128,640]{2,1,0:T(8,128)(2,1)S(1)}, bf16[2,128,640]{2,1,0:T(8,128)(2,1)S(1)}, u32[]{:S(2)}, u32[]{:S(2)}) %collective-permute-start.2) | collective-permute-done | bytes 327712 | tf_op jit(solution)/shard_map/ppermute | solution.py:147
  70.9 4.3 %collective-permute-start.6 = (bf16[2,128,640]{2,1,0:T(8,128)(2,1)S(1)}, bf16[2,128,640]{2,1,0:T(8,128)(2,1)S(1)}, u32[]{:S(2)}, u32[]{:S(2)}) collective-permute-start(bf16[2,128,640]{2,1,0:T(8,128)(2,1)S(1)} %collective-permute-done.2.refs_2_), channel_id=1, source_target_pairs={{0,448},{64,128},{128,64},{192,256},{256,192},{320,384},{384,320},... | collective-permute-start | bytes 983048 | tf_op jit(solution)/shard_map/ppermute | solution.py:147
  75.9 1.9 %collective-permute-start.7 = (bf16[2,128,640]{2,1,0:T(8,128)(2,1)S(1)}, bf16[2,128,640]{2,1,0:T(8,128)(2,1)}, u32[]{:S(2)}, u32[]{:S(2)}) collective-permute-start(bf16[2,128,640]{2,1,0:T(8,128)(2,1)S(1)} %collective-permute-done.5.refs_5_.refs_6_), channel_id=1, source_target_pairs={{0,64},{64,0},{128,192},{192,128},{256,320},{320,256},{384,448},{4... | collective-permute-start | bytes 983048 | tf_op jit(solution)/shard_map/ppermute | solution.py:147
  79.1 1.6 early.1
  82.2 8.1 %collective-permute-done.6.refs_3_ = bf16[2,128,640]{2,1,0:T(8,128)(2,1)S(1)} collective-permute-done((bf16[2,128,640]{2,1,0:T(8,128)(2,1)S(1)}, bf16[2,128,640]{2,1,0:T(8,128)(2,1)S(1)}, u32[]{:S(2)}, u32[]{:S(2)}) %collective-permute-start.6) | collective-permute-done | bytes 327712 | tf_op jit(solution)/shard_map/ppermute | solution.py:147
  90.3 2.9 %collective-permute-done.7.refs_7_ = bf16[2,128,640]{2,1,0:T(8,128)(2,1)} collective-permute-done((bf16[2,128,640]{2,1,0:T(8,128)(2,1)S(1)}, bf16[2,128,640]{2,1,0:T(8,128)(2,1)}, u32[]{:S(2)}, u32[]{:S(2)}) %collective-permute-start.7) | collective-permute-done | bytes 327712 | tf_op jit(solution)/shard_map/ppermute | solution.py:147
  93.2 3.2 %project.1 = (f32[128,384]{1,0:T(8,128)}, f32[128,384]{1,0:T(8,128)}, f32[8,1,256]{2,1,0:T(1,128)}, bf16[2,128,256]{2,1,0:T(8,128)(2,1)}, bf16[8,256,256]{2,1,0:T(8,128)(2,1)}) custom-call(s32[2,8]{1,0:T(2,128)} %copy-done.3, s32[2]{0:T(128)} %pad_add_fusion.here.place, bf16[8,256,256]{2,1,0:T(8,128)(2,1)S(1)} %all-to-all-done.x_ref, ...), custom_call_target="tpu_custom_call" | custom-call | tf_op jit(solution)/shard_map/project/pallas_call | solution.py:290
  96.4 6.2 %collective-permute-start.10 = (bf16[8,256,256]{2,1,0:T(8,128)(2,1)}, bf16[8,256,256]{2,1,0:T(8,128)(2,1)S(1)}, u32[]{:S(2)}, u32[]{:S(2)}) collective-permute-start(bf16[8,256,256]{2,1,0:T(8,128)(2,1)} %get-tuple-element.27.my_emis), channel_id=1, source_target_pairs={{0,1},{1,0},{2,3},{3,2},{4,5},{5,4},{6,7},{7,6},{8,9},{9,8},{10,11... | collective-permute-start | bytes 3145736 | tf_op jit(solution)/shard_map/ppermute | solution.py:306
  102.6 1.9 %collective-permute-start.9 = (f32[400,128]{1,0:T(8,128)}, f32[400,128]{1,0:T(8,128)S(1)}, u32[]{:S(2)}, u32[]{:S(2)}) collective-permute-start(f32[400,128]{1,0:T(8,128)} %get-tuple-element.26.my_group), channel_id=1, source_target_pairs={{0,1},{1,0},{2,3},{3,2},{4,5},{5,4},{6,7},{7,6},{8,9},{9,8},{10,11... | collective-permute-start | bytes 614408 | tf_op jit(solution)/shard_map/ppermute | solution.py:271
  104.5 2.4 %collective-permute-start.8 = (f32[128,384]{1,0:T(8,128)}, f32[128,384]{1,0:T(8,128)S(1)}, u32[]{:S(2)}, u32[]{:S(2)}) collective-permute-start(f32[128,384]{1,0:T(8,128)} %get-tuple-element.24), channel_id=1, source_target_pairs={{0,1},{1,0},{2,3},{3,2},{4,5},{5,4},{6,7},{7,6},{8,9},{9,8},{10,11... | collective-permute-start | bytes 589832 | tf_op jit(solution)/shard_map/ppermute | solution.py:305
  107.0 4.7 %all-to-all-start.2 = ((f32[8,1,256]{2,1,0:T(1,128)}), f32[8,1,256]{2,1,0:T(1,128)S(1)}, u32[]{:S(2)}, u32[]{:S(2)}) async-start(f32[8,1,256]{2,1,0:T(1,128)} %get-tuple-element.25), calls=%async_computation.2 | async-start | bytes 16384 | tf_op jit(solution)/shard_map/all_to_all | solution.py:304
  111.7 4.7 %all-to-all-done.2.sq_ref = f32[8,1,256]{2,1,0:T(1,128)S(1)} async-done(((f32[8,1,256]{2,1,0:T(1,128)}), f32[8,1,256]{2,1,0:T(1,128)S(1)}, u32[]{:S(2)}, u32[]{:S(2)}) %all-to-all-start.2) | async-done | bytes 8224 | tf_op jit(solution)/shard_map/all_to_all | solution.py:304
  117.4 4.0 %gating.1 = bf16[8,128,256]{2,1,0:T(8,128)(2,1)} custom-call(s32[2]{0:T(128)} %pad_add_fusion.here.place, f32[128,384]{1,0:T(8,128)} %get-tuple-element.23.mine, f32[128,384]{1,0:T(8,128)} %copy-done.8, f32[8,1,256]{2,1,0:T(1,128)} %copy-done.9, f32[400,128]{1,0:T(8,128)} %get-tuple-element.26.my_group, f32[400,128]{1,0:T(8,128)} %copy-done.7, ...), custom_call_target="tpu_custom_call" | custom-call | tf_op jit(solution)/shard_map/gating/pallas_call | solution.py:307
  121.5 12.0 %all_to_all.31 = bf16[4,2,128,256]{3,2,1,0:T(8,128)(2,1)S(1)} all-to-all(bf16[4,2,128,256]{3,2,1,0:T(8,128)(2,1)} %bitcast.31), channel_id=1, replica_groups=mesh['z'=8,'y'=8,'x'=4,'c'=2] {'x'}, dimensions={0} | all-to-all | bytes 1048576 | tf_op jit(solution)/shard_map/all_to_all | solution.py:316
  133.6 0.9 add_convert_fusion.1
  134.6 10.1 %all_to_all.32 = bf16[4,2,128,256]{3,2,1,0:T(8,128)(2,1)S(1)} all-to-all(bf16[4,2,128,256]{3,2,1,0:T(8,128)(2,1)S(1)} %broadcast_in_dim.2), channel_id=1, replica_groups=mesh['z'=8,'y'=8,'x'=4,'c'=2] {'x'}, dimensions={0} | all-to-all | bytes 1048576 | tf_op jit(solution)/shard_map/all_to_all | solution.py:22
  144.7 9.4 %ffn.1 = bf16[8,128,256]{2,1,0:T(8,128)(2,1)} custom-call(bf16[8,128,256]{2,1,0:T(8,128)(2,1)S(1)} %bitcast.28, f32[8,1,256]{2,1,0:T(1,128)} %copy-done.4, bf16[8,8,2,32,2112]{4,3,2,1,0:T(8,128)(2,1)} %bitcast.29), custom_call_target="tpu_custom_call" | custom-call | tf_op jit(solution)/shard_map/ffn/pallas_call | solution.py:319
  154.0 6.1 %all-to-all-start.5 = ((bf16[8,128,256]{2,1,0:T(8,128)(2,1)}), bf16[8,128,256]{2,1,0:T(8,128)(2,1)S(1)}, u32[]{:S(2)}, u32[]{:S(2)}) async-start(bf16[8,128,256]{2,1,0:T(8,128)(2,1)} %ffn.1), calls=%async_computation.5 | async-start | bytes 1048576 | tf_op jit(solution)/shard_map/all_to_all | solution.py:332
  160.2 2.0 %collective-permute-start.11 = (bf16[128,256]{1,0:T(8,128)(2,1)S(1)}, bf16[128,256]{1,0:T(8,128)(2,1)S(1)}, u32[]{:S(2)}, u32[]{:S(2)}) collective-permute-start(bf16[128,256]{1,0:T(8,128)(2,1)S(1)} %dynamic-slice_bitcast_fusion), channel_id=1, source_target_pairs={{0,1},{1,0},{2,3},{3,2},{4,5},{5,4},{6,7},{7,6},{8,9},{9,8},{10,11... | collective-permute-start | bytes 196616 | tf_op jit(solution)/shard_map/ppermute | solution.py:335
  162.2 1.1 collective-permute-done.11
  163.3 6.2 %all-to-all-done.5 = bf16[8,128,256]{2,1,0:T(8,128)(2,1)S(1)} async-done(((bf16[8,128,256]{2,1,0:T(8,128)(2,1)}), bf16[8,128,256]{2,1,0:T(8,128)(2,1)S(1)}, u32[]{:S(2)}, u32[]{:S(2)}) %all-to-all-start.5) | async-done | bytes 524320 | tf_op jit(solution)/shard_map/all_to_all | solution.py:332
  (44 shorter events, 5.4 us)
Async XLA Ops:
  6.5 138.1 %all-gather.2.cloned.1.call-start = ((), (), s32[]{:S(2)}) async-start(), calls=%async_computation.6 | async-start | bytes 17965056 | tf_op jit(solution)/shard_map/all_gather | solution.py:272
  27.6 14.6 %collective-permute-start = (bf16[1,128,640]{2,1,0:T(8,128)(2,1)S(1)}, bf16[1,128,640]{2,1,0:T(8,128)(2,1)S(1)}, u32[]{:S(2)}, u32[]{:S(2)}) collective-permute-start(bf16[1,128,640]{2,1,0:T(8,128)(2,1)S(1)} %bitcast.34), channel_id=1, source_target_pairs={{0,64},{64,0},{128,192},{192,128},{256,320},{320,256},{384,448},{4... | collective-permute-start | bytes 491528 | tf_op jit(solution)/shard_map/ppermute | solution.py:143
  33.4 13.5 %collective-permute-start.3 = (bf16[1,128,640]{2,1,0:T(8,128)(2,1)S(1)}, bf16[1,128,640]{2,1,0:T(8,128)(2,1)S(1)}, u32[]{:S(2)}, u32[]{:S(2)}) collective-permute-start(bf16[1,128,640]{2,1,0:T(8,128)(2,1)S(1)} %bitcast.32), channel_id=1, source_target_pairs={{0,448},{64,128},{128,64},{192,256},{256,192},{320,384},{384,320},... | collective-permute-start | bytes 491528 | tf_op jit(solution)/shard_map/ppermute | solution.py:143
  42.3 16.9 %collective-permute-start.1 = (bf16[2,128,640]{2,1,0:T(8,128)(2,1)S(1)}, bf16[2,128,640]{2,1,0:T(8,128)(2,1)S(1)}, u32[]{:S(2)}, u32[]{:S(2)}) collective-permute-start(bf16[2,128,640]{2,1,0:T(8,128)(2,1)S(1)} %pad_maximum_fusion.refs_0_), channel_id=1, source_target_pairs={{0,448},{64,128},{128,64},{192,256},{256,192},{320,384},{384,320},... | collective-permute-start | bytes 983048 | tf_op jit(solution)/shard_map/ppermute | solution.py:147
  47.0 15.9 %collective-permute-start.4 = (bf16[2,128,640]{2,1,0:T(8,128)(2,1)S(1)}, bf16[2,128,640]{2,1,0:T(8,128)(2,1)S(1)}, u32[]{:S(2)}, u32[]{:S(2)}) collective-permute-start(bf16[2,128,640]{2,1,0:T(8,128)(2,1)S(1)} %pad_maximum_fusion.1.refs_3_.refs_4_), channel_id=1, source_target_pairs={{0,64},{64,0},{128,192},{192,128},{256,320},{320,256},{384,448},{4... | collective-permute-start | bytes 983048 | tf_op jit(solution)/shard_map/ppermute | solution.py:147
  51.0 8.2 %copy-start.4 = (f32[8,1,256]{2,1,0:T(1,128)}, f32[8,1,256]{2,1,0:T(1,128)S(1)}, u32[]{:S(2)}) copy-start(f32[8,1,256]{2,1,0:T(1,128)S(1)} %get-tuple-element.28.gain) | copy-start | bytes 24580
  51.0 8.2 %copy-start.5 = (f32[1,384]{1,0:T(1,128)}, f32[1,384]{1,0:T(1,128)S(1)}, u32[]{:S(2)}) copy-start(f32[1,384]{1,0:T(1,128)S(1)} %get-tuple-element.19.scales) | copy-start | bytes 4612
  51.0 42.2 %copy-start.2 = (f32[8,1,256]{2,1,0:T(1,128)}, f32[8,1,256]{2,1,0:T(1,128)S(1)}, u32[]{:S(2)}) copy-start(f32[8,1,256]{2,1,0:T(1,128)S(1)} %get-tuple-element.18.gain) | copy-start | bytes 24580
  51.0 28.2 %all-to-all-start = ((bf16[8,256,256]{2,1,0:T(8,128)(2,1)}), bf16[8,256,256]{2,1,0:T(8,128)(2,1)S(1)}, u32[]{:S(2)}, u32[]{:S(2)}) async-start(bf16[8,256,256]{2,1,0:T(8,128)(2,1)} %get-tuple-element.17), calls=%async_computation | async-start | bytes 2097152 | tf_op jit(solution)/shard_map/all_to_all | solution.py:275
  59.2 11.7 %collective-permute-start.2 = (bf16[2,128,640]{2,1,0:T(8,128)(2,1)S(1)}, bf16[2,128,640]{2,1,0:T(8,128)(2,1)S(1)}, u32[]{:S(2)}, u32[]{:S(2)}) collective-permute-start(bf16[2,128,640]{2,1,0:T(8,128)(2,1)S(1)} %collective-permute-done.1.refs_1_), channel_id=1, source_target_pairs={{0,64},{64,0},{128,192},{192,128},{256,320},{320,256},{384,448},{4... | collective-permute-start | bytes 983048 | tf_op jit(solution)/shard_map/ppermute | solution.py:147
  62.9 13.0 %collective-permute-start.5 = (bf16[2,128,640]{2,1,0:T(8,128)(2,1)S(1)}, bf16[2,128,640]{2,1,0:T(8,128)(2,1)S(1)}, u32[]{:S(2)}, u32[]{:S(2)}) collective-permute-start(bf16[2,128,640]{2,1,0:T(8,128)(2,1)S(1)} %collective-permute-done.4.refs_4_.refs_5_), channel_id=1, source_target_pairs={{0,448},{64,128},{128,64},{192,256},{256,192},{320,384},{384,320},... | collective-permute-start | bytes 983048 | tf_op jit(solution)/shard_map/ppermute | solution.py:147
  70.9 19.4 %collective-permute-start.6 = (bf16[2,128,640]{2,1,0:T(8,128)(2,1)S(1)}, bf16[2,128,640]{2,1,0:T(8,128)(2,1)S(1)}, u32[]{:S(2)}, u32[]{:S(2)}) collective-permute-start(bf16[2,128,640]{2,1,0:T(8,128)(2,1)S(1)} %collective-permute-done.2.refs_2_), channel_id=1, source_target_pairs={{0,448},{64,128},{128,64},{192,256},{256,192},{320,384},{384,320},... | collective-permute-start | bytes 983048 | tf_op jit(solution)/shard_map/ppermute | solution.py:147
  75.9 17.3 %collective-permute-start.7 = (bf16[2,128,640]{2,1,0:T(8,128)(2,1)S(1)}, bf16[2,128,640]{2,1,0:T(8,128)(2,1)}, u32[]{:S(2)}, u32[]{:S(2)}) collective-permute-start(bf16[2,128,640]{2,1,0:T(8,128)(2,1)S(1)} %collective-permute-done.5.refs_5_.refs_6_), channel_id=1, source_target_pairs={{0,64},{64,0},{128,192},{192,128},{256,320},{320,256},{384,448},{4... | collective-permute-start | bytes 983048 | tf_op jit(solution)/shard_map/ppermute | solution.py:147
  79.1 14.0 %copy-start.3 = (s32[2,8]{1,0:T(2,128)}, s32[2,8]{1,0:T(2,128)S(1)}, u32[]{:S(2)}) copy-start(s32[2,8]{1,0:T(2,128)S(1)} %add_and_fusion.order) | copy-start | bytes 196
  80.8 0.8 copy-start
  81.5 0.7 copy-start.1
  96.4 20.0 %collective-permute-start.10 = (bf16[8,256,256]{2,1,0:T(8,128)(2,1)}, bf16[8,256,256]{2,1,0:T(8,128)(2,1)S(1)}, u32[]{:S(2)}, u32[]{:S(2)}) collective-permute-start(bf16[8,256,256]{2,1,0:T(8,128)(2,1)} %get-tuple-element.27.my_emis), channel_id=1, source_target_pairs={{0,1},{1,0},{2,3},{3,2},{4,5},{5,4},{6,7},{7,6},{8,9},{9,8},{10,11... | collective-permute-start | bytes 3145736 | tf_op jit(solution)/shard_map/ppermute | solution.py:306
  102.6 9.1 %collective-permute-start.9 = (f32[400,128]{1,0:T(8,128)}, f32[400,128]{1,0:T(8,128)S(1)}, u32[]{:S(2)}, u32[]{:S(2)}) collective-permute-start(f32[400,128]{1,0:T(8,128)} %get-tuple-element.26.my_group), channel_id=1, source_target_pairs={{0,1},{1,0},{2,3},{3,2},{4,5},{5,4},{6,7},{7,6},{8,9},{9,8},{10,11... | collective-permute-start | bytes 614408 | tf_op jit(solution)/shard_map/ppermute | solution.py:271
  104.5 11.8 %collective-permute-start.8 = (f32[128,384]{1,0:T(8,128)}, f32[128,384]{1,0:T(8,128)S(1)}, u32[]{:S(2)}, u32[]{:S(2)}) collective-permute-start(f32[128,384]{1,0:T(8,128)} %get-tuple-element.24), channel_id=1, source_target_pairs={{0,1},{1,0},{2,3},{3,2},{4,5},{5,4},{6,7},{7,6},{8,9},{9,8},{10,11... | collective-permute-start | bytes 589832 | tf_op jit(solution)/shard_map/ppermute | solution.py:305
  107.0 9.4 %all-to-all-start.2 = ((f32[8,1,256]{2,1,0:T(1,128)}), f32[8,1,256]{2,1,0:T(1,128)S(1)}, u32[]{:S(2)}, u32[]{:S(2)}) async-start(f32[8,1,256]{2,1,0:T(1,128)} %get-tuple-element.25), calls=%async_computation.2 | async-start | bytes 16384 | tf_op jit(solution)/shard_map/all_to_all | solution.py:304
  111.7 4.7 %copy-start.7 = (f32[400,128]{1,0:T(8,128)}, f32[400,128]{1,0:T(8,128)S(1)}, u32[]{:S(2)}) copy-start(f32[400,128]{1,0:T(8,128)S(1)} %collective-permute-done.9.their_group) | copy-start | bytes 614404
  116.4 0.6 copy-start.9
  116.4 0.7 copy-start.8
  116.4 1.0 copy-start.6
  154.0 15.5 %all-to-all-start.5 = ((bf16[8,128,256]{2,1,0:T(8,128)(2,1)}), bf16[8,128,256]{2,1,0:T(8,128)(2,1)S(1)}, u32[]{:S(2)}, u32[]{:S(2)}) async-start(bf16[8,128,256]{2,1,0:T(8,128)(2,1)} %ffn.1), calls=%async_computation.5 | async-start | bytes 1048576 | tf_op jit(solution)/shard_map/all_to_all | solution.py:332
  160.2 3.1 %collective-permute-start.11 = (bf16[128,256]{1,0:T(8,128)(2,1)S(1)}, bf16[128,256]{1,0:T(8,128)(2,1)S(1)}, u32[]{:S(2)}, u32[]{:S(2)}) collective-permute-start(bf16[128,256]{1,0:T(8,128)(2,1)S(1)} %dynamic-slice_bitcast_fusion), channel_id=1, source_target_pairs={{0,1},{1,0},{2,3},{3,2},{4,5},{5,4},{6,7},{7,6},{8,9},{9,8},{10,11... | collective-permute-start | bytes 196616 | tf_op jit(solution)/shard_map/ppermute | solution.py:335
Sparse Core Ops, SparseCore 0:
  10.5 116.2 all-gather.1

commit v9 on v6

--- a/solution.py
+++ b/solution.py
@@ -86,7 +86,8 @@
     prior_ref[...] = multiply(found, x_ref, gain, factor, jnp.zeros((256, 384), F32))
 
 
-def project_kernel(order, x_ref, gain, scales, prior, factor, left, right, act_ref, sq_ref):
+def project_kernel(order, here, x_ref, gain, scales, prior, factor, left, right, act_ref, sq_ref, base):
+    base[...] = x_ref[pl.ds(2 * here[0], 2), pl.ds(pl.multiple_of(128 * here[1], 128), 128), :]
     found = spread(order, [left], [right], 6)
     prior = multiply(found, x_ref, gain, factor[:, 0:1], prior[...])
     act = gelu(prior * scales[...])
@@ -96,10 +97,10 @@
     sums = lax.dot_general(
         ones, signal * signal, NT, precision=lax.Precision.HIGHEST, preferred_element_type=F32
     )
-    sq_ref[0] = sums[0:1]
-
-
-def gate_kernel(order, core, act_ref, sq_ref, mats, offs, gain, *refs):
+    sq_ref[...] = jnp.broadcast_to(sums[0:1].reshape(1, 1, 256), (8, 1, 256))
+
+
+def gate_kernel(order, place, act_ref, sq_ref, mats, offs, gain, *refs):
     pieces, kept, sent, gated = refs[:8], refs[8], refs[9], refs[10]
     total = jnp.sum(sq_ref[...], axis=0)
     factor = lax.rsqrt(total / 1536.0 + EPS)
@@ -117,7 +118,7 @@
             gated[b, :, 64 * g : 64 * g + 64] = (
                 act_ref[at, 64 * g : 64 * g + 64] * mixed
             ).astype(BF)
-    here = core[0]
+    here = place[1]
     mine, other = gated[here], gated[1 - here]
     for block, half, ref, k in spread(order, pieces[:4], pieces[4:]):
         piece = ref[k, :, 384:576]
@@ -272,15 +273,20 @@
         compiler_params=limit(4),
         name="early",
     )(order, near, gain, *left[:3], *right[:3])
-    act, own_sq = pl.pallas_call(
+    here = jnp.stack([x, c]).astype(jnp.int32)
+    act, own_sq, base = pl.pallas_call(
         project_kernel,
-        in_specs=[SM] + [VM] * 7,
-        out_specs=[VM, VM],
-        out_shape=[pltpu.VMEM((256, 384), F32), jax.ShapeDtypeStruct((1, 1, 256), F32)],
+        in_specs=[SM, SM] + [VM] * 7,
+        out_specs=[VM] * 3,
+        out_shape=[
+            pltpu.VMEM((256, 384), F32),
+            jax.ShapeDtypeStruct((8, 1, 256), F32),
+            jax.ShapeDtypeStruct((2, 128, 256), BF),
+        ],
         compiler_params=limit(4),
         name="project",
-    )(order, near, gain, scales, prior, factor, left[3], right[3])
-    all_sq = lax.all_gather(own_sq, TP, axis=0, tiled=True)
+    )(order, here, near, gain, scales, prior, factor, left[3], right[3])
+    all_sq = lax.all_to_all(own_sq, TP, 0, 0, tiled=True)
     kept, sent = pl.pallas_call(
         gate_kernel,
         in_specs=[SM, SM] + [VM] * 13,
@@ -291,7 +297,7 @@
         name="gating",
     )(
         order,
-        c.astype(jnp.int32).reshape(1),
+        here,
         act,
         all_sq,
         mats,
@@ -302,7 +308,6 @@
     got = lax.ppermute(sent, "c", swap)
     both = (kept.astype(F32) + got.astype(F32)).astype(BF).reshape(4, 2, 128, 256)
     shares = lax.all_to_all(both, "x", 0, 0, tiled=True)
-    base = lax.dynamic_slice(rows, (2 * x, 128 * c, 0), (2, 128, 256))
     mid_own = (base.astype(F32) + jnp.sum(shares.astype(F32), axis=0)).astype(BF)
     mid = from_everyone(mid_own, "x").reshape(8, 128, 256)
     outs = pl.pallas_call(

time: 172 us -> 168 us (0.977)
  waiting for transfers between devices: 34.3 us -> 24.1 us
  blocking collectives: 43.7 us -> 53.7 us
  starting transfers between devices: 57.9 us -> 55 us
    all_to_all x0 -> x2, blocking collectives: none -> 25.3 us  [the longest x1 13.6 us: on_device(): all_sq = lax.all_to_all(own_sq, TP, 0, 0, tiled=True)]
    all_gather x1 -> x0, blocking collectives: 15 us -> none  [on_device(): all_sq = lax.all_gather(own_sq, TP, axis=0, tiled=True)]
    all_to_all x1 -> x0, waiting for transfers between devices: 9.39 us -> none  [on_device(): shares = lax.all_to_all(both, 'x', 0, 0, tiled=True)]
    all_to_all x1 -> x0, starting transfers between devices: 3.47 us -> none  [on_device(): shares = lax.all_to_all(both, 'x', 0, 0, tiled=True)]
  transfers between devices with their start and end apart: 14 -> 13, of which waited for: 8 -> 7; matrix products, arithmetic and copies ran while one was open for 1% -> 1% of each run, Pallas kernels for 4% -> 4%
where the time goes in v9:
time: 168 us; the launch traced here: 167 us
  starting transfers between devices  55 us (33%)
  blocking collectives  53.7 us (32%)
  waiting for transfers between devices  24.1 us (14%)
  Pallas kernels  18.9 us (11%)
  between operations  13.6 us (8%)
  other arithmetic  1.91 us (1%)
    ppermute x6, starting transfers between devices, exchange(): batch = lax.ppermute(batch, 'z', turn)  21.9 us
    all_to_all x1, blocking collectives, on_device(): first = lax.all_to_all(own, 'y', 0, 0, tiled=True)  17.6 us
    ppermute x6, waiting for transfers between devices, exchange(): batch = lax.ppermute(batch, 'z', turn)  15 us
    ppermute x2, starting transfers between devices, exchange(): got = lax.ppermute(own, 'z', to_pair)  14.6 us
    all_to_all x1, blocking collectives, on_device(): all_sq = lax.all_to_all(own_sq, TP, 0, 0, tiled=True)  13.6 us
    all_to_all x1, blocking collectives, on_device(): shares = lax.all_to_all(both, 'x', 0, 0, tiled=True)  11.7 us
    all_to_all x1, blocking collectives, from_everyone(): return lax.all_to_all(copies, axis, split_axis=0, concat_axis=0, tiled=True)  10.8 us
    pallas_call x1, Pallas kernels, on_device(): pl.pallas_call(ffn_kernel, in_specs=[VM, VM, pl.BlockSpec(memory_space=pl...  9.36 us
  transfers between devices with their start and end apart: 13, of which 7 were waited for; matrix products, arithmetic and copies ran while one was open for 1% of the time, Pallas kernels for 4%

profile of v9, /device:TPU:1, one launch (start us, length us, event | category | flops | bytes accessed | tf_op | source)
XLA Modules:
  0.0 167.4 jit_solution(11618721119012686143)
XLA Ops:
  6.5 2.3 %pack_later.1 = (bf16[32,2112]{1,0:T(8,128)(2,1)}, bf16[8,256,256]{2,1,0:T(8,128)(2,1)}, f32[1,384]{1,0:T(1,128)S(1)}, f32[8,1,256]{2,1,0:T(1,128)S(1)}, f32[8,1...) custom-call(f32[32,704]{1,0:T(8,128)} %valve.1, ...), custom_call_target="tpu_custom_call" | custom-call | tf_op jit(solution)/shard_map/pack_later/pallas_call | solution.py:227
  8.9 1.6 pack.1
  10.5 17.6 %all_to_all.30 = bf16[8,32,640]{2,1,0:T(8,128)(2,1)S(1)} all-to-all(bf16[8,32,640]{2,1,0:T(8,128)(2,1)} %pack.1), channel_id=1, replica_groups=mesh['z'=8,'y'=8,'x'=4,'c'=2] {'y'}, dimensions={0} | all-to-all | bytes 655360 | tf_op jit(solution)/shard_map/all_to_all | solution.py:260
  28.2 5.8 %collective-permute-start = (bf16[1,128,640]{2,1,0:T(8,128)(2,1)S(1)}, bf16[1,128,640]{2,1,0:T(8,128)(2,1)S(1)}, u32[]{:S(2)}, u32[]{:S(2)}) collective-permute-start(bf16[1,128,640]{2,1,0:T(8,128)(2,1)S(1)} %bitcast.34), channel_id=1, source_target_pairs={{0,64},{64,0},{128,192},{192,128},{256,320},{320,256},{384,448},{4... | collective-permute-start | bytes 491528 | tf_op jit(solution)/shard_map/ppermute | solution.py:135
  33.9 8.8 %collective-permute-start.3 = (bf16[1,128,640]{2,1,0:T(8,128)(2,1)S(1)}, bf16[1,128,640]{2,1,0:T(8,128)(2,1)S(1)}, u32[]{:S(2)}, u32[]{:S(2)}) collective-permute-start(bf16[1,128,640]{2,1,0:T(8,128)(2,1)S(1)} %bitcast.32), channel_id=1, source_target_pairs={{0,448},{64,128},{128,64},{192,256},{256,192},{320,384},{384,320},... | collective-permute-start | bytes 491528 | tf_op jit(solution)/shard_map/ppermute | solution.py:135
  42.9 4.2 %collective-permute-start.1 = (bf16[2,128,640]{2,1,0:T(8,128)(2,1)S(1)}, bf16[2,128,640]{2,1,0:T(8,128)(2,1)S(1)}, u32[]{:S(2)}, u32[]{:S(2)}) collective-permute-start(bf16[2,128,640]{2,1,0:T(8,128)(2,1)S(1)} %pad_maximum_fusion.refs_0_), channel_id=1, source_target_pairs={{0,448},{64,128},{128,64},{192,256},{256,192},{320,384},{384,320},... | collective-permute-start | bytes 983048 | tf_op jit(solution)/shard_map/ppermute | solution.py:139
  47.1 1.9 %collective-permute-start.4 = (bf16[2,128,640]{2,1,0:T(8,128)(2,1)S(1)}, bf16[2,128,640]{2,1,0:T(8,128)(2,1)S(1)}, u32[]{:S(2)}, u32[]{:S(2)}) collective-permute-start(bf16[2,128,640]{2,1,0:T(8,128)(2,1)S(1)} %pad_maximum_fusion.1.refs_3_.refs_4_), channel_id=1, source_target_pairs={{0,64},{64,0},{128,192},{192,128},{256,320},{320,256},{384,448},{4... | collective-permute-start | bytes 983048 | tf_op jit(solution)/shard_map/ppermute | solution.py:139
  49.1 8.5 %all-to-all-start = ((bf16[8,256,256]{2,1,0:T(8,128)(2,1)}), bf16[8,256,256]{2,1,0:T(8,128)(2,1)S(1)}, u32[]{:S(2)}, u32[]{:S(2)}) async-start(bf16[8,256,256]{2,1,0:T(8,128)(2,1)} %get-tuple-element.20), calls=%async_computation | async-start | bytes 2097152 | tf_op jit(solution)/shard_map/all_to_all | solution.py:261
  57.6 3.6 %collective-permute-start.2 = (bf16[2,128,640]{2,1,0:T(8,128)(2,1)S(1)}, bf16[2,128,640]{2,1,0:T(8,128)(2,1)S(1)}, u32[]{:S(2)}, u32[]{:S(2)}) collective-permute-start(bf16[2,128,640]{2,1,0:T(8,128)(2,1)S(1)} %collective-permute-done.1.refs_1_), channel_id=1, source_target_pairs={{0,64},{64,0},{128,192},{192,128},{256,320},{320,256},{384,448},{4... | collective-permute-start | bytes 983048 | tf_op jit(solution)/shard_map/ppermute | solution.py:139
  61.2 5.1 %collective-permute-start.5 = (bf16[2,128,640]{2,1,0:T(8,128)(2,1)S(1)}, bf16[2,128,640]{2,1,0:T(8,128)(2,1)}, u32[]{:S(2)}, u32[]{:S(2)}) collective-permute-start(bf16[2,128,640]{2,1,0:T(8,128)(2,1)S(1)} %collective-permute-done.4.refs_4_.refs_5_), channel_id=1, source_target_pairs={{0,448},{64,128},{128,64},{192,256},{256,192},{320,384},{384,320},... | collective-permute-start | bytes 983048 | tf_op jit(solution)/shard_map/ppermute | solution.py:139
  66.3 2.3 %collective-permute-done.2.refs_2_ = bf16[2,128,640]{2,1,0:T(8,128)(2,1)S(1)} collective-permute-done((bf16[2,128,640]{2,1,0:T(8,128)(2,1)S(1)}, bf16[2,128,640]{2,1,0:T(8,128)(2,1)S(1)}, u32[]{:S(2)}, u32[]{:S(2)}) %collective-permute-start.2) | collective-permute-done | bytes 327712 | tf_op jit(solution)/shard_map/ppermute | solution.py:139
  68.6 5.2 %collective-permute-start.6 = (bf16[2,128,640]{2,1,0:T(8,128)(2,1)S(1)}, bf16[2,128,640]{2,1,0:T(8,128)(2,1)S(1)}, u32[]{:S(2)}, u32[]{:S(2)}) collective-permute-start(bf16[2,128,640]{2,1,0:T(8,128)(2,1)S(1)} %collective-permute-done.2.refs_2_), channel_id=1, source_target_pairs={{0,448},{64,128},{128,64},{192,256},{256,192},{320,384},{384,320},... | collective-permute-start | bytes 983048 | tf_op jit(solution)/shard_map/ppermute | solution.py:139
  73.8 0.5 collective-permute-done.5.refs_5_.refs_6_
  74.3 1.9 %collective-permute-start.7 = (bf16[2,128,640]{2,1,0:T(8,128)(2,1)}, bf16[2,128,640]{2,1,0:T(8,128)(2,1)S(1)}, u32[]{:S(2)}, u32[]{:S(2)}) collective-permute-start(bf16[2,128,640]{2,1,0:T(8,128)(2,1)} %collective-permute-done.5.refs_5_.refs_6_), channel_id=1, source_target_pairs={{0,64},{64,0},{128,192},{192,128},{256,320},{320,256},{384,448},{4... | collective-permute-start | bytes 983048 | tf_op jit(solution)/shard_map/ppermute | solution.py:139
  76.3 0.7 add_and_fusion.order
  77.0 2.0 %early.1 = (f32[256,384]{1,0:T(8,128)S(1)}, f32[256,128]{1,0:T(8,128)S(1)}) custom-call(s32[2,8]{1,0:T(2,128)S(1)} %add_and_fusion.order, bf16[8,256,256]{2,1,0:T(8,128)(2,1)S(1)} %all-to-all-done.x_ref, f32[8,1,256]{2,1,0:T(1,128)S(1)} %get-tuple-element.21.gain, bf16[2,128,640]{2,1,0:T(8,128)(2,1)S(1)} %pad_maximum_fusion.refs_0_, ...), custom_call_target="tpu_custom_call" | custom-call | tf_op jit(solution)/shard_map/early/pallas_call | solution.py:268
  79.1 9.3 %collective-permute-done.6.left.refs_3_ = bf16[2,128,640]{2,1,0:T(8,128)(2,1)S(1)} collective-permute-done((bf16[2,128,640]{2,1,0:T(8,128)(2,1)S(1)}, bf16[2,128,640]{2,1,0:T(8,128)(2,1)S(1)}, u32[]{:S(2)}, u32[]{:S(2)}) %collective-permute-start.6) | collective-permute-done | bytes 327712 | tf_op jit(solution)/shard_map/ppermute | solution.py:139
  88.3 3.0 %collective-permute-done.7.right.refs_7_ = bf16[2,128,640]{2,1,0:T(8,128)(2,1)S(1)} collective-permute-done((bf16[2,128,640]{2,1,0:T(8,128)(2,1)}, bf16[2,128,640]{2,1,0:T(8,128)(2,1)S(1)}, u32[]{:S(2)}, u32[]{:S(2)}) %collective-permute-start.7) | collective-permute-done | bytes 327712 | tf_op jit(solution)/shard_map/ppermute | solution.py:139
  91.3 1.5 project.1
  92.8 13.6 %all_to_all.31.sq_ref = f32[8,1,256]{2,1,0:T(1,128)S(1)} all-to-all(f32[8,1,256]{2,1,0:T(1,128)S(1)} %get-tuple-element.27), channel_id=1, replica_groups=mesh['z'=8,'y'=8,'x'=4,'c'=2] {'x','c'}, dimensions={0} | all-to-all | bytes 16384 | tf_op jit(solution)/shard_map/all_to_all | solution.py:289
  106.4 2.1 %gating.1 = (bf16[8,128,256]{2,1,0:T(8,128)(2,1)S(1)}, bf16[8,128,256]{2,1,0:T(8,128)(2,1)S(1)}) custom-call(s32[2,8]{1,0:T(2,128)S(1)} %add_and_fusion.order, s32[2]{0:T(128)S(1)} %pad_add_fusion.here.place, f32[256,384]{1,0:T(8,128)S(1)} %get-tuple-element.26.act_ref, f32[8,1,256]{2,1,0:T(1,128)S(1)} %all_to_all.31.sq_ref, ...), custom_call_target="tpu_custom_call" | custom-call | tf_op jit(solution)/shard_map/gating/pallas_call | solution.py:290
  108.5 2.5 %collective-permute-start.8 = (bf16[8,128,256]{2,1,0:T(8,128)(2,1)S(1)}, bf16[8,128,256]{2,1,0:T(8,128)(2,1)S(1)}, u32[]{:S(2)}, u32[]{:S(2)}) collective-permute-start(bf16[8,128,256]{2,1,0:T(8,128)(2,1)S(1)} %get-tuple-element.32), channel_id=1, source_target_pairs={{0,1},{1,0},{2,3},{3,2},{4,5},{5,4},{6,7},{7,6},{8,9},{9,8},{10,11... | collective-permute-start | bytes 1572872 | tf_op jit(solution)/shard_map/ppermute | solution.py:308
  111.0 1.8 %collective-permute-done.8 = bf16[8,128,256]{2,1,0:T(8,128)(2,1)S(1)} collective-permute-done((bf16[8,128,256]{2,1,0:T(8,128)(2,1)S(1)}, bf16[8,128,256]{2,1,0:T(8,128)(2,1)S(1)}, u32[]{:S(2)}, u32[]{:S(2)}) %collective-permute-start.8) | collective-permute-done | bytes 524320 | tf_op jit(solution)/shard_map/ppermute | solution.py:308
  112.8 0.1 add_convert_fusion
  112.9 11.7 %all_to_all.32 = bf16[4,2,128,256]{3,2,1,0:T(8,128)(2,1)S(1)} all-to-all(bf16[4,2,128,256]{3,2,1,0:T(8,128)(2,1)S(1)} %bitcast.30), channel_id=1, replica_groups=mesh['z'=8,'y'=8,'x'=4,'c'=2] {'x'}, dimensions={0} | all-to-all | bytes 1048576 | tf_op jit(solution)/shard_map/all_to_all | solution.py:310
  124.8 10.8 %all_to_all.33 = bf16[4,2,128,256]{3,2,1,0:T(8,128)(2,1)S(1)} all-to-all(bf16[4,2,128,256]{3,2,1,0:T(8,128)(2,1)S(1)} %broadcast_in_dim.2), channel_id=1, replica_groups=mesh['z'=8,'y'=8,'x'=4,'c'=2] {'x'}, dimensions={0} | all-to-all | bytes 1048576 | tf_op jit(solution)/shard_map/all_to_all | solution.py:22
  135.6 9.4 %ffn.1 = bf16[8,128,256]{2,1,0:T(8,128)(2,1)} custom-call(bf16[8,128,256]{2,1,0:T(8,128)(2,1)S(1)} %bitcast.28, f32[8,1,256]{2,1,0:T(1,128)} %copy-done, bf16[8,8,2,32,2112]{4,3,2,1,0:T(8,128)(2,1)} %bitcast.29), custom_call_target="tpu_custom_call" | custom-call | tf_op jit(solution)/shard_map/ffn/pallas_call | solution.py:313
  145.0 5.4 %all-to-all-start.5 = ((bf16[8,128,256]{2,1,0:T(8,128)(2,1)}), bf16[8,128,256]{2,1,0:T(8,128)(2,1)S(1)}, u32[]{:S(2)}, u32[]{:S(2)}) async-start(bf16[8,128,256]{2,1,0:T(8,128)(2,1)} %ffn.1), calls=%async_computation.5 | async-start | bytes 1048576 | tf_op jit(solution)/shard_map/all_to_all | solution.py:326
  150.4 2.0 %collective-permute-start.9 = (bf16[128,256]{1,0:T(8,128)(2,1)S(1)}, bf16[128,256]{1,0:T(8,128)(2,1)S(1)}, u32[]{:S(2)}, u32[]{:S(2)}) collective-permute-start(bf16[128,256]{1,0:T(8,128)(2,1)S(1)} %dynamic-slice_bitcast_fusion), channel_id=1, source_target_pairs={{0,1},{1,0},{2,3},{3,2},{4,5},{5,4},{6,7},{7,6},{8,9},{9,8},{10,11... | collective-permute-start | bytes 196616 | tf_op jit(solution)/shard_map/ppermute | solution.py:329
  152.4 1.1 collective-permute-done.9
  153.5 6.2 %all-to-all-done.5 = bf16[8,128,256]{2,1,0:T(8,128)(2,1)S(1)} async-done(((bf16[8,128,256]{2,1,0:T(8,128)(2,1)}), bf16[8,128,256]{2,1,0:T(8,128)(2,1)S(1)}, u32[]{:S(2)}, u32[]{:S(2)}) %all-to-all-start.5) | async-done | bytes 524320 | tf_op jit(solution)/shard_map/all_to_all | solution.py:326
  159.8 0.7 add_convert_fusion.1
  (21 shorter events, 0.5 us)
Async XLA Ops:
  6.5 129.1 %all-gather.2.cloned.1.call-start = ((), (), s32[]{:S(2)}) async-start(), calls=%async_computation.6 | async-start | bytes 17965056 | tf_op jit(solution)/shard_map/all_gather | solution.py:258
  8.9 40.2 %copy-start = (f32[8,1,256]{2,1,0:T(1,128)}, f32[8,1,256]{2,1,0:T(1,128)S(1)}, u32[]{:S(2)}) copy-start(f32[8,1,256]{2,1,0:T(1,128)S(1)} %get-tuple-element.33.gain) | copy-start | bytes 24580
  28.2 14.6 %collective-permute-start = (bf16[1,128,640]{2,1,0:T(8,128)(2,1)S(1)}, bf16[1,128,640]{2,1,0:T(8,128)(2,1)S(1)}, u32[]{:S(2)}, u32[]{:S(2)}) collective-permute-start(bf16[1,128,640]{2,1,0:T(8,128)(2,1)S(1)} %bitcast.34), channel_id=1, source_target_pairs={{0,64},{64,0},{128,192},{192,128},{256,320},{320,256},{384,448},{4... | collective-permute-start | bytes 491528 | tf_op jit(solution)/shard_map/ppermute | solution.py:135
  33.9 13.1 %collective-permute-start.3 = (bf16[1,128,640]{2,1,0:T(8,128)(2,1)S(1)}, bf16[1,128,640]{2,1,0:T(8,128)(2,1)S(1)}, u32[]{:S(2)}, u32[]{:S(2)}) collective-permute-start(bf16[1,128,640]{2,1,0:T(8,128)(2,1)S(1)} %bitcast.32), channel_id=1, source_target_pairs={{0,448},{64,128},{128,64},{192,256},{256,192},{320,384},{384,320},... | collective-permute-start | bytes 491528 | tf_op jit(solution)/shard_map/ppermute | solution.py:135
  42.9 14.7 %collective-permute-start.1 = (bf16[2,128,640]{2,1,0:T(8,128)(2,1)S(1)}, bf16[2,128,640]{2,1,0:T(8,128)(2,1)S(1)}, u32[]{:S(2)}, u32[]{:S(2)}) collective-permute-start(bf16[2,128,640]{2,1,0:T(8,128)(2,1)S(1)} %pad_maximum_fusion.refs_0_), channel_id=1, source_target_pairs={{0,448},{64,128},{128,64},{192,256},{256,192},{320,384},{384,320},... | collective-permute-start | bytes 983048 | tf_op jit(solution)/shard_map/ppermute | solution.py:139
  47.1 14.1 %collective-permute-start.4 = (bf16[2,128,640]{2,1,0:T(8,128)(2,1)S(1)}, bf16[2,128,640]{2,1,0:T(8,128)(2,1)S(1)}, u32[]{:S(2)}, u32[]{:S(2)}) collective-permute-start(bf16[2,128,640]{2,1,0:T(8,128)(2,1)S(1)} %pad_maximum_fusion.1.refs_3_.refs_4_), channel_id=1, source_target_pairs={{0,64},{64,0},{128,192},{192,128},{256,320},{320,256},{384,448},{4... | collective-permute-start | bytes 983048 | tf_op jit(solution)/shard_map/ppermute | solution.py:139
  49.1 27.9 %all-to-all-start = ((bf16[8,256,256]{2,1,0:T(8,128)(2,1)}), bf16[8,256,256]{2,1,0:T(8,128)(2,1)S(1)}, u32[]{:S(2)}, u32[]{:S(2)}) async-start(bf16[8,256,256]{2,1,0:T(8,128)(2,1)} %get-tuple-element.20), calls=%async_computation | async-start | bytes 2097152 | tf_op jit(solution)/shard_map/all_to_all | solution.py:261
  57.6 11.0 %collective-permute-start.2 = (bf16[2,128,640]{2,1,0:T(8,128)(2,1)S(1)}, bf16[2,128,640]{2,1,0:T(8,128)(2,1)S(1)}, u32[]{:S(2)}, u32[]{:S(2)}) collective-permute-start(bf16[2,128,640]{2,1,0:T(8,128)(2,1)S(1)} %collective-permute-done.1.refs_1_), channel_id=1, source_target_pairs={{0,64},{64,0},{128,192},{192,128},{256,320},{320,256},{384,448},{4... | collective-permute-start | bytes 983048 | tf_op jit(solution)/shard_map/ppermute | solution.py:139
  61.2 13.1 %collective-permute-start.5 = (bf16[2,128,640]{2,1,0:T(8,128)(2,1)S(1)}, bf16[2,128,640]{2,1,0:T(8,128)(2,1)}, u32[]{:S(2)}, u32[]{:S(2)}) collective-permute-start(bf16[2,128,640]{2,1,0:T(8,128)(2,1)S(1)} %collective-permute-done.4.refs_4_.refs_5_), channel_id=1, source_target_pairs={{0,448},{64,128},{128,64},{192,256},{256,192},{320,384},{384,320},... | collective-permute-start | bytes 983048 | tf_op jit(solution)/shard_map/ppermute | solution.py:139
  68.6 19.7 %collective-permute-start.6 = (bf16[2,128,640]{2,1,0:T(8,128)(2,1)S(1)}, bf16[2,128,640]{2,1,0:T(8,128)(2,1)S(1)}, u32[]{:S(2)}, u32[]{:S(2)}) collective-permute-start(bf16[2,128,640]{2,1,0:T(8,128)(2,1)S(1)} %collective-permute-done.2.refs_2_), channel_id=1, source_target_pairs={{0,448},{64,128},{128,64},{192,256},{256,192},{320,384},{384,320},... | collective-permute-start | bytes 983048 | tf_op jit(solution)/shard_map/ppermute | solution.py:139
  74.3 17.0 %collective-permute-start.7 = (bf16[2,128,640]{2,1,0:T(8,128)(2,1)}, bf16[2,128,640]{2,1,0:T(8,128)(2,1)S(1)}, u32[]{:S(2)}, u32[]{:S(2)}) collective-permute-start(bf16[2,128,640]{2,1,0:T(8,128)(2,1)} %collective-permute-done.5.refs_5_.refs_6_), channel_id=1, source_target_pairs={{0,64},{64,0},{128,192},{192,128},{256,320},{320,256},{384,448},{4... | collective-permute-start | bytes 983048 | tf_op jit(solution)/shard_map/ppermute | solution.py:139
  108.5 4.3 %collective-permute-start.8 = (bf16[8,128,256]{2,1,0:T(8,128)(2,1)S(1)}, bf16[8,128,256]{2,1,0:T(8,128)(2,1)S(1)}, u32[]{:S(2)}, u32[]{:S(2)}) collective-permute-start(bf16[8,128,256]{2,1,0:T(8,128)(2,1)S(1)} %get-tuple-element.32), channel_id=1, source_target_pairs={{0,1},{1,0},{2,3},{3,2},{4,5},{5,4},{6,7},{7,6},{8,9},{9,8},{10,11... | collective-permute-start | bytes 1572872 | tf_op jit(solution)/shard_map/ppermute | solution.py:308
  145.0 14.8 %all-to-all-start.5 = ((bf16[8,128,256]{2,1,0:T(8,128)(2,1)}), bf16[8,128,256]{2,1,0:T(8,128)(2,1)S(1)}, u32[]{:S(2)}, u32[]{:S(2)}) async-start(bf16[8,128,256]{2,1,0:T(8,128)(2,1)} %ffn.1), calls=%async_computation.5 | async-start | bytes 1048576 | tf_op jit(solution)/shard_map/all_to_all | solution.py:326
  150.4 3.1 %collective-permute-start.9 = (bf16[128,256]{1,0:T(8,128)(2,1)S(1)}, bf16[128,256]{1,0:T(8,128)(2,1)S(1)}, u32[]{:S(2)}, u32[]{:S(2)}) collective-permute-start(bf16[128,256]{1,0:T(8,128)(2,1)S(1)} %dynamic-slice_bitcast_fusion), channel_id=1, source_target_pairs={{0,1},{1,0},{2,3},{3,2},{4,5},{5,4},{6,7},{7,6},{8,9},{9,8},{10,11... | collective-permute-start | bytes 196616 | tf_op jit(solution)/shard_map/ppermute | solution.py:329
Sparse Core Ops, SparseCore 0:
  10.5 115.3 all-gather.1
